TPU v7x, 768 devices: a whole 4x8x12 slice. The times are simulated.
768 devices in a mesh: sp: 384 (over z, y, x), tp: 2 (over core).
Axes of the slice: x: 4, y: 8, z: 12, core: 2. Of those that a mesh axis runs over, the one named last changes fastest.
Arguments:
- queries: bfloat16 [98304, 512], P('sp', 'tp'), may hold values from -6 to 6
- keys: bfloat16 [98304, 512], P('sp', 'tp'), may hold values from -6 to 6
- values: bfloat16 [98304, 512], P('sp', 'tp'), may hold values from -6 to 6
- gains: float32 [2, 128], replicated, may hold values from 0.1 to 1.9
- bias_table: float32 [192, 4], P(None, 'tp'), may hold values from -6 to 270
- d_out: bfloat16 [98304, 512], P('sp', 'tp'), may hold values from -32 to 32
Outputs:
- d_queries: bfloat16 [98304, 512], P('sp', 'tp')
- d_keys: bfloat16 [98304, 512], P('sp', 'tp')
- d_values: bfloat16 [98304, 512], P('sp', 'tp')
- d_table: float32 [192, 4], P(None, 'tp')
- d_gains: float32 [2, 128], replicated
All inputs are finite; a program needn't handle non-finite values.
Results may differ from a plain program's by a relative error of at most 0.008.
Values may be sent and summed in bfloat16 or wider, within the bound.
A program may use at most 32 MiB of HBM per device.

v0:
```python
import functools

import jax
import jax.numpy as jnp
from jax import lax
from jax.sharding import Mesh
from jax.sharding import PartitionSpec as P

HEAD_DIM = 128
SEG = 64
LEFT = 4
MAX_REL = 128
SP = ("sp_0", "sp_1", "sp_2")
SP_TP = ("sp_0", "sp_1", "sp_2", "tp")


EPSILON = 1e-06


def shifted(block, axis, distance):
    devices = range(lax.axis_size(axis))
    route = [(i - distance, i) for i in devices if i - distance in devices]
    return lax.ppermute(block, axis, route)


def over_axes(value, axes):
    return functools.reduce(lax.psum, axes, value)


def norm_rows(row_block, gain_vec):
    row_count = row_block.shape[0]
    widened = row_block.astype(jnp.float32).reshape(row_count, -1, HEAD_DIM)
    inv_rms = lax.rsqrt(jnp.mean(widened * widened, axis=-1, keepdims=True) + EPSILON)
    unit_part = widened * inv_rms
    return ((unit_part * gain_vec).astype(jnp.bfloat16).reshape(row_count, -1), unit_part, inv_rms)


def norm_back(d_normed, unit_part, inv_rms, gain_vec):
    d_unit = d_normed * gain_vec
    d_rows = inv_rms * (d_unit - unit_part * jnp.mean(d_unit * unit_part, axis=-1, keepdims=True))
    return (
        d_rows.reshape(unit_part.shape[0], -1).astype(jnp.bfloat16),
        jnp.sum(d_normed * unit_part, axis=(0, 1)),
    )


def build_bias(table_heads):
    head_count, entries = table_heads.shape
    last_entry = table_heads[:, entries - 1 :]
    padded = jnp.concatenate(
        [table_heads, jnp.broadcast_to(last_entry, (head_count, SEG - 1))], axis=1
    )
    length = entries + SEG - 1
    repeated = jnp.tile(padded, (1, SEG + 1))[:, : SEG * (length + 1)]
    hankel = repeated.reshape(head_count, SEG, length + 1)[:, :, :entries]
    near_part = hankel[:, :, ::-1]
    far_part = jnp.broadcast_to(last_entry[:, :, None], (head_count, SEG, LEFT * SEG - MAX_REL))
    return jnp.concatenate([far_part, near_part], axis=2)


def table_grad(d_band):
    head_count = d_band.shape[0]
    far_width = LEFT * SEG - MAX_REL
    far_total = jnp.sum(d_band[:, :, :far_width], axis=(1, 2))
    flipped = d_band[:, :, far_width:][:, :, ::-1]
    entries = flipped.shape[2]
    width = entries + SEG
    padded = jnp.pad(flipped, ((0, 0), (0, 0), (0, SEG)))
    skewed = padded.reshape(head_count, SEG * width)[:, : SEG * (width - 1)].reshape(
        head_count, SEG, width - 1
    )
    columns = jnp.sum(skewed, axis=1)
    tail_sum = jnp.sum(columns[:, entries - 1 :], axis=1) + far_total
    return jnp.concatenate([columns[:, : entries - 1], tail_sum[:, None]], axis=1).T


def band_of(rows_ext, seg_count):
    feature_count = rows_ext.shape[1]
    segments = rows_ext.reshape(LEFT + seg_count, SEG, feature_count)
    stacked = jnp.stack(
        [segments[offset : offset + seg_count] for offset in range(LEFT + 1)], axis=1
    )
    return stacked.reshape(seg_count, (LEFT + 1) * SEG, feature_count)


def unband(grad_band, seg_count):
    pieces = grad_band.reshape(seg_count, LEFT + 1, SEG, -1)
    summed = jnp.zeros((LEFT + seg_count, SEG, pieces.shape[3]), jnp.float32)
    for offset in range(LEFT + 1):
        summed = summed + jnp.pad(pieces[:, offset], ((offset, LEFT - offset), (0, 0), (0, 0)))
    return summed.reshape((LEFT + seg_count) * SEG, -1)


def band_grads(q_norm, d_out, k_ext, v_ext, bias_tiles, key_valid):
    seg_count = q_norm.shape[0] // SEG
    head_count = bias_tiles.shape[0]
    factor = HEAD_DIM ** (-0.5)
    q_seg = q_norm.reshape(seg_count, SEG, head_count, HEAD_DIM)
    do_seg = d_out.reshape(seg_count, SEG, head_count, HEAD_DIM)
    k_band = band_of(k_ext, seg_count).reshape(seg_count, -1, head_count, HEAD_DIM)
    v_band = band_of(v_ext, seg_count).reshape(seg_count, -1, head_count, HEAD_DIM)
    scores = (
        jnp.einsum("cihd,cjhd->chij", q_seg, k_band, preferred_element_type=jnp.float32) * factor
        + bias_tiles[None]
    )
    scores = jnp.where(key_valid, scores, -jnp.inf)
    row_max = jnp.max(scores, axis=-1, keepdims=True)
    log_total = row_max + jnp.log(jnp.sum(jnp.exp(scores - row_max), axis=-1, keepdims=True))
    prob = jnp.exp(scores - log_total)
    d_prob = jnp.einsum("cihd,cjhd->chij", do_seg, v_band, preferred_element_type=jnp.float32)
    row_delta = jnp.sum(prob * d_prob, axis=-1, keepdims=True)
    d_score = prob * (d_prob - row_delta)
    prob_low = prob.astype(jnp.bfloat16)
    d_low = d_score.astype(jnp.bfloat16)
    grad_v = jnp.einsum("chij,cihd->cjhd", prob_low, do_seg, preferred_element_type=jnp.float32)
    grad_k = (
        jnp.einsum("chij,cihd->cjhd", d_low, q_seg, preferred_element_type=jnp.float32) * factor
    )
    grad_q = (
        jnp.einsum("chij,cjhd->cihd", d_low, k_band, preferred_element_type=jnp.float32) * factor
    )
    grad_q = grad_q.reshape(seg_count * SEG, head_count, HEAD_DIM)
    return (
        grad_q,
        unband(grad_k, seg_count),
        unband(grad_v, seg_count),
        jnp.sum(d_score, axis=0),
        log_total,
        row_delta,
    )


def local(queries, keys, values, gains, bias_table, d_out):
    row_count, feature_count = queries.shape
    head_count = feature_count // HEAD_DIM
    tail_rows = LEFT * SEG
    seg_count = row_count // SEG
    device_slot = lax.axis_index(SP)
    q_norm, q_unit, q_rms = norm_rows(queries, gains[0])
    k_norm, k_unit, k_rms = norm_rows(keys, gains[1])
    earlier_k, earlier_v = shifted((k_norm, values), SP, 1)
    k_ext = jnp.concatenate([earlier_k, k_norm])
    v_ext = jnp.concatenate([earlier_v, values])
    bias_tiles = build_bias(bias_table.T)
    band_seg = jnp.arange((LEFT + 1) * SEG, dtype=jnp.int32) // SEG
    key_seg = (
        device_slot * seg_count
        + jnp.arange(seg_count, dtype=jnp.int32)[:, None]
        - LEFT
        + band_seg[None, :]
    )
    key_valid = (key_seg >= 0)[:, None, None, :]
    d_qn, dk_ext, dv_ext, d_band, log_total, row_delta = band_grads(
        q_norm, d_out, k_ext, v_ext, bias_tiles, key_valid
    )
    dk_own = dk_ext[tail_rows:]
    dv_own = dv_ext[tail_rows:]
    back_k, back_v = (
        shifted(dk_ext[:tail_rows].astype(jnp.bfloat16), SP, -1).astype(jnp.float32),
        shifted(dv_ext[:tail_rows].astype(jnp.bfloat16), SP, -1).astype(jnp.float32),
    )
    dk_total = dk_own + back_k
    dv_total = dv_own + back_v
    d_queries, gain_q = norm_back(d_qn, q_unit, q_rms, gains[0])
    d_keys, gain_k = norm_back(
        dk_total.reshape(row_count, head_count, HEAD_DIM), k_unit, k_rms, gains[1]
    )
    d_values = dv_total.astype(jnp.bfloat16)
    table_part = table_grad(d_band)
    gain_part = jnp.stack([gain_q, gain_k])
    d_table = over_axes(table_part, SP)
    d_gains = over_axes(gain_part, SP_TP)
    return (d_queries, d_keys, d_values, d_table, d_gains)


def solution(mesh):
    split = Mesh(mesh.devices.reshape(12, 8, 4, mesh.shape["tp"]), ("sp_0", "sp_1", "sp_2", "tp"))
    placed = (P(SP, "tp"), P(SP, "tp"), P(SP, "tp"), P(), P(None, "tp"), P(SP, "tp"))
    return jax.shard_map(
        local,
        mesh=split,
        in_specs=placed,
        out_specs=(P(SP, "tp"), P(SP, "tp"), P(SP, "tp"), P(None, "tp"), P()),
        check_vma=False,
    )
```

profile of v0, /device:TPU:1, one launch (start us, length us, event | category | flops | bytes accessed | tf_op | source)
XLA Modules:
  0.0 112.4 jit_solution(12762319601571604397)
XLA Ops:
  0.7 4.1 %collective-permute-start.1 = (bf16[256,256]{1,0:T(8,128)(2,1)}, bf16[256,256]{1,0:T(8,128)(2,1)S(1)}, u32[]{:S(2)}, u32[]{:S(2)}) collective-permute-start(bf16[256,256]{1,0:T(8,128)(2,1)} %param.8), channel_id=1, source_target_pairs={{0,2},{2,4},{4,6},{6,8},{8,10},{10,12},{12,14},{14,16},{16,18},{18... | collective-permute-start | bytes 393224 | tf_op jit(solution)/shard_map/ppermute | solution.py:23
  4.8 0.8 slice_bitcast_fusion.10
  5.5 1.0 reshape.206
  6.6 0.3 multiply_reduce_fusion.4
  7.0 0.3 mul.199
  7.4 3.1 %collective-permute-start = (bf16[256,256]{1,0:T(8,128)(2,1)S(1)}, bf16[256,256]{1,0:T(8,128)(2,1)S(1)}, u32[]{:S(2)}, u32[]{:S(2)}) collective-permute-start(bf16[256,256]{1,0:T(8,128)(2,1)S(1)} %multiply_convert_fusion.1), channel_id=1, source_target_pairs={{0,2},{2,4},{4,6},{6,8},{8,10},{10,12},{12,14},{14,16},{16,18},{18... | collective-permute-start | bytes 393224 | tf_op jit(solution)/shard_map/ppermute | solution.py:23
  10.5 0.5 broadcast_multiply_fusion.1
  11.0 0.2 slice_reduce_fusion.2
  11.2 0.6 broadcast_bitcast_fusion
  11.8 0.1 mul.195
  11.9 0.3 reduce_sum.115
  12.4 0.1 add_compare_fusion
  12.5 0.1 pad_maximum_fusion.2
  12.6 0.1 reshape.207
  12.8 0.3 tile.10
  13.1 0.2 reverse
  13.3 0.1 slice.208
  13.4 0.1 copy.149
  13.6 0.1 copy-done.14
  13.9 0.2 reshape_reshape.7
  14.2 0.2 reshape_reshape.8
  14.4 0.5 fusion.28
  14.9 0.3 exponential_reduce_fusion
  15.2 0.4 multiply_reduce_fusion
  15.6 0.3 fusion.18
  15.9 0.6 slice_reduce_fusion
  16.5 0.7 slice.172
  17.2 0.6 convolution_bitcast_fusion
  17.8 0.5 fusion
  18.3 0.2 copy-done.23
  18.4 1.5 %multiply_reduce_fusion.2 = (f32[128]{0:T(128)}, f32[4,64,2]{1,2,0:T(2,128)S(1)}, f32[4,2,128,64]{2,3,1,0:T(8,128)}) fusion(f32[4,64,2,128]{3,2,1,0:T(2,128)S(1)} %copy-done.1, f32[4,64,2]{1,2,0:T(2,128)S(1)} %copy.149, f32[128]{0:T(128)S(1)} %copy-done.23, bf16[4,2,64,320]{3,2,1,0:T(8,128)(2,1)S(1)} %get-tuple-element.16, ...), kind=kOutput, calls=%fused_computation.53 | convolution fusion | flops 42401152 | bytes 1512448 | tf_op jit(solution)/shard_map/chij,cjhd->cihd/dot_general | solution.py:120
  19.9 1.0 reverse.1
  20.9 0.1 slice.209
  21.1 0.1 copy.192
  21.2 0.2 reshape.215
  21.4 0.8 slice_reduce_fusion.1
  22.2 0.1 copy.177
  22.4 0.9 copy.160
  23.3 2.1 %copy.171 = f32[4,320,2,128]{3,2,1,0:T(2,128)} copy(f32[4,320,2,128]{3,1,2,0:T(8,128)S(1)} %convolution_bitcast_fusion) | data formatting | bytes 2621440 | tf_op jit(solution)/shard_map/chij,cihd->cjhd/transpose | solution.py:115
  25.3 2.3 %reshape.213 = f32[4,5,64,256]{3,2,1,0:T(8,128)S(1)} reshape(f32[4,320,2,128]{3,2,1,0:T(2,128)} %copy.171) | data formatting | bytes 2621440 | tf_op jit(solution)/shard_map/reshape | solution.py:87
  27.7 0.1 slice_bitcast_fusion.4
  27.8 0.1 pad_add_fusion
  27.9 0.7 slice.210
  28.6 1.3 %collective-permute-start.3 = (bf16[256,256]{1,0:T(8,128)(2,1)}, bf16[256,256]{1,0:T(8,128)(2,1)}, u32[]{:S(2)}, u32[]{:S(2)}) collective-permute-start(bf16[256,256]{1,0:T(8,128)(2,1)} %bitcast.44), channel_id=1, source_target_pairs={{2,0},{4,2},{6,4},{8,6},{10,8},{12,10},{14,12},{16,14},{18,16},{20... | collective-permute-start | bytes 393224 | tf_op jit(solution)/shard_map/ppermute | solution.py:23
  29.9 1.0 copy.163
  30.9 1.0 reshape.211
  32.0 0.1 slice_bitcast_fusion.9
  32.1 0.1 pad_add_fusion.1
  32.3 1.4 %collective-permute-start.2 = (bf16[256,256]{1,0:T(8,128)(2,1)S(1)}, bf16[256,256]{1,0:T(8,128)(2,1)S(1)}, u32[]{:S(2)}, u32[]{:S(2)}) collective-permute-start(bf16[256,256]{1,0:T(8,128)(2,1)S(1)} %bitcast.195), channel_id=1, source_target_pairs={{2,0},{4,2},{6,4},{8,6},{10,8},{12,10},{14,12},{16,14},{18,16},{20... | collective-permute-start | bytes 393224 | tf_op jit(solution)/shard_map/ppermute | solution.py:23
  33.7 0.3 mul.196
  34.1 0.3 mul.233
  34.4 0.7 fusion.15
  35.2 0.1 copy.176
  35.3 0.1 maximum_bitcast_fusion
  35.4 3.4 %collective-permute-done.2 = bf16[256,256]{1,0:T(8,128)(2,1)S(1)} collective-permute-done((bf16[256,256]{1,0:T(8,128)(2,1)S(1)}, bf16[256,256]{1,0:T(8,128)(2,1)S(1)}, u32[]{:S(2)}, u32[]{:S(2)}) %collective-permute-start.2) | collective-permute-done | bytes 131104 | tf_op jit(solution)/shard_map/ppermute | solution.py:23
  38.9 32.4 %all-reduce.11 = (f32[192,2]{0,1:T(2,128)S(1)}, f32[2,128]{1,0:T(2,128)S(1)}) all-reduce(f32[192,2]{0,1:T(2,128)S(1)} %maximum_bitcast_fusion, f32[2,128]{1,0:T(2,128)S(1)} %pad_maximum_fusion.3), channel_id=1, replica_groups=mesh['sp_0'=12,'sp_1'=8,'sp_2'=4,'tp'=2] {'sp_0'}, use_global_device_ids=true, to_apply=%region_11.12 | all-reduce | flops 640 | bytes 5120 | tf_op jit(solution)/shard_map/psum | solution.py:27
  71.3 11.7 %all-reduce.12 = (f32[192,2]{0,1:T(2,128)S(1)}, f32[2,128]{1,0:T(2,128)S(1)}) all-reduce(f32[192,2]{0,1:T(2,128)S(1)} %get-tuple-element.7, f32[2,128]{1,0:T(2,128)S(1)} %get-tuple-element.8), channel_id=1, replica_groups=mesh['sp_0'=12,'sp_1'=8,'sp_2'=4,'tp'=2] {'sp_1'}, use_global_device_ids=true, to_apply=%region_12.13 | all-reduce | flops 640 | bytes 5120 | tf_op jit(solution)/shard_map/psum | solution.py:27
  83.0 9.6 %all-reduce.13 = (f32[192,2]{0,1:T(2,128)}, f32[2,128]{1,0:T(2,128)S(1)}) all-reduce(f32[192,2]{0,1:T(2,128)S(1)} %get-tuple-element.9, f32[2,128]{1,0:T(2,128)S(1)} %get-tuple-element.10), channel_id=1, replica_groups=mesh['sp_0'=12,'sp_1'=8,'sp_2'=4,'tp'=2] {'sp_2'}, use_global_device_ids=true, to_apply=%region_13.14 | all-reduce | flops 640 | bytes 5120 | tf_op jit(solution)/shard_map/psum | solution.py:27
  92.6 16.3 %psum.55 = f32[2,128]{1,0:T(2,128)} all-reduce(f32[2,128]{1,0:T(2,128)S(1)} %get-tuple-element.12), channel_id=1, replica_groups=mesh['sp_0'=12,'sp_1'=8,'sp_2'=4,'tp'=2] {'tp'}, use_global_device_ids=true, to_apply=%region_20.21 | all-reduce | flops 256 | bytes 2048 | tf_op jit(solution)/shard_map/psum | solution.py:27
  108.9 0.1 reshape.212
  109.1 0.6 multiply_reduce_fusion.3
  109.8 0.3 mul.245
  110.1 0.7 fusion.12
  110.8 1.6 %fusion.16 = bf16[256,256]{1,0:T(8,128)(2,1)} fusion(f32[4,64,256]{2,1,0:T(8,128)S(1)} %slice-done, bf16[256,256]{1,0:T(8,128)(2,1)} %collective-permute-done.3), kind=kLoop, calls=%fused_computation.47 | loop fusion | flops 196608 | bytes 524288 | tf_op jit(solution)/shard_map/convert_element_type | solution.py:168
  (91 shorter events, 0.9 us)
Async XLA Ops:
  0.6 9.9 %copy-start.19 = (f32[2,128]{1,0:T(2,128)S(1)}, f32[2,128]{1,0:T(2,128)}, u32[]{:S(2)}) copy-start(f32[2,128]{1,0:T(2,128)} %param.9) | copy-start | bytes 3076
  0.6 6.7 %copy-start.4 = (bf16[256,256]{1,0:T(8,128)(2,1)S(1)}, bf16[256,256]{1,0:T(8,128)(2,1)}, u32[]{:S(2)}) copy-start(bf16[256,256]{1,0:T(8,128)(2,1)} %param.7) | copy-start | bytes 393220
  0.7 10.4 %copy-start.17 = (f32[192,2]{0,1:T(2,128)S(1)}, f32[192,2]{0,1:T(2,128)}, u32[]{:S(2)}) copy-start(f32[192,2]{0,1:T(2,128)} %param.10) | copy-start | bytes 4612
  0.7 11.1 %copy-start.7 = (bf16[256,256]{1,0:T(8,128)(2,1)S(1)}, bf16[256,256]{1,0:T(8,128)(2,1)}, u32[]{:S(2)}) copy-start(bf16[256,256]{1,0:T(8,128)(2,1)} %param.6) | copy-start | bytes 393220
  0.7 12.9 %collective-permute-start.1 = (bf16[256,256]{1,0:T(8,128)(2,1)}, bf16[256,256]{1,0:T(8,128)(2,1)S(1)}, u32[]{:S(2)}, u32[]{:S(2)}) collective-permute-start(bf16[256,256]{1,0:T(8,128)(2,1)} %param.8), channel_id=1, source_target_pairs={{0,2},{2,4},{4,6},{6,8},{8,10},{10,12},{12,14},{14,16},{16,18},{18... | collective-permute-start | bytes 393224 | tf_op jit(solution)/shard_map/ppermute | solution.py:23
  6.6 5.7 %copy-start.2 = (f32[256,2,128]{2,1,0:T(2,128)}, f32[256,2,128]{2,1,0:T(2,128)S(1)}, u32[]{:S(2)}) copy-start(f32[256,2,128]{2,1,0:T(2,128)S(1)} %reshape.206) | copy-start | bytes 786436
  7.0 5.8 %copy-start.11 = (f32[256,2]{1,0:T(8,128)}, f32[256,2]{1,0:T(8,128)S(1)}, u32[]{:S(2)}) copy-start(f32[256,2]{1,0:T(8,128)S(1)} %add_rsqrt_fusion) | copy-start | bytes 6148
  7.3 5.4 %copy-start.16 = (bf16[256,256]{1,0:T(8,128)(2,1)S(1)}, bf16[256,256]{1,0:T(8,128)(2,1)}, u32[]{:S(2)}) copy-start(bf16[256,256]{1,0:T(8,128)(2,1)} %param.11) | copy-start | bytes 393220
  7.4 6.4 %collective-permute-start = (bf16[256,256]{1,0:T(8,128)(2,1)S(1)}, bf16[256,256]{1,0:T(8,128)(2,1)S(1)}, u32[]{:S(2)}, u32[]{:S(2)}) collective-permute-start(bf16[256,256]{1,0:T(8,128)(2,1)S(1)} %multiply_convert_fusion.1), channel_id=1, source_target_pairs={{0,2},{2,4},{4,6},{6,8},{8,10},{10,12},{12,14},{14,16},{16,18},{18... | collective-permute-start | bytes 393224 | tf_op jit(solution)/shard_map/ppermute | solution.py:23
  12.3 1.3 %copy-start.9 = (f32[256,2]{1,0:T(8,128)}, f32[256,2]{1,0:T(8,128)S(1)}, u32[]{:S(2)}) copy-start(f32[256,2]{1,0:T(8,128)S(1)} %add_rsqrt_fusion.1) | copy-start | bytes 6148
  12.7 1.6 %copy-start = (f32[4,64,2,128]{3,2,1,0:T(2,128)}, f32[4,64,2,128]{3,2,1,0:T(2,128)S(1)}, u32[]{:S(2)}) copy-start(f32[4,64,2,128]{3,2,1,0:T(2,128)S(1)} %reshape.207) | copy-start | bytes 786436
  12.7 1.0 copy-start.14
  15.9 1.9 %copy-start.1 = (f32[4,64,2,128]{3,2,1,0:T(2,128)S(1)}, f32[4,64,2,128]{3,2,1,0:T(2,128)}, u32[]{:S(2)}) copy-start(f32[4,64,2,128]{3,2,1,0:T(2,128)} %copy-done) | copy-start | bytes 786436
  17.7 0.7 copy-start.23
  19.9 2.4 %copy-start.15 = (f32[4,2,128,64]{2,3,1,0:T(8,128)S(1)}, f32[4,2,128,64]{2,3,1,0:T(8,128)}, u32[]{:S(2)}) copy-start(f32[4,2,128,64]{2,3,1,0:T(8,128)} %get-tuple-element.39) | copy-start | bytes 786436
  27.9 7.3 %copy-start.6 = (f32[8,64,256]{2,1,0:T(8,128)}, f32[8,64,256]{2,1,0:T(8,128)S(1)}, u32[]{:S(2)}) copy-start(f32[8,64,256]{2,1,0:T(8,128)S(1)} %pad_add_fusion) | copy-start | bytes 1572868
  28.6 82.2 %collective-permute-start.3 = (bf16[256,256]{1,0:T(8,128)(2,1)}, bf16[256,256]{1,0:T(8,128)(2,1)}, u32[]{:S(2)}, u32[]{:S(2)}) collective-permute-start(bf16[256,256]{1,0:T(8,128)(2,1)} %bitcast.44), channel_id=1, source_target_pairs={{2,0},{4,2},{6,4},{8,6},{10,8},{12,10},{14,12},{16,14},{18,16},{20... | collective-permute-start | bytes 393224 | tf_op jit(solution)/shard_map/ppermute | solution.py:23
  32.1 1.6 %copy-start.10 = (f32[256,2]{1,0:T(8,128)S(1)}, f32[256,2]{1,0:T(8,128)}, u32[]{:S(2)}) copy-start(f32[256,2]{1,0:T(8,128)} %copy-done.9) | copy-start | bytes 6148
  32.1 2.3 %copy-start.8 = (bf16[256,256]{1,0:T(8,128)(2,1)S(1)}, bf16[256,256]{1,0:T(8,128)(2,1)}, u32[]{:S(2)}) copy-start(bf16[256,256]{1,0:T(8,128)(2,1)} %param.6) | copy-start | bytes 393220
  32.1 2.3 %copy-start.13 = (f32[4,64,2,128]{3,2,1,0:T(2,128)S(1)}, f32[4,64,2,128]{3,2,1,0:T(2,128)}, u32[]{:S(2)}) copy-start(f32[4,64,2,128]{3,2,1,0:T(2,128)} %copy.160) | copy-start | bytes 786436
  32.1 2.3 %copy-start.18 = (f32[256]{0:T(256)S(1)}, f32[256]{0:T(256)}, u32[]{:S(2)}) copy-start(f32[256]{0:T(256)} %broadcast_bitcast_fusion) | copy-start | bytes 3076
  32.2 2.9 %copy-start.20 = (f32[2]{0:T(128)S(1)}, f32[2]{0:T(128)}, u32[]{:S(2)}) copy-start(f32[2]{0:T(128)} %slice_reduce_fusion) | copy-start | bytes 28
  32.2 2.9 %copy-start.22 = (f32[2]{0:T(128)S(1)}, f32[2]{0:T(128)}, u32[]{:S(2)}) copy-start(f32[2]{0:T(128)} %slice_reduce_fusion.1) | copy-start | bytes 28
  32.3 6.5 %collective-permute-start.2 = (bf16[256,256]{1,0:T(8,128)(2,1)S(1)}, bf16[256,256]{1,0:T(8,128)(2,1)S(1)}, u32[]{:S(2)}, u32[]{:S(2)}) collective-permute-start(bf16[256,256]{1,0:T(8,128)(2,1)S(1)} %bitcast.195), channel_id=1, source_target_pairs={{2,0},{4,2},{6,4},{8,6},{10,8},{12,10},{14,12},{16,14},{18,16},{20... | collective-permute-start | bytes 393224 | tf_op jit(solution)/shard_map/ppermute | solution.py:23
  34.0 4.7 %copy-start.5 = (bf16[256,256]{1,0:T(8,128)(2,1)S(1)}, bf16[256,256]{1,0:T(8,128)(2,1)}, u32[]{:S(2)}) copy-start(bf16[256,256]{1,0:T(8,128)(2,1)} %param.7) | copy-start | bytes 393220
  35.1 3.7 %copy-start.21 = (f32[128]{0:T(128)S(1)}, f32[128]{0:T(128)}, u32[]{:S(2)}) copy-start(f32[128]{0:T(128)} %get-tuple-element.5) | copy-start | bytes 1540
  35.2 73.9 %copy-start.3 = (f32[256,2,128]{2,1,0:T(2,128)S(1)}, f32[256,2,128]{2,1,0:T(2,128)}, u32[]{:S(2)}) copy-start(f32[256,2,128]{2,1,0:T(2,128)} %copy-done.2) | copy-start | bytes 786436
  35.2 73.9 %copy-start.12 = (f32[256,2]{1,0:T(8,128)S(1)}, f32[256,2]{1,0:T(8,128)}, u32[]{:S(2)}) copy-start(f32[256,2]{1,0:T(8,128)} %copy-done.11) | copy-start | bytes 6148
  109.1 1.7 %slice-start = ((f32[8,64,256]{2,1,0:T(8,128)}), f32[4,64,256]{2,1,0:T(8,128)S(1)}, s32[]{:S(2)}) async-start(f32[8,64,256]{2,1,0:T(8,128)} %copy-done.6), calls=%async_computation | async-start | bytes 524288 | tf_op jit(solution)/shard_map/slice | solution.py:157
where the time goes:
time: 113 us; the launch traced here: 112 us
  blocking collectives  70.1 us (62%)
  local copies, waits for them, and re-layouts  16.6 us (15%)
  starting transfers between devices  9.9 us (9%)
  other arithmetic  7.59 us (7%)
  matrix products  3.45 us (3%)
  waiting for transfers between devices  3.37 us (3%)
  between operations  1.41 us (1%)
    psum x4, blocking collectives, over_axes(): return functools.reduce(lax.psum, axes, value)  70.1 us
    ppermute x4, starting transfers between devices, shifted(): return lax.ppermute(block, axis, route)  9.9 us
    reshape x2, local copies, waits for them, and re-layouts, unband(): pieces = grad_band.reshape(seg_count, LEFT + 1, SEG, -1)  3.38 us
    ppermute x4, waiting for transfers between devices, shifted(): return lax.ppermute(block, axis, route)  3.37 us
  transfers between devices with their start and end apart: 4, of which 1 were waited for; matrix products, arithmetic and copies ran while one was open for 10% of the time, Pallas kernels for 0%

commit v1 on v0

v1 whole, which is shorter than its diff:
```python
import functools

import jax
import jax.numpy as jnp
import numpy as np
from jax import lax
from jax.experimental import pallas as pl
from jax.experimental.pallas import tpu as pltpu
from jax.sharding import Mesh
from jax.sharding import PartitionSpec as P

HEAD_DIM = 128
SEG = 64
LEFT = 4
MAX_REL = 128
ENTRIES = MAX_REL + SEG
ROWS = LEFT * SEG
HEADS = 2
PAIR = 2 * SEG
AXES = ("sp_0", "sp_1", "sp_2", "tp")
SP = AXES[:3]

EPSILON = 1e-06
FACTOR = HEAD_DIM ** (-0.5)
LOG2E = 1.4426950408889634
MASKED = -1e30
F32, BF16 = jnp.float32, jnp.bfloat16


def dot(a, b, a_dim, b_dim):
    return lax.dot_general(a, b, (((a_dim,), (b_dim,)), ((), ())), preferred_element_type=F32)


def near(size, step=1):
    return sorted({step % size, -step % size} - {0})


def far_first(size):
    return sorted(range(1, size), key=lambda d: -min(d, size - d))


def unit(raw):
    wide = raw.astype(F32)
    inv_rms = lax.rsqrt(jnp.mean(wide * wide, axis=-1, keepdims=True) + EPSILON)
    return wide * inv_rms, inv_rms


def kernel(sizes, q_hbm, k_hbm, v_hbm, do_hbm, gains_hbm, table_hbm,
           dq_hbm, dk_hbm, dv_hbm, dtab_hbm, dgain_hbm,
           qx, kx, vx, dox, gains_v, table_v,
           qn, qu, qr, kn, ku, kr, bias_v, e_v, dp_v,
           dkx, dvx, dqx, d_v, back_out, back_in,
           dq_v, dk_v, dv_v, dtab_v, dgain_v, xbuf, ybuf, zbuf, fin,
           in_sem, halo_send, halo_recv, back_send, back_recv,
           x_send, x_recv, y_send, y_recv, z_send, z_recv, fin_send, fin_recv, out_sem,
           round1, round2, round3, row_sem):
    nz, ny, nx = sizes
    z, y, x, tp = (lax.axis_index(a) for a in AXES)
    place = (z * ny + y) * nx + x
    total = nz * ny * nx

    def at(number, core):
        return (number // (ny * nx), (number // nx) % ny, number % nx, core)

    after = at(lax.rem(place + 1, total), tp)
    before = at(lax.rem(place + total - 1, total), tp)

    def along(axis, offset, core=1):
        if axis == 0:
            return (lax.rem(z + offset, nz), y, x, core)
        if axis == 1:
            return (z, lax.rem(y + offset, ny), x, core)
        return (z, y, lax.rem(x + offset, nx), core)

    def signal(sem, target):
        pl.semaphore_signal(sem, inc=1, device_id=target, device_id_type=pl.DeviceIdType.MESH)

    def remote(src, dst, send, recv, target):
        return pltpu.make_async_remote_copy(
            src_ref=src, dst_ref=dst, send_sem=send, recv_sem=recv,
            device_id=target, device_id_type=pl.DeviceIdType.MESH)

    barrier = pltpu.get_barrier_semaphore()
    signal(barrier, before)
    signal(barrier, after)
    loads = []
    for n, (src, dst, first) in enumerate(((k_hbm, kx, ROWS), (v_hbm, vx, ROWS), (q_hbm, qx, 0), (do_hbm, dox, 0))):
        for h in range(HEADS):
            loads.append(pltpu.make_async_copy(
                src.at[:, h * HEAD_DIM:(h + 1) * HEAD_DIM], dst.at[h, first:first + ROWS], in_sem.at[2 * n + h]))
    loads.append(pltpu.make_async_copy(gains_hbm, gains_v, in_sem.at[8]))
    loads.append(pltpu.make_async_copy(table_hbm, table_v, in_sem.at[9]))
    for load in loads:
        load.start()

    close = [(a, o) for a, n in enumerate(sizes) for o in near(n)]

    @pl.when(tp == 1)
    def _():
        for a, o in close:
            signal(barrier, along(a, o))
        signal(barrier, (z, y, x, 0))
        pl.semaphore_wait(barrier, 3 + len(close))

    @pl.when(tp == 0)
    def _():
        signal(barrier, (z, y, x, 1))
        pl.semaphore_wait(barrier, 3)

    halo = {}
    for load in loads[:4]:
        load.wait()
    for h in range(HEADS):
        for half in (1, 0):
            for n, buf in enumerate((kx, vx)):
                slot = (h * 2 + half) * 2 + n
                copy = remote(
                    buf.at[h, ROWS + half * PAIR:ROWS + (half + 1) * PAIR],
                    buf.at[h, half * PAIR:(half + 1) * PAIR],
                    halo_send.at[slot], halo_recv.at[slot], after)
                copy.start()
                halo[h, half, n] = copy

    @pl.when(tp == 1)
    def _():
        for a, o in close:
            signal(round1, along(a, o))

    for load in loads[4:]:
        load.wait()

    gains = gains_v[...]
    gain_q, gain_k = gains[0:1, :], gains[1:2, :]

    def norm_keys(h, first, size):
        u, r = unit(kx[h, first:first + size])
        ku[h, first:first + size] = u
        kn[h, first:first + size] = (u * gain_k).astype(BF16)
        if first >= ROWS:
            kr[h, first - ROWS:first - ROWS + size] = jnp.broadcast_to(r, u.shape)

    for h in range(HEADS):
        u, r = unit(qx[h])
        qu[h] = u
        qr[h] = jnp.broadcast_to(r, u.shape)
        qn[h] = (u * gain_q).astype(BF16)
        norm_keys(h, ROWS, ROWS)

    key_at = lax.broadcasted_iota(jnp.int32, (PAIR, PAIR), 0)
    query_at = lax.broadcasted_iota(jnp.int32, (PAIR, PAIR), 1)
    past = query_at >= key_at
    early = query_at < SEG
    high = key_at >= SEG
    lane = lax.broadcasted_iota(jnp.int32, (1, PAIR), 1)
    table = table_v[...]
    low_part = table[:, :PAIR]
    high_part = jnp.concatenate([table[:, PAIR:], jnp.zeros((HEADS, 2 * PAIR - ENTRIES), F32)], axis=1)
    low_rolled = pltpu.roll(low_part, PAIR - SEG + 1, 1)
    high_rolled = pltpu.roll(high_part, PAIR - SEG + 1, 1)
    is_first = place == 0
    for h in range(HEADS):
        last = table[h:h + 1, ENTRIES - 1:ENTRIES]
        dist_low = low_rolled[h:h + 1]
        dist_row = jnp.where(lane <= SEG, dist_low, high_rolled[h:h + 1])
        ahead = pltpu.roll(jnp.broadcast_to(dist_low, (PAIR, PAIR)), 0, 1, stride=1, stride_axis=0)
        behind = pltpu.roll(jnp.broadcast_to(dist_row, (PAIR, PAIR)), 0, 1, stride=1, stride_axis=0)
        tile0 = jnp.where(jnp.logical_or(early, high), last, MASKED)
        tile1 = jnp.where(past, last, behind)
        tile2 = jnp.where(jnp.logical_and(early, high), MASKED, jnp.where(past, behind, ahead))
        tile0 = jnp.where(is_first, MASKED, tile0)
        for p in range(2):
            mid = jnp.where(is_first, MASKED, tile1) if p == 0 else tile1
            top = jnp.max(jnp.maximum(jnp.maximum(tile0, mid), tile2), axis=0, keepdims=True)
            for b, tile in enumerate((tile0, mid, tile2)):
                bias_v[h, p, b * PAIR:(b + 1) * PAIR] = (tile - top) * LOG2E

    sums = {(h, p): (jnp.zeros((1, PAIR), F32), jnp.zeros((1, PAIR), F32)) for h in range(HEADS) for p in range(2)}

    def block(h, p, b):
        first = (p + b) * PAIR
        own = slice(p * PAIR, (p + 1) * PAIR)
        s = dot(kn[h, first:first + PAIR], qn[h, own], 1, 1)
        e = jnp.exp2(s * (FACTOR * LOG2E) + bias_v[h, p, b * PAIR:(b + 1) * PAIR])
        dp = dot(vx[h, first:first + PAIR], dox[h, own], 1, 1)
        e_v[h, p, b * PAIR:(b + 1) * PAIR] = e
        dp_v[h, p, b * PAIR:(b + 1) * PAIR] = dp
        norm, weighted = sums[h, p]
        sums[h, p] = (norm + jnp.sum(e, axis=0, keepdims=True), weighted + jnp.sum(e * dp, axis=0, keepdims=True))

    gain_sums = [jnp.zeros((1, HEAD_DIM), F32), jnp.zeros((1, HEAD_DIM), F32)]

    def finish(h, p):
        norm, weighted = sums[h, p]
        inv = 1.0 / norm
        delta = weighted * inv
        own = slice(p * PAIR, (p + 1) * PAIR)
        keys = slice(p * PAIR, (p + 3) * PAIR)
        prob = e_v[h, p] * inv
        d_score = prob * (dp_v[h, p] - delta)
        prob_low = prob.astype(BF16)
        d_low = d_score.astype(BF16)
        dv = dot(prob_low, dox[h, own], 1, 0)
        dk = dot(d_low, qn[h, own], 1, 0)
        dq = dot(d_low, kn[h, keys], 0, 0)
        dqx[h, own] = dq
        gain_sums[0] = gain_sums[0] + jnp.sum(dq * qu[h, own], axis=0, keepdims=True)
        gain_sums[1] = gain_sums[1] + jnp.sum(dk * ku[h, keys], axis=0, keepdims=True)
        if p == 1:
            dkx[h, keys] = dk
            dvx[h, keys] = dv
            d_v[h] = d_score
        else:
            dkx[h, 0:PAIR] = dk[:PAIR]
            dvx[h, 0:PAIR] = dv[:PAIR]
            dkx[h, PAIR:3 * PAIR] = dkx[h, PAIR:3 * PAIR] + dk[PAIR:]
            dvx[h, PAIR:3 * PAIR] = dvx[h, PAIR:3 * PAIR] + dv[PAIR:]
            d_v[h] = d_v[h] + d_score

    table_rows = []
    sublane = lax.broadcasted_iota(jnp.int32, (8, PAIR), 0)

    def skewed_sum(tile):
        total = tile[:8]
        for first in range(8, PAIR, 8):
            total = total + pltpu.roll(tile[first:first + 8], PAIR - first, 1)
        for bit in (1, 2, 4):
            total = jnp.where((sublane & bit) == 0, total, pltpu.roll(total, PAIR - bit, 1))
        return jnp.sum(total, axis=0, keepdims=True)

    def fold_table(h):
        d0, d1, d2 = (d_v[h, b * PAIR:(b + 1) * PAIR] for b in range(3))
        mixed = jnp.where(past, d2, d1)
        ahead = jnp.where(past, 0.0, d2)
        rest = d0 + jnp.where(past, d1, 0.0)
        behind_row, ahead_row = skewed_sum(mixed), skewed_sum(ahead)
        rest_sum = jnp.sum(jnp.sum(rest, axis=0, keepdims=True), axis=1, keepdims=True)
        behind_row = pltpu.roll(behind_row, SEG - 1, 1)
        ahead_row = pltpu.roll(ahead_row, SEG - 1, 1)
        table_rows.append((
            jnp.where(lane < SEG - 1, ahead_row, behind_row),
            jnp.where(lane == SEG - 1, rest_sum, behind_row),
        ))

    for h in range(HEADS):
        block(h, 1, 1)
        block(h, 1, 2)
        block(h, 0, 2)

    @pl.when(tp == 1)
    def _():
        pl.semaphore_wait(round1, len(close))
        signal(row_sem, (z, y, x, 0))
        for a, n in enumerate(sizes[:2]):
            if n > 5:
                for o in near(n, 2):
                    signal(round2, along(a, o))

    for h in range(HEADS):
        for half in (1, 0):
            halo[h, half, 0].wait_recv()
            norm_keys(h, half * PAIR, PAIR)
            halo[h, half, 1].wait_recv()
            if half:
                block(h, 1, 0)
                block(h, 0, 1)
                finish(h, 1)
            else:
                block(h, 0, 0)
                finish(h, 0)
        fold_table(h)
        if h == 0:
            @pl.when(tp == 1)
            def _():
                count = sum(len(near(n, 2)) for n in sizes[:2] if n > 5)
                if count:
                    pl.semaphore_wait(round2, count)
                if nz > 9:
                    for o in near(nz, 2):
                        signal(round3, along(0, o))

    row = lax.broadcasted_iota(jnp.int32, (8, HEAD_DIM), 0)
    vec = jnp.zeros((8, HEAD_DIM), F32)
    second = jnp.where(lane < SEG, table_rows[0][1], pltpu.roll(table_rows[1][1], SEG, 1))
    for j, part in enumerate((table_rows[0][0], table_rows[1][0], second)):
        vec = jnp.where(row == 3 * tp + j, part, vec)
    for j in range(2):
        vec = jnp.where(row == 6 + j, gain_sums[j] * FACTOR, vec)
    mine = 2 * x + tp
    xbuf[mine] = vec

    def back_copies(h):
        return [
            remote(back_out.at[n, h], back_in.at[n, h], back_send.at[2 * n + h], back_recv.at[2 * n + h], before)
            for n in range(2)]

    def stage_back():
        for h in range(HEADS):
            back_out[0, h] = (dkx[h, :ROWS] * FACTOR).astype(BF16)
            back_out[1, h] = dvx[h, :ROWS].astype(BF16)

    def finish_queries():
        for h in range(HEADS):
            g = dqx[h] * FACTOR * gain_q
            u = qu[h]
            dq_v[:, h * HEAD_DIM:(h + 1) * HEAD_DIM] = (
                qr[h] * (g - u * jnp.mean(g * u, axis=-1, keepdims=True))).astype(BF16)

    dq_copy = pltpu.make_async_copy(dq_v, dq_hbm, out_sem.at[0])

    @pl.when(tp == 1)
    def _():
        if nz > 9:
            pl.semaphore_wait(round3, len(near(nz, 2)))
        sends = [
            remote(xbuf.at[mine], xbuf.at[mine], x_send.at[o], x_recv.at[mine], along(2, o)) for o in far_first(nx)]
        for copy in sends:
            copy.start()
        stage_back()
        for o in range(nx):
            for core in range(2):
                if o or not core:
                    slot = 2 * lax.rem(x + o, nx) + core
                    pltpu.make_async_copy(xbuf.at[slot], xbuf.at[slot], x_recv.at[slot]).wait()
        part = xbuf[0]
        for n in range(1, 2 * nx):
            part = part + xbuf[n]
        ybuf[y] = part
        moves = [remote(ybuf.at[y], ybuf.at[y], y_send.at[o], y_recv.at[y], along(1, o)) for o in far_first(ny)]
        for copy in moves:
            copy.start()
        sends += moves
        finish_queries()
        for o in range(1, ny):
            slot = lax.rem(y + o, ny)
            pltpu.make_async_copy(ybuf.at[slot], ybuf.at[slot], y_recv.at[slot]).wait()
        part = ybuf[0]
        for n in range(1, ny):
            part = part + ybuf[n]
        zbuf[z] = part
        moves = [remote(zbuf.at[z], zbuf.at[z], z_send.at[o], z_recv.at[z], along(0, o)) for o in far_first(nz)]
        for copy in moves:
            copy.start()
        sends += moves
        for h in range(HEADS):
            for copy in back_copies(h):
                copy.start()
        dq_copy.start()
        for copy in sends:
            copy.wait_send()

    @pl.when(tp == 0)
    def _():
        pl.semaphore_wait(row_sem, 1)
        sends = [
            remote(xbuf.at[mine], xbuf.at[mine], x_send.at[o], x_recv.at[mine], along(2, o))
            for o in [*far_first(nx), 0]]
        for copy in sends:
            copy.start()
        stage_back()
        finish_queries()
        for h in range(HEADS):
            for copy in back_copies(h):
                copy.start()
        dq_copy.start()
        for copy in sends:
            copy.wait_send()

    for copy in halo.values():
        copy.wait_send()
    out_copies = [dq_copy]
    for h in range(HEADS):
        back_k, back_v = back_copies(h)
        back_k.wait()
        back_v.wait()
        lanes = slice(h * HEAD_DIM, (h + 1) * HEAD_DIM)
        keep = jnp.where(place == total - 1, 0.0, 1.0)
        g = (dkx[h, ROWS:] * FACTOR + back_in[0, h].astype(F32) * keep) * gain_k
        u = ku[h, ROWS:]
        dk_v[:, lanes] = (kr[h] * (g - u * jnp.mean(g * u, axis=-1, keepdims=True))).astype(BF16)
        dv_v[:, lanes] = (dvx[h, ROWS:] + back_in[1, h].astype(F32) * keep).astype(BF16)
    for n, (src, dst) in enumerate(((dk_v, dk_hbm), (dv_v, dv_hbm))):
        copy = pltpu.make_async_copy(src, dst, out_sem.at[1 + n])
        copy.start()
        out_copies.append(copy)

    pass_on = remote(fin, fin, fin_send, fin_recv, (z, y, x, 0))

    @pl.when(tp == 1)
    def _():
        for o in range(1, nz):
            slot = lax.rem(z + o, nz)
            pltpu.make_async_copy(zbuf.at[slot], zbuf.at[slot], z_recv.at[slot]).wait()
        part = zbuf[0]
        for n in range(1, nz):
            part = part + zbuf[n]
        fin[...] = part
        pass_on.start()

    @pl.when(tp == 0)
    def _():
        pltpu.make_async_copy(fin, fin, fin_recv).wait()

    tail = fin[pl.ds(3 * tp + 2, 1), :]
    for j in range(HEADS):
        dtab_v[j:j + 1, :PAIR] = fin[pl.ds(3 * tp + j, 1), :]
        dtab_v[j:j + 1, PAIR:] = tail[:, j * SEG:(j + 1) * SEG]
    dgain_v[...] = fin[6:8, :]
    for n, (src, dst) in enumerate(((dtab_v, dtab_hbm), (dgain_v, dgain_hbm))):
        copy = pltpu.make_async_copy(src, dst, out_sem.at[3 + n])
        copy.start()
        out_copies.append(copy)

    @pl.when(tp == 1)
    def _():
        pass_on.wait_send()

    for copy in out_copies:
        copy.wait()


def local(sizes, queries, keys, values, gains, bias_table, d_out):
    nz, ny, nx = sizes
    width = HEADS * HEAD_DIM
    any_spec = pl.BlockSpec(memory_space=pl.ANY)
    tile = (HEADS, ROWS, HEAD_DIM)
    wide = (HEADS, 2 * ROWS, HEAD_DIM)
    pairs = (HEADS, 2, 3 * PAIR, PAIR)
    dma, regular = pltpu.SemaphoreType.DMA, pltpu.SemaphoreType.REGULAR
    vmem = pltpu.VMEM
    out = pl.pallas_call(
        functools.partial(kernel, sizes),
        out_shape=(
            jax.ShapeDtypeStruct((ROWS, width), BF16),
            jax.ShapeDtypeStruct((ROWS, width), BF16),
            jax.ShapeDtypeStruct((ROWS, width), BF16),
            jax.ShapeDtypeStruct((HEADS, ENTRIES), F32),
            jax.ShapeDtypeStruct((2, HEAD_DIM), F32),
        ),
        in_specs=[any_spec] * 6,
        out_specs=(any_spec,) * 5,
        scratch_shapes=[
            vmem(tile, BF16), vmem(wide, BF16), vmem(wide, BF16), vmem(tile, BF16),
            vmem((2, HEAD_DIM), F32), vmem((HEADS, ENTRIES), F32),
            vmem(tile, BF16), vmem(tile, F32), vmem(tile, F32),
            vmem(wide, BF16), vmem(wide, F32), vmem(tile, F32),
            vmem(pairs, F32), vmem(pairs, F32), vmem(pairs, F32),
            vmem(wide, F32), vmem(wide, F32), vmem(tile, F32), vmem((HEADS, 3 * PAIR, PAIR), F32),
            vmem((2, *tile), BF16), vmem((2, *tile), BF16),
            vmem((ROWS, width), BF16), vmem((ROWS, width), BF16), vmem((ROWS, width), BF16),
            vmem((HEADS, ENTRIES), F32), vmem((2, HEAD_DIM), F32),
            vmem((2 * nx, 8, HEAD_DIM), F32), vmem((ny, 8, HEAD_DIM), F32), vmem((nz, 8, HEAD_DIM), F32),
            vmem((8, HEAD_DIM), F32),
            dma((10,)), dma((8,)), dma((8,)), dma((4,)), dma((4,)),
            dma((nx,)), dma((2 * nx,)), dma((ny,)), dma((ny,)), dma((nz,)), dma((nz,)), dma, dma, dma((5,)),
            regular, regular, regular, regular,
        ],
        compiler_params=pltpu.CompilerParams(
            collective_id=0, has_side_effects=True, vmem_limit_bytes=56 * 1024 * 1024),
        name="segment_attention_grad",
    )(queries, keys, values, d_out, gains, bias_table.T)
    d_queries, d_keys, d_values, d_table, d_gains = out
    return d_queries, d_keys, d_values, d_table.T, d_gains


def solution(mesh):
    shape = (12, 8, 4)
    if mesh.shape["sp"] != int(np.prod(shape)):
        shape = mesh.small_shape
    split = Mesh(mesh.devices.reshape(*shape, mesh.shape["tp"]), AXES)
    placed = (P(SP, "tp"), P(SP, "tp"), P(SP, "tp"), P(), P(None, "tp"), P(SP, "tp"))
    return jax.shard_map(
        functools.partial(local, shape),
        mesh=split,
        in_specs=placed,
        out_specs=(P(SP, "tp"), P(SP, "tp"), P(SP, "tp"), P(None, "tp"), P()),
        check_vma=False,
    )
```

time: 113 us -> 44.2 us (0.39)
  the two profiles are of different devices: /device:TPU:1 before, /device:TPU:6 now
where the time goes in v1:
time: 44.2 us; the launch traced here: 44 us
  Pallas kernels  38.9 us (88%)
  local copies, waits for them, and re-layouts  4.45 us (10%)
  between operations  0.65 us (1%)
    pallas_call x1, Pallas kernels, local(): pl.pallas_call(functools.partial(kernel, sizes), out_shape=(jax.ShapeDtyp...  38.9 us
    unnamed x13, local copies, waits for them, and re-layouts  4.45 us

profile of v1, /device:TPU:6, one launch (start us, length us, event | category | flops | bytes accessed | tf_op | source)
XLA Modules:
  0.0 44.0 jit_solution(11930394961565975321)
XLA Ops:
  0.6 38.9 %segment_attention_grad.1 = (bf16[256,256]{1,0:T(8,128)(2,1)}, bf16[256,256]{1,0:T(8,128)(2,1)}, bf16[256,256]{1,0:T(8,128)(2,1)}, f32[2,192]{1,0:T(2,128)}, f32[2,128]{1,0:T(2,128)}) custom-call(bf16[256,256]{1,0:T(8,128)(2,1)} %q_hbm.1, bf16[256,256]{1,0:T(8,128)(2,1)} %k_hbm.1, bf16[256,256]{1,0:T(8,128)(2,1)} %v_hbm.1, bf16[256,256]{1,0:T(8,128)(2,1)} %do_hbm.1, ...), custom_call_target="tpu_custom_call" | custom-call | tf_op jit(solution)/shard_map/segment_attention_grad/pallas_call | solution.py:430
  39.5 0.0 copy-start.1
  39.5 1.6 %copy.16 = bf16[256,256]{1,0:T(8,128)(2,1)} copy(bf16[256,256]{1,0:T(8,128)(2,1)} %get-tuple-element.20) | data formatting | bytes 262144
  41.1 0.0 copy-done.1
  41.1 0.0 copy-start
  41.1 0.7 %copy.17 = bf16[256,256]{1,0:T(8,128)(2,1)} copy(bf16[256,256]{1,0:T(8,128)(2,1)S(1)} %copy-done.1) | data formatting | bytes 262144
  41.8 0.3 copy-done
  42.1 0.0 copy-start.2
  42.1 0.7 %copy.18 = bf16[256,256]{1,0:T(8,128)(2,1)} copy(bf16[256,256]{1,0:T(8,128)(2,1)S(1)} %copy-done) | data formatting | bytes 262144
  42.7 0.0 copy-done.2
  42.8 0.0 copy-start.3
  42.8 0.6 %copy.19 = f32[192,2]{0,1:T(2,128)} copy(f32[192,2]{0,1:T(2,128)S(1)} %bitcast.3) | data formatting | bytes 3072
  43.3 0.1 copy-done.3
  43.4 0.6 %copy.20 = f32[2,128]{1,0:T(2,128)} copy(f32[2,128]{1,0:T(2,128)S(1)} %copy-done.3) | data formatting | bytes 2048
Async XLA Ops:
  39.5 1.6 %copy-start.1 = (bf16[256,256]{1,0:T(8,128)(2,1)S(1)}, bf16[256,256]{1,0:T(8,128)(2,1)}, u32[]{:S(2)}) copy-start(bf16[256,256]{1,0:T(8,128)(2,1)} %get-tuple-element.21) | copy-start | bytes 393220
  41.1 1.0 %copy-start = (bf16[256,256]{1,0:T(8,128)(2,1)S(1)}, bf16[256,256]{1,0:T(8,128)(2,1)}, u32[]{:S(2)}) copy-start(bf16[256,256]{1,0:T(8,128)(2,1)} %get-tuple-element.22) | copy-start | bytes 393220
  42.1 0.7 %copy-start.2 = (f32[2,192]{1,0:T(2,128)S(1)}, f32[2,192]{1,0:T(2,128)}, u32[]{:S(2)}) copy-start(f32[2,192]{1,0:T(2,128)} %get-tuple-element.13) | copy-start | bytes 4612
  42.8 0.7 %copy-start.3 = (f32[2,128]{1,0:T(2,128)S(1)}, f32[2,128]{1,0:T(2,128)}, u32[]{:S(2)}) copy-start(f32[2,128]{1,0:T(2,128)} %get-tuple-element.24) | copy-start | bytes 3076

commit v2 on v1

--- a/solution.py
+++ b/solution.py
@@ -46,13 +46,13 @@
 
 
 def kernel(sizes, q_hbm, k_hbm, v_hbm, do_hbm, gains_hbm, table_hbm,
-           dq_hbm, dk_hbm, dv_hbm, dtab_hbm, dgain_hbm,
+           dq_v, dk_v, dv_v, dtab_v, dgain_v,
            qx, kx, vx, dox, gains_v, table_v,
            qn, qu, qr, kn, ku, kr, bias_v, e_v, dp_v,
            dkx, dvx, dqx, d_v, back_out, back_in,
-           dq_v, dk_v, dv_v, dtab_v, dgain_v, xbuf, ybuf, zbuf, fin,
+           xbuf, ybuf, zbuf, fin,
            in_sem, halo_send, halo_recv, back_send, back_recv,
-           x_send, x_recv, y_send, y_recv, z_send, z_recv, fin_send, fin_recv, out_sem,
+           x_send, x_recv, y_send, y_recv, z_send, z_recv, fin_send, fin_recv,
            round1, round2, round3, row_sem):
     nz, ny, nx = sizes
     z, y, x, tp = (lax.axis_index(a) for a in AXES)
@@ -304,8 +304,6 @@
             u = qu[h]
             dq_v[:, h * HEAD_DIM:(h + 1) * HEAD_DIM] = (
                 qr[h] * (g - u * jnp.mean(g * u, axis=-1, keepdims=True))).astype(BF16)
-
-    dq_copy = pltpu.make_async_copy(dq_v, dq_hbm, out_sem.at[0])
 
     @pl.when(tp == 1)
     def _():
@@ -344,7 +342,6 @@
         for h in range(HEADS):
             for copy in back_copies(h):
                 copy.start()
-        dq_copy.start()
         for copy in sends:
             copy.wait_send()
 
@@ -361,13 +358,11 @@
         for h in range(HEADS):
             for copy in back_copies(h):
                 copy.start()
-        dq_copy.start()
         for copy in sends:
             copy.wait_send()
 
     for copy in halo.values():
         copy.wait_send()
-    out_copies = [dq_copy]
     for h in range(HEADS):
         back_k, back_v = back_copies(h)
         back_k.wait()
@@ -378,11 +373,6 @@
         u = ku[h, ROWS:]
         dk_v[:, lanes] = (kr[h] * (g - u * jnp.mean(g * u, axis=-1, keepdims=True))).astype(BF16)
         dv_v[:, lanes] = (dvx[h, ROWS:] + back_in[1, h].astype(F32) * keep).astype(BF16)
-    for n, (src, dst) in enumerate(((dk_v, dk_hbm), (dv_v, dv_hbm))):
-        copy = pltpu.make_async_copy(src, dst, out_sem.at[1 + n])
-        copy.start()
-        out_copies.append(copy)
-
     pass_on = remote(fin, fin, fin_send, fin_recv, (z, y, x, 0))
 
     @pl.when(tp == 1)
@@ -405,39 +395,36 @@
         dtab_v[j:j + 1, :PAIR] = fin[pl.ds(3 * tp + j, 1), :]
         dtab_v[j:j + 1, PAIR:] = tail[:, j * SEG:(j + 1) * SEG]
     dgain_v[...] = fin[6:8, :]
-    for n, (src, dst) in enumerate(((dtab_v, dtab_hbm), (dgain_v, dgain_hbm))):
-        copy = pltpu.make_async_copy(src, dst, out_sem.at[3 + n])
+    @pl.when(tp == 1)
+    def _():
+        pass_on.wait_send()
+
+
+def write_out(*refs):
+    count = len(refs) // 2
+    copies = [pltpu.make_async_copy(refs[n], refs[count + n], refs[-1].at[n]) for n in range(count)]
+    for copy in copies:
         copy.start()
-        out_copies.append(copy)
-
-    @pl.when(tp == 1)
-    def _():
-        pass_on.wait_send()
-
-    for copy in out_copies:
+    for copy in copies:
         copy.wait()
 
 
 def local(sizes, queries, keys, values, gains, bias_table, d_out):
     nz, ny, nx = sizes
     width = HEADS * HEAD_DIM
-    any_spec = pl.BlockSpec(memory_space=pl.ANY)
+    hbm_spec = pl.BlockSpec(memory_space=pltpu.HBM)
+    vmem_spec = pl.BlockSpec(memory_space=pltpu.VMEM)
     tile = (HEADS, ROWS, HEAD_DIM)
     wide = (HEADS, 2 * ROWS, HEAD_DIM)
     pairs = (HEADS, 2, 3 * PAIR, PAIR)
     dma, regular = pltpu.SemaphoreType.DMA, pltpu.SemaphoreType.REGULAR
     vmem = pltpu.VMEM
+    outs = [((ROWS, width), BF16)] * 3 + [((HEADS, ENTRIES), F32), ((2, HEAD_DIM), F32)]
     out = pl.pallas_call(
         functools.partial(kernel, sizes),
-        out_shape=(
-            jax.ShapeDtypeStruct((ROWS, width), BF16),
-            jax.ShapeDtypeStruct((ROWS, width), BF16),
-            jax.ShapeDtypeStruct((ROWS, width), BF16),
-            jax.ShapeDtypeStruct((HEADS, ENTRIES), F32),
-            jax.ShapeDtypeStruct((2, HEAD_DIM), F32),
-        ),
-        in_specs=[any_spec] * 6,
-        out_specs=(any_spec,) * 5,
+        out_shape=tuple(vmem(*o) for o in outs),
+        in_specs=[hbm_spec] * 6,
+        out_specs=(vmem_spec,) * 5,
         scratch_shapes=[
             vmem(tile, BF16), vmem(wide, BF16), vmem(wide, BF16), vmem(tile, BF16),
             vmem((2, HEAD_DIM), F32), vmem((HEADS, ENTRIES), F32),
@@ -446,19 +433,24 @@
             vmem(pairs, F32), vmem(pairs, F32), vmem(pairs, F32),
             vmem(wide, F32), vmem(wide, F32), vmem(tile, F32), vmem((HEADS, 3 * PAIR, PAIR), F32),
             vmem((2, *tile), BF16), vmem((2, *tile), BF16),
-            vmem((ROWS, width), BF16), vmem((ROWS, width), BF16), vmem((ROWS, width), BF16),
-            vmem((HEADS, ENTRIES), F32), vmem((2, HEAD_DIM), F32),
             vmem((2 * nx, 8, HEAD_DIM), F32), vmem((ny, 8, HEAD_DIM), F32), vmem((nz, 8, HEAD_DIM), F32),
             vmem((8, HEAD_DIM), F32),
             dma((10,)), dma((8,)), dma((8,)), dma((4,)), dma((4,)),
-            dma((nx,)), dma((2 * nx,)), dma((ny,)), dma((ny,)), dma((nz,)), dma((nz,)), dma, dma, dma((5,)),
+            dma((nx,)), dma((2 * nx,)), dma((ny,)), dma((ny,)), dma((nz,)), dma((nz,)), dma, dma,
             regular, regular, regular, regular,
         ],
         compiler_params=pltpu.CompilerParams(
-            collective_id=0, has_side_effects=True, vmem_limit_bytes=56 * 1024 * 1024),
+            collective_id=0, has_side_effects=True, vmem_limit_bytes=32 * 1024 * 1024),
         name="segment_attention_grad",
-    )(queries, keys, values, d_out, gains, bias_table.T)
-    d_queries, d_keys, d_values, d_table, d_gains = out
+    )(*(pltpu.with_memory_space_constraint(a, pltpu.HBM) for a in (queries, keys, values, d_out, gains, bias_table.T)))
+    d_queries, d_keys, d_values, d_table, d_gains = pl.pallas_call(
+        write_out,
+        out_shape=tuple(jax.ShapeDtypeStruct(*o) for o in outs),
+        in_specs=[vmem_spec] * 5,
+        out_specs=(hbm_spec,) * 5,
+        scratch_shapes=[dma((5,))],
+        name="write_out",
+    )(*(pltpu.with_memory_space_constraint(o, pltpu.VMEM) for o in out))
     return d_queries, d_keys, d_values, d_table.T, d_gains
 
 

time: 44.2 us -> 40.1 us (0.907)
  the two profiles are of different devices: /device:TPU:6 before, /device:TPU:1 now
where the time goes in v2:
time: 40.1 us; the launch traced here: 39.4 us
  Pallas kernels  38.7 us (97%)
  between operations  0.64 us (2%)
    pallas_call x1, Pallas kernels, local(): pl.pallas_call(functools.partial(kernel, sizes), out_shape=tuple((vmem(*o...  38 us

profile of v2, /device:TPU:1, one launch (start us, length us, event | category | flops | bytes accessed | tf_op | source)
XLA Modules:
  0.0 39.4 jit_solution(88575679953363698)
XLA Ops:
  0.6 38.0 %segment_attention_grad.1 = (bf16[256,256]{1,0:T(8,128)(2,1)S(1)}, bf16[256,256]{1,0:T(8,128)(2,1)S(1)}, bf16[256,256]{1,0:T(8,128)(2,1)S(1)}, f32[2,192]{1,0:T(2,128)S(1)}, f32[2,128]{1,0:T(2,128)S(1)}) custom-call(bf16[256,256]{1,0:T(8,128)(2,1)} %q_hbm.1, bf16[256,256]{1,0:T(8,128)(2,1)} %k_hbm.1, bf16[256,256]{1,0:T(8,128)(2,1)} %v_hbm.1, ...), custom_call_target="tpu_custom_call" | custom-call | tf_op jit(solution)/shard_map/segment_attention_grad/pallas_call | solution.py:423
  38.6 0.8 %write_out.1 = (bf16[256,256]{1,0:T(8,128)(2,1)}, bf16[256,256]{1,0:T(8,128)(2,1)}, bf16[256,256]{1,0:T(8,128)(2,1)}, f32[2,192]{1,0:T(2,128)}, f32[2,128]{1,0:T(2,128)}) custom-call(bf16[256,256]{1,0:T(8,128)(2,1)S(1)} %get-tuple-element.15.refs_0_, bf16[256,256]{1,0:T(8,128)(2,1)S(1)} %get-tuple-element.16.refs_1_, ...), custom_call_target="tpu_custom_call" | custom-call | tf_op jit(solution)/shard_map/write_out/pallas_call | solution.py:446

commit v3 on v2

--- a/solution.py
+++ b/solution.py
@@ -47,13 +47,12 @@
 
 def kernel(sizes, q_hbm, k_hbm, v_hbm, do_hbm, gains_hbm, table_hbm,
            dq_v, dk_v, dv_v, dtab_v, dgain_v,
-           qx, kx, vx, dox, gains_v, table_v,
+           qdx, kvx, gains_v, table_v,
            qn, qu, qr, kn, ku, kr, bias_v, e_v, dp_v,
            dkx, dvx, dqx, d_v, back_out, back_in,
-           xbuf, ybuf, zbuf, fin,
-           in_sem, halo_send, halo_recv, back_send, back_recv,
-           x_send, x_recv, y_send, y_recv, z_send, z_recv, fin_send, fin_recv,
-           round1, round2, round3, row_sem):
+           lines, zout, zbuf,
+           load_sem, gains_sem, table_sem, halo_send, halo_recv, back_send, back_recv,
+           xy_send, x_recv, y_recv, z_send, z_recv, round1, round2, round3, row_sem):
     nz, ny, nx = sizes
     z, y, x, tp = (lax.axis_index(a) for a in AXES)
     place = (z * ny + y) * nx + x
@@ -83,15 +82,16 @@
     barrier = pltpu.get_barrier_semaphore()
     signal(barrier, before)
     signal(barrier, after)
-    loads = []
-    for n, (src, dst, first) in enumerate(((k_hbm, kx, ROWS), (v_hbm, vx, ROWS), (q_hbm, qx, 0), (do_hbm, dox, 0))):
+    for n, (src, dst, first) in enumerate(((k_hbm, kvx.at[0], ROWS), (v_hbm, kvx.at[1], ROWS), (q_hbm, qdx.at[0], 0), (do_hbm, qdx.at[1], 0))):
         for h in range(HEADS):
-            loads.append(pltpu.make_async_copy(
-                src.at[:, h * HEAD_DIM:(h + 1) * HEAD_DIM], dst.at[h, first:first + ROWS], in_sem.at[2 * n + h]))
-    loads.append(pltpu.make_async_copy(gains_hbm, gains_v, in_sem.at[8]))
-    loads.append(pltpu.make_async_copy(table_hbm, table_v, in_sem.at[9]))
-    for load in loads:
+            pltpu.make_async_copy(
+                src.at[:, h * HEAD_DIM:(h + 1) * HEAD_DIM], dst.at[h, first:first + ROWS], load_sem.at[n // 2]).start()
+    small_loads = [pltpu.make_async_copy(gains_hbm, gains_v, gains_sem), pltpu.make_async_copy(table_hbm, table_v, table_sem)]
+    for load in small_loads:
         load.start()
+
+    def wait_bytes(ref, sem):
+        pltpu.make_async_copy(ref, ref, sem).wait()
 
     close = [(a, o) for a, n in enumerate(sizes) for o in near(n)]
 
@@ -107,40 +107,38 @@
         signal(barrier, (z, y, x, 1))
         pl.semaphore_wait(barrier, 3)
 
+    wait_bytes(kvx.at[:, :, ROWS:], load_sem.at[0])
     halo = {}
-    for load in loads[:4]:
-        load.wait()
     for h in range(HEADS):
         for half in (1, 0):
-            for n, buf in enumerate((kx, vx)):
-                slot = (h * 2 + half) * 2 + n
-                copy = remote(
-                    buf.at[h, ROWS + half * PAIR:ROWS + (half + 1) * PAIR],
-                    buf.at[h, half * PAIR:(half + 1) * PAIR],
-                    halo_send.at[slot], halo_recv.at[slot], after)
-                copy.start()
-                halo[h, half, n] = copy
+            slot = h * 2 + half
+            halo[h, half] = remote(
+                kvx.at[:, h, ROWS + half * PAIR:ROWS + (half + 1) * PAIR],
+                kvx.at[:, h, half * PAIR:(half + 1) * PAIR],
+                halo_send, halo_recv.at[slot], after)
+            halo[h, half].start()
 
     @pl.when(tp == 1)
     def _():
         for a, o in close:
             signal(round1, along(a, o))
 
-    for load in loads[4:]:
+    wait_bytes(qdx, load_sem.at[1])
+    for load in small_loads:
         load.wait()
 
     gains = gains_v[...]
     gain_q, gain_k = gains[0:1, :], gains[1:2, :]
 
     def norm_keys(h, first, size):
-        u, r = unit(kx[h, first:first + size])
+        u, r = unit(kvx[0, h, first:first + size])
         ku[h, first:first + size] = u
         kn[h, first:first + size] = (u * gain_k).astype(BF16)
         if first >= ROWS:
             kr[h, first - ROWS:first - ROWS + size] = jnp.broadcast_to(r, u.shape)
 
     for h in range(HEADS):
-        u, r = unit(qx[h])
+        u, r = unit(qdx[0, h])
         qu[h] = u
         qr[h] = jnp.broadcast_to(r, u.shape)
         qn[h] = (u * gain_q).astype(BF16)
@@ -181,7 +179,7 @@
         own = slice(p * PAIR, (p + 1) * PAIR)
         s = dot(kn[h, first:first + PAIR], qn[h, own], 1, 1)
         e = jnp.exp2(s * (FACTOR * LOG2E) + bias_v[h, p, b * PAIR:(b + 1) * PAIR])
-        dp = dot(vx[h, first:first + PAIR], dox[h, own], 1, 1)
+        dp = dot(kvx[1, h, first:first + PAIR], qdx[1, h, own], 1, 1)
         e_v[h, p, b * PAIR:(b + 1) * PAIR] = e
         dp_v[h, p, b * PAIR:(b + 1) * PAIR] = dp
         norm, weighted = sums[h, p]
@@ -199,7 +197,7 @@
         d_score = prob * (dp_v[h, p] - delta)
         prob_low = prob.astype(BF16)
         d_low = d_score.astype(BF16)
-        dv = dot(prob_low, dox[h, own], 1, 0)
+        dv = dot(prob_low, qdx[1, h, own], 1, 0)
         dk = dot(d_low, qn[h, own], 1, 0)
         dq = dot(d_low, kn[h, keys], 0, 0)
         dqx[h, own] = dq
@@ -257,9 +255,8 @@
 
     for h in range(HEADS):
         for half in (1, 0):
-            halo[h, half, 0].wait_recv()
+            halo[h, half].wait_recv()
             norm_keys(h, half * PAIR, PAIR)
-            halo[h, half, 1].wait_recv()
             if half:
                 block(h, 1, 0)
                 block(h, 0, 1)
@@ -275,7 +272,7 @@
                 if count:
                     pl.semaphore_wait(round2, count)
                 if nz > 9:
-                    for o in near(nz, 2):
+                    for o in near(nz, 3):
                         signal(round3, along(0, o))
 
     row = lax.broadcasted_iota(jnp.int32, (8, HEAD_DIM), 0)
@@ -286,12 +283,10 @@
     for j in range(2):
         vec = jnp.where(row == 6 + j, gain_sums[j] * FACTOR, vec)
     mine = 2 * x + tp
-    xbuf[mine] = vec
-
-    def back_copies(h):
-        return [
-            remote(back_out.at[n, h], back_in.at[n, h], back_send.at[2 * n + h], back_recv.at[2 * n + h], before)
-            for n in range(2)]
+    lines[mine] = vec
+
+    backs = [
+        remote(back_out.at[:, h], back_in.at[:, h], back_send, back_recv.at[h], before) for h in range(HEADS)]
 
     def stage_back():
         for h in range(HEADS):
@@ -305,99 +300,80 @@
             dq_v[:, h * HEAD_DIM:(h + 1) * HEAD_DIM] = (
                 qr[h] * (g - u * jnp.mean(g * u, axis=-1, keepdims=True))).astype(BF16)
 
+    def line_sum(first, count):
+        part = lines[first]
+        for n in range(first + 1, first + count):
+            part = part + lines[n]
+        return part
+
+    ys, zs = 2 * nx, 2 * nx + ny
+
     @pl.when(tp == 1)
     def _():
         if nz > 9:
-            pl.semaphore_wait(round3, len(near(nz, 2)))
-        sends = [
-            remote(xbuf.at[mine], xbuf.at[mine], x_send.at[o], x_recv.at[mine], along(2, o)) for o in far_first(nx)]
-        for copy in sends:
+            pl.semaphore_wait(round3, len(near(nz, 3)))
+        for o in far_first(nx):
+            remote(lines.at[mine], lines.at[mine], xy_send, x_recv, along(2, o)).start()
+        stage_back()
+        wait_bytes(lines.at[:2 * nx - 1], x_recv)
+        lines[ys + y] = line_sum(0, 2 * nx)
+        for o in far_first(ny):
+            remote(lines.at[ys + y], lines.at[ys + y], xy_send, y_recv, along(1, o)).start()
+        finish_queries()
+        if ny > 1:
+            wait_bytes(lines.at[:ny - 1], y_recv)
+        part = line_sum(ys, ny)
+        for core in range(2):
+            zout[core, :3] = part[3 * core:3 * core + 3]
+            zout[core, 3:] = part[6:]
+        zbuf[z] = zout[1]
+        for o in [*far_first(nz), 0]:
+            for core in range(2 if o else 1):
+                remote(zout.at[core], zbuf.at[z], z_send, z_recv, along(0, o, core)).start()
+        for copy in backs:
             copy.start()
-        stage_back()
-        for o in range(nx):
-            for core in range(2):
-                if o or not core:
-                    slot = 2 * lax.rem(x + o, nx) + core
-                    pltpu.make_async_copy(xbuf.at[slot], xbuf.at[slot], x_recv.at[slot]).wait()
-        part = xbuf[0]
-        for n in range(1, 2 * nx):
-            part = part + xbuf[n]
-        ybuf[y] = part
-        moves = [remote(ybuf.at[y], ybuf.at[y], y_send.at[o], y_recv.at[y], along(1, o)) for o in far_first(ny)]
-        for copy in moves:
-            copy.start()
-        sends += moves
-        finish_queries()
-        for o in range(1, ny):
-            slot = lax.rem(y + o, ny)
-            pltpu.make_async_copy(ybuf.at[slot], ybuf.at[slot], y_recv.at[slot]).wait()
-        part = ybuf[0]
-        for n in range(1, ny):
-            part = part + ybuf[n]
-        zbuf[z] = part
-        moves = [remote(zbuf.at[z], zbuf.at[z], z_send.at[o], z_recv.at[z], along(0, o)) for o in far_first(nz)]
-        for copy in moves:
-            copy.start()
-        sends += moves
-        for h in range(HEADS):
-            for copy in back_copies(h):
-                copy.start()
-        for copy in sends:
-            copy.wait_send()
 
     @pl.when(tp == 0)
     def _():
         pl.semaphore_wait(row_sem, 1)
-        sends = [
-            remote(xbuf.at[mine], xbuf.at[mine], x_send.at[o], x_recv.at[mine], along(2, o))
-            for o in [*far_first(nx), 0]]
-        for copy in sends:
-            copy.start()
+        for o in [*far_first(nx), 0]:
+            remote(lines.at[mine], lines.at[mine], xy_send, x_recv, along(2, o)).start()
         stage_back()
         finish_queries()
-        for h in range(HEADS):
-            for copy in back_copies(h):
-                copy.start()
-        for copy in sends:
-            copy.wait_send()
-
-    for copy in halo.values():
-        copy.wait_send()
-    for h in range(HEADS):
-        back_k, back_v = back_copies(h)
-        back_k.wait()
-        back_v.wait()
+        for copy in backs:
+            copy.start()
+
+    wait_bytes(kvx.at[:, :, ROWS:], halo_send)
+    for h in range(HEADS):
+        backs[h].wait_recv()
         lanes = slice(h * HEAD_DIM, (h + 1) * HEAD_DIM)
         keep = jnp.where(place == total - 1, 0.0, 1.0)
         g = (dkx[h, ROWS:] * FACTOR + back_in[0, h].astype(F32) * keep) * gain_k
         u = ku[h, ROWS:]
         dk_v[:, lanes] = (kr[h] * (g - u * jnp.mean(g * u, axis=-1, keepdims=True))).astype(BF16)
         dv_v[:, lanes] = (dvx[h, ROWS:] + back_in[1, h].astype(F32) * keep).astype(BF16)
-    pass_on = remote(fin, fin, fin_send, fin_recv, (z, y, x, 0))
+    wait_bytes(back_out, back_send)
 
     @pl.when(tp == 1)
     def _():
-        for o in range(1, nz):
-            slot = lax.rem(z + o, nz)
-            pltpu.make_async_copy(zbuf.at[slot], zbuf.at[slot], z_recv.at[slot]).wait()
-        part = zbuf[0]
-        for n in range(1, nz):
-            part = part + zbuf[n]
-        fin[...] = part
-        pass_on.start()
+        if nx + ny > 2:
+            wait_bytes(lines.at[:nx + ny - 2], xy_send)
+        wait_bytes(zbuf.at[:2 * nz - 1], z_send)
+        if nz > 1:
+            wait_bytes(zbuf.at[:nz - 1], z_recv)
 
     @pl.when(tp == 0)
     def _():
-        pltpu.make_async_copy(fin, fin, fin_recv).wait()
-
-    tail = fin[pl.ds(3 * tp + 2, 1), :]
+        wait_bytes(lines.at[:nx], xy_send)
+        wait_bytes(zbuf.at[:nz], z_recv)
+
+    result = zbuf[0]
+    for n in range(1, nz):
+        result = result + zbuf[n]
     for j in range(HEADS):
-        dtab_v[j:j + 1, :PAIR] = fin[pl.ds(3 * tp + j, 1), :]
-        dtab_v[j:j + 1, PAIR:] = tail[:, j * SEG:(j + 1) * SEG]
-    dgain_v[...] = fin[6:8, :]
-    @pl.when(tp == 1)
-    def _():
-        pass_on.wait_send()
+        dtab_v[j:j + 1, :PAIR] = result[j:j + 1]
+        dtab_v[j:j + 1, PAIR:] = result[2:3, j * SEG:(j + 1) * SEG]
+    dgain_v[...] = result[3:]
 
 
 def write_out(*refs):
@@ -426,18 +402,16 @@
         in_specs=[hbm_spec] * 6,
         out_specs=(vmem_spec,) * 5,
         scratch_shapes=[
-            vmem(tile, BF16), vmem(wide, BF16), vmem(wide, BF16), vmem(tile, BF16),
+            vmem((2, *tile), BF16), vmem((2, *wide), BF16),
             vmem((2, HEAD_DIM), F32), vmem((HEADS, ENTRIES), F32),
             vmem(tile, BF16), vmem(tile, F32), vmem(tile, F32),
             vmem(wide, BF16), vmem(wide, F32), vmem(tile, F32),
             vmem(pairs, F32), vmem(pairs, F32), vmem(pairs, F32),
             vmem(wide, F32), vmem(wide, F32), vmem(tile, F32), vmem((HEADS, 3 * PAIR, PAIR), F32),
             vmem((2, *tile), BF16), vmem((2, *tile), BF16),
-            vmem((2 * nx, 8, HEAD_DIM), F32), vmem((ny, 8, HEAD_DIM), F32), vmem((nz, 8, HEAD_DIM), F32),
-            vmem((8, HEAD_DIM), F32),
-            dma((10,)), dma((8,)), dma((8,)), dma((4,)), dma((4,)),
-            dma((nx,)), dma((2 * nx,)), dma((ny,)), dma((ny,)), dma((nz,)), dma((nz,)), dma, dma,
-            regular, regular, regular, regular,
+            vmem((2 * nx + ny, 8, HEAD_DIM), F32), vmem((2, 5, HEAD_DIM), F32), vmem((2 * nz, 5, HEAD_DIM), F32),
+            dma((2,)), dma, dma, dma, dma((4,)), dma, dma((HEADS,)),
+            dma, dma, dma, dma, dma, regular, regular, regular, regular,
         ],
         compiler_params=pltpu.CompilerParams(
             collective_id=0, has_side_effects=True, vmem_limit_bytes=32 * 1024 * 1024),

time: 40.1 us -> 39 us (0.973)
  Pallas kernels: 38.7 us -> 37.7 us
    pallas_call x1, Pallas kernels: 38 us -> 36.9 us  [local(): pl.pallas_call(functools.partial(kernel, sizes), out_shape=tuple((vmem(*o...]
where the time goes in v3:
time: 39 us; the launch traced here: 38.4 us
  Pallas kernels  37.7 us (97%)
  between operations  0.64 us (2%)
    pallas_call x1, Pallas kernels, local(): pl.pallas_call(functools.partial(kernel, sizes), out_shape=tuple((vmem(*o...  36.9 us
    pallas_call x1, Pallas kernels, local(): pl.pallas_call(write_out, out_shape=tuple((jax.ShapeDtypeStruct(*o) for o...  0.79 us

profile of v3, /device:TPU:1, one launch (start us, length us, event | category | flops | bytes accessed | tf_op | source)
XLA Modules:
  0.0 38.4 jit_solution(15102363284181789983)
XLA Ops:
  0.6 36.9 %segment_attention_grad.1 = (bf16[256,256]{1,0:T(8,128)(2,1)S(1)}, bf16[256,256]{1,0:T(8,128)(2,1)S(1)}, bf16[256,256]{1,0:T(8,128)(2,1)S(1)}, f32[2,192]{1,0:T(2,128)S(1)}, f32[2,128]{1,0:T(2,128)S(1)}) custom-call(bf16[256,256]{1,0:T(8,128)(2,1)} %q_hbm.1, bf16[256,256]{1,0:T(8,128)(2,1)} %k_hbm.1, bf16[256,256]{1,0:T(8,128)(2,1)} %v_hbm.1, ...), custom_call_target="tpu_custom_call" | custom-call | tf_op jit(solution)/shard_map/segment_attention_grad/pallas_call | solution.py:399
  37.6 0.8 %write_out.1 = (bf16[256,256]{1,0:T(8,128)(2,1)}, bf16[256,256]{1,0:T(8,128)(2,1)}, bf16[256,256]{1,0:T(8,128)(2,1)}, f32[2,192]{1,0:T(2,128)}, f32[2,128]{1,0:T(2,128)}) custom-call(bf16[256,256]{1,0:T(8,128)(2,1)S(1)} %get-tuple-element.15.refs_0_, bf16[256,256]{1,0:T(8,128)(2,1)S(1)} %get-tuple-element.16.refs_1_, ...), custom_call_target="tpu_custom_call" | custom-call | tf_op jit(solution)/shard_map/write_out/pallas_call | solution.py:420

commit v4 on v3

--- a/solution.py
+++ b/solution.py
@@ -17,6 +17,7 @@
 ROWS = LEFT * SEG
 HEADS = 2
 PAIR = 2 * SEG
+BEFORE = 3 * SEG
 AXES = ("sp_0", "sp_1", "sp_2", "tp")
 SP = AXES[:3]
 
@@ -47,22 +48,24 @@
 
 def kernel(sizes, q_hbm, k_hbm, v_hbm, do_hbm, gains_hbm, table_hbm,
            dq_v, dk_v, dv_v, dtab_v, dgain_v,
-           qdx, kvx, gains_v, table_v,
+           qdx, qd0, kvx, gains_v, table_v,
            qn, qu, qr, kn, ku, kr, bias_v, e_v, dp_v,
-           dkx, dvx, dqx, d_v, back_out, back_in,
+           dkx, dvx, dqx, d_v, extra_gains,
+           to_before, from_after, to_after, from_before, dq_to_after, dq_from_before,
            lines, zout, zbuf,
-           load_sem, gains_sem, table_sem, halo_send, halo_recv, back_send, back_recv,
+           load_sem, gains_sem, table_sem, halo_send, left_recv, right_recv, back_send, after_recv, before_recv,
            xy_send, x_recv, y_recv, z_send, z_recv, round1, round2, round3, row_sem):
     nz, ny, nx = sizes
     z, y, x, tp = (lax.axis_index(a) for a in AXES)
     place = (z * ny + y) * nx + x
     total = nz * ny * nx
+    is_first, is_last = place == 0, place == total - 1
 
     def at(number, core):
         return (number // (ny * nx), (number // nx) % ny, number % nx, core)
 
-    after = at(lax.rem(place + 1, total), tp)
-    before = at(lax.rem(place + total - 1, total), tp)
+    after = at(jnp.minimum(place + 1, total - 1), tp)
+    before = at(jnp.maximum(place - 1, 0), tp)
 
     def along(axis, offset, core=1):
         if axis == 0:
@@ -79,20 +82,32 @@
             src_ref=src, dst_ref=dst, send_sem=send, recv_sem=recv,
             device_id=target, device_id_type=pl.DeviceIdType.MESH)
 
+    def wait_bytes(ref, sem):
+        pltpu.make_async_copy(ref, ref, sem).wait()
+
     barrier = pltpu.get_barrier_semaphore()
-    signal(barrier, before)
-    signal(barrier, after)
-    for n, (src, dst, first) in enumerate(((k_hbm, kvx.at[0], ROWS), (v_hbm, kvx.at[1], ROWS), (q_hbm, qdx.at[0], 0), (do_hbm, qdx.at[1], 0))):
+
+    @pl.when(place > 0)
+    def _():
+        signal(barrier, before)
+
+    @pl.when(place < total - 1)
+    def _():
+        signal(barrier, after)
+
+    sides = jnp.where(is_first, 0, 1) + jnp.where(is_last, 0, 1)
+    for n, (src, dst) in enumerate(((k_hbm, kvx.at[0]), (v_hbm, kvx.at[1]), (q_hbm, qdx.at[0]), (do_hbm, qdx.at[1]))):
         for h in range(HEADS):
-            pltpu.make_async_copy(
-                src.at[:, h * HEAD_DIM:(h + 1) * HEAD_DIM], dst.at[h, first:first + ROWS], load_sem.at[n // 2]).start()
+            lanes = slice(h * HEAD_DIM, (h + 1) * HEAD_DIM)
+            if n < 2:
+                pltpu.make_async_copy(src.at[:, lanes], dst.at[h, BEFORE:BEFORE + ROWS], load_sem.at[0]).start()
+            else:
+                pltpu.make_async_copy(src.at[:SEG, lanes], qd0.at[n - 2, h], load_sem.at[0]).start()
+                pltpu.make_async_copy(src.at[SEG:, lanes], dst.at[h, :BEFORE], load_sem.at[1]).start()
     small_loads = [pltpu.make_async_copy(gains_hbm, gains_v, gains_sem), pltpu.make_async_copy(table_hbm, table_v, table_sem)]
     for load in small_loads:
         load.start()
 
-    def wait_bytes(ref, sem):
-        pltpu.make_async_copy(ref, ref, sem).wait()
-
     close = [(a, o) for a, n in enumerate(sizes) for o in near(n)]
 
     @pl.when(tp == 1)
@@ -100,32 +115,62 @@
         for a, o in close:
             signal(barrier, along(a, o))
         signal(barrier, (z, y, x, 0))
-        pl.semaphore_wait(barrier, 3 + len(close))
+        pl.semaphore_wait(barrier, 1 + len(close) + sides)
 
     @pl.when(tp == 0)
     def _():
         signal(barrier, (z, y, x, 1))
-        pl.semaphore_wait(barrier, 3)
-
-    wait_bytes(kvx.at[:, :, ROWS:], load_sem.at[0])
-    halo = {}
+        pl.semaphore_wait(barrier, 1 + sides)
+
+    wait_bytes(kvx.at[:, :, :ROWS + SEG], load_sem.at[0])
+    forth, back = {}, {}
     for h in range(HEADS):
-        for half in (1, 0):
-            slot = h * 2 + half
-            halo[h, half] = remote(
-                kvx.at[:, h, ROWS + half * PAIR:ROWS + (half + 1) * PAIR],
-                kvx.at[:, h, half * PAIR:(half + 1) * PAIR],
-                halo_send, halo_recv.at[slot], after)
-            halo[h, half].start()
+        forth[h, 1] = remote(
+            kvx.at[:, h, ROWS + PAIR:ROWS + BEFORE], kvx.at[:, h, PAIR:BEFORE],
+            halo_send.at[0], left_recv.at[2 * h + 1], after)
+        forth[h, 0] = remote(
+            kvx.at[:, h, ROWS:ROWS + PAIR], kvx.at[:, h, :PAIR],
+            halo_send.at[0], left_recv.at[2 * h], after)
+        back[h] = [
+            remote(kvx.at[:, h, BEFORE:ROWS], kvx.at[:, h, BEFORE + ROWS:], halo_send.at[1], right_recv.at[h], before),
+            remote(qd0.at[:, h], qdx.at[:, h, BEFORE:], halo_send.at[1], right_recv.at[h], before)]
+
+    @pl.when(place < total - 1)
+    def _():
+        for copy in forth.values():
+            copy.start()
+
+    @pl.when(place > 0)
+    def _():
+        for copies in back.values():
+            for copy in copies:
+                copy.start()
 
     @pl.when(tp == 1)
     def _():
         for a, o in close:
             signal(round1, along(a, o))
 
-    wait_bytes(qdx, load_sem.at[1])
+    wait_bytes(qdx.at[:, :, :BEFORE], load_sem.at[1])
     for load in small_loads:
         load.wait()
+
+    @pl.when(is_first)
+    def _():
+        for h in range(HEADS):
+            for n in range(2):
+                kvx[n, h, :BEFORE] = kvx[n, h, BEFORE:2 * BEFORE]
+                from_before[n, h] = jnp.zeros((SEG, HEAD_DIM), BF16)
+        extra_gains[...] = jnp.zeros((2, HEAD_DIM), F32)
+
+    @pl.when(is_last)
+    def _():
+        for h in range(HEADS):
+            for n in range(2):
+                kvx[n, h, BEFORE + ROWS:] = kvx[n, h, BEFORE:ROWS]
+                from_after[n, h] = jnp.zeros((BEFORE, HEAD_DIM), BF16)
+            qdx[0, h, BEFORE:] = qd0[0, h]
+            qdx[1, h, BEFORE:] = jnp.zeros((SEG, HEAD_DIM), BF16)
 
     gains = gains_v[...]
     gain_q, gain_k = gains[0:1, :], gains[1:2, :]
@@ -134,15 +179,18 @@
         u, r = unit(kvx[0, h, first:first + size])
         ku[h, first:first + size] = u
         kn[h, first:first + size] = (u * gain_k).astype(BF16)
-        if first >= ROWS:
-            kr[h, first - ROWS:first - ROWS + size] = jnp.broadcast_to(r, u.shape)
+        if size == ROWS:
+            kr[h] = jnp.broadcast_to(r, u.shape)
+
+    def norm_queries(h, first, size):
+        u, r = unit(qdx[0, h, first:first + size])
+        qu[h, first:first + size] = u
+        qr[h, first:first + size] = jnp.broadcast_to(r, u.shape)
+        qn[h, first:first + size] = (u * gain_q).astype(BF16)
 
     for h in range(HEADS):
-        u, r = unit(qdx[0, h])
-        qu[h] = u
-        qr[h] = jnp.broadcast_to(r, u.shape)
-        qn[h] = (u * gain_q).astype(BF16)
-        norm_keys(h, ROWS, ROWS)
+        norm_queries(h, 0, BEFORE)
+        norm_keys(h, BEFORE, ROWS)
 
     key_at = lax.broadcasted_iota(jnp.int32, (PAIR, PAIR), 0)
     query_at = lax.broadcasted_iota(jnp.int32, (PAIR, PAIR), 1)
@@ -155,7 +203,6 @@
     high_part = jnp.concatenate([table[:, PAIR:], jnp.zeros((HEADS, 2 * PAIR - ENTRIES), F32)], axis=1)
     low_rolled = pltpu.roll(low_part, PAIR - SEG + 1, 1)
     high_rolled = pltpu.roll(high_part, PAIR - SEG + 1, 1)
-    is_first = place == 0
     for h in range(HEADS):
         last = table[h:h + 1, ENTRIES - 1:ENTRIES]
         dist_low = low_rolled[h:h + 1]
@@ -165,11 +212,12 @@
         tile0 = jnp.where(jnp.logical_or(early, high), last, MASKED)
         tile1 = jnp.where(past, last, behind)
         tile2 = jnp.where(jnp.logical_and(early, high), MASKED, jnp.where(past, behind, ahead))
-        tile0 = jnp.where(is_first, MASKED, tile0)
-        for p in range(2):
-            mid = jnp.where(is_first, MASKED, tile1) if p == 0 else tile1
-            top = jnp.max(jnp.maximum(jnp.maximum(tile0, mid), tile2), axis=0, keepdims=True)
-            for b, tile in enumerate((tile0, mid, tile2)):
+        none, low = (jnp.where(is_first, MASKED, t) for t in (tile0, tile1))
+        for p, tiles in enumerate((
+                (none, jnp.where(high, tile1, low), tile2),
+                (jnp.where(high, tile0, none), tile1, tile2))):
+            top = jnp.max(jnp.maximum(jnp.maximum(tiles[0], tiles[1]), tiles[2]), axis=0, keepdims=True)
+            for b, tile in enumerate(tiles):
                 bias_v[h, p, b * PAIR:(b + 1) * PAIR] = (tile - top) * LOG2E
 
     sums = {(h, p): (jnp.zeros((1, PAIR), F32), jnp.zeros((1, PAIR), F32)) for h in range(HEADS) for p in range(2)}
@@ -214,13 +262,40 @@
             dvx[h, PAIR:3 * PAIR] = dvx[h, PAIR:3 * PAIR] + dv[PAIR:]
             d_v[h] = d_v[h] + d_score
 
+    def query_rows(g, u, r):
+        g = g * FACTOR * gain_q
+        return (r * (g - u * jnp.mean(g * u, axis=-1, keepdims=True))).astype(BF16)
+
+    def first_segment(h):
+        u, r = unit(qd0[0, h])
+        queries = (u * gain_q).astype(BF16)
+        keys = kn[h, BEFORE:ROWS]
+        bias = bias_v[h, 0, 2 * PAIR:2 * PAIR + SEG][:, :SEG]
+        bias = bias - jnp.max(bias, axis=0, keepdims=True)
+        e = jnp.exp2(dot(keys, queries, 1, 1) * (FACTOR * LOG2E) + bias)
+        dp = dot(kvx[1, h, BEFORE:ROWS], qd0[1, h], 1, 1)
+        inv = 1.0 / jnp.sum(e, axis=0, keepdims=True)
+        delta = jnp.sum(e * dp, axis=0, keepdims=True) * inv
+        prob = e * inv
+        d_score = prob * (dp - delta)
+        d_low = d_score.astype(BF16)
+        dk = dot(d_low, queries, 1, 0)
+        dq = dot(d_low, keys, 0, 0)
+        from_before[0, h] = (dk * FACTOR).astype(BF16)
+        from_before[1, h] = dot(prob.astype(BF16), qd0[1, h], 1, 0).astype(BF16)
+        dq_from_before[:, h * HEAD_DIM:(h + 1) * HEAD_DIM] = query_rows(dq, u, r)
+        at_tile = slice(2 * PAIR, 2 * PAIR + SEG)
+        d_v[h, at_tile] = d_v[h, at_tile] + jnp.concatenate([d_score, jnp.zeros((SEG, SEG), F32)], axis=1)
+        extra_gains[0:1] = extra_gains[0:1] + jnp.sum(dq * u, axis=0, keepdims=True)
+        extra_gains[1:2] = extra_gains[1:2] + jnp.sum(dk * ku[h, BEFORE:ROWS], axis=0, keepdims=True)
+
     table_rows = []
     sublane = lax.broadcasted_iota(jnp.int32, (8, PAIR), 0)
 
     def skewed_sum(tile):
-        total = tile[:8]
+        total = pltpu.roll(tile[:8], SEG - 1, 1)
         for first in range(8, PAIR, 8):
-            total = total + pltpu.roll(tile[first:first + 8], PAIR - first, 1)
+            total = total + pltpu.roll(tile[first:first + 8], (SEG - 1 - first) % PAIR, 1)
         for bit in (1, 2, 4):
             total = jnp.where((sublane & bit) == 0, total, pltpu.roll(total, PAIR - bit, 1))
         return jnp.sum(total, axis=0, keepdims=True)
@@ -232,16 +307,12 @@
         rest = d0 + jnp.where(past, d1, 0.0)
         behind_row, ahead_row = skewed_sum(mixed), skewed_sum(ahead)
         rest_sum = jnp.sum(jnp.sum(rest, axis=0, keepdims=True), axis=1, keepdims=True)
-        behind_row = pltpu.roll(behind_row, SEG - 1, 1)
-        ahead_row = pltpu.roll(ahead_row, SEG - 1, 1)
         table_rows.append((
             jnp.where(lane < SEG - 1, ahead_row, behind_row),
             jnp.where(lane == SEG - 1, rest_sum, behind_row),
         ))
 
     for h in range(HEADS):
-        block(h, 1, 1)
-        block(h, 1, 2)
         block(h, 0, 2)
 
     @pl.when(tp == 1)
@@ -254,16 +325,35 @@
                     signal(round2, along(a, o))
 
     for h in range(HEADS):
-        for half in (1, 0):
-            halo[h, half].wait_recv()
-            norm_keys(h, half * PAIR, PAIR)
-            if half:
-                block(h, 1, 0)
-                block(h, 0, 1)
-                finish(h, 1)
-            else:
-                block(h, 0, 0)
-                finish(h, 0)
+        @pl.when(place < total - 1)
+        def _(h=h):
+            wait_bytes(kvx.at[:, h, :PAIR], right_recv.at[h])
+
+        norm_keys(h, BEFORE + ROWS, SEG)
+        norm_queries(h, BEFORE, SEG)
+        block(h, 1, 1)
+        block(h, 1, 2)
+
+        @pl.when(place > 0)
+        def _(h=h):
+            forth[h, 1].wait_recv()
+
+        norm_keys(h, PAIR, SEG)
+        block(h, 1, 0)
+        block(h, 0, 1)
+        finish(h, 1)
+
+        @pl.when(is_first)
+        def _(h=h):
+            first_segment(h)
+
+        @pl.when(place > 0)
+        def _(h=h):
+            forth[h, 0].wait_recv()
+
+        norm_keys(h, 0, PAIR)
+        block(h, 0, 0)
+        finish(h, 0)
         fold_table(h)
         if h == 0:
             @pl.when(tp == 1)
@@ -281,24 +371,38 @@
     for j, part in enumerate((table_rows[0][0], table_rows[1][0], second)):
         vec = jnp.where(row == 3 * tp + j, part, vec)
     for j in range(2):
-        vec = jnp.where(row == 6 + j, gain_sums[j] * FACTOR, vec)
+        part = gain_sums[j] + jnp.where(is_first, extra_gains[j:j + 1], 0.0)
+        vec = jnp.where(row == 6 + j, part * FACTOR, vec)
     mine = 2 * x + tp
     lines[mine] = vec
 
-    backs = [
-        remote(back_out.at[:, h], back_in.at[:, h], back_send, back_recv.at[h], before) for h in range(HEADS)]
-
-    def stage_back():
+    to_neighbours = [
+        remote(to_before.at[:, h], from_after.at[:, h], back_send.at[0], after_recv.at[h], before) for h in range(HEADS)]
+    to_next = [
+        remote(to_after, from_before, back_send.at[1], before_recv, after),
+        remote(dq_to_after, dq_from_before, back_send.at[1], before_recv, after)]
+
+    def stage_results():
         for h in range(HEADS):
-            back_out[0, h] = (dkx[h, :ROWS] * FACTOR).astype(BF16)
-            back_out[1, h] = dvx[h, :ROWS].astype(BF16)
-
-    def finish_queries():
-        for h in range(HEADS):
-            g = dqx[h] * FACTOR * gain_q
-            u = qu[h]
-            dq_v[:, h * HEAD_DIM:(h + 1) * HEAD_DIM] = (
-                qr[h] * (g - u * jnp.mean(g * u, axis=-1, keepdims=True))).astype(BF16)
+            lanes = slice(h * HEAD_DIM, (h + 1) * HEAD_DIM)
+            to_before[0, h] = (dkx[h, :BEFORE] * FACTOR).astype(BF16)
+            to_before[1, h] = dvx[h, :BEFORE].astype(BF16)
+            to_after[0, h] = (dkx[h, BEFORE + ROWS:] * FACTOR).astype(BF16)
+            to_after[1, h] = dvx[h, BEFORE + ROWS:].astype(BF16)
+            rows = query_rows(dqx[h], qu[h], qr[h])
+            dq_v[SEG:, lanes] = rows[:BEFORE]
+            dq_to_after[:, lanes] = rows[BEFORE:]
+
+    def send_results(when):
+        @pl.when(jnp.logical_and(when, place > 0))
+        def _():
+            for copy in to_neighbours:
+                copy.start()
+
+        @pl.when(jnp.logical_and(when, place < total - 1))
+        def _():
+            for copy in to_next:
+                copy.start()
 
     def line_sum(first, count):
         part = lines[first]
@@ -307,6 +411,7 @@
         return part
 
     ys, zs = 2 * nx, 2 * nx + ny
+    at_end = jnp.logical_or(x == 0, x == nx - 1)
 
     @pl.when(tp == 1)
     def _():
@@ -314,12 +419,13 @@
             pl.semaphore_wait(round3, len(near(nz, 3)))
         for o in far_first(nx):
             remote(lines.at[mine], lines.at[mine], xy_send, x_recv, along(2, o)).start()
-        stage_back()
+        stage_results()
+        send_results(jnp.logical_not(at_end))
         wait_bytes(lines.at[:2 * nx - 1], x_recv)
         lines[ys + y] = line_sum(0, 2 * nx)
         for o in far_first(ny):
             remote(lines.at[ys + y], lines.at[ys + y], xy_send, y_recv, along(1, o)).start()
-        finish_queries()
+        send_results(at_end)
         if ny > 1:
             wait_bytes(lines.at[:ny - 1], y_recv)
         part = line_sum(ys, ny)
@@ -330,29 +436,42 @@
         for o in [*far_first(nz), 0]:
             for core in range(2 if o else 1):
                 remote(zout.at[core], zbuf.at[z], z_send, z_recv, along(0, o, core)).start()
-        for copy in backs:
-            copy.start()
 
     @pl.when(tp == 0)
     def _():
         pl.semaphore_wait(row_sem, 1)
         for o in [*far_first(nx), 0]:
             remote(lines.at[mine], lines.at[mine], xy_send, x_recv, along(2, o)).start()
-        stage_back()
-        finish_queries()
-        for copy in backs:
-            copy.start()
-
-    wait_bytes(kvx.at[:, :, ROWS:], halo_send)
+        stage_results()
+        send_results(place >= 0)
+
+    @pl.when(place > 0)
+    def _():
+        wait_bytes(from_after.at[:, 0], before_recv)
+
+    dq_v[:SEG] = dq_from_before[...]
     for h in range(HEADS):
-        backs[h].wait_recv()
+        @pl.when(place < total - 1)
+        def _(h=h):
+            to_neighbours[h].wait_recv()
+
         lanes = slice(h * HEAD_DIM, (h + 1) * HEAD_DIM)
-        keep = jnp.where(place == total - 1, 0.0, 1.0)
-        g = (dkx[h, ROWS:] * FACTOR + back_in[0, h].astype(F32) * keep) * gain_k
-        u = ku[h, ROWS:]
+        sums_in = [
+            jnp.concatenate([from_before[n, h].astype(F32), from_after[n, h].astype(F32)], axis=0) for n in range(2)]
+        g = (dkx[h, BEFORE:BEFORE + ROWS] * FACTOR + sums_in[0]) * gain_k
+        u = ku[h, BEFORE:BEFORE + ROWS]
         dk_v[:, lanes] = (kr[h] * (g - u * jnp.mean(g * u, axis=-1, keepdims=True))).astype(BF16)
-        dv_v[:, lanes] = (dvx[h, ROWS:] + back_in[1, h].astype(F32) * keep).astype(BF16)
-    wait_bytes(back_out, back_send)
+        dv_v[:, lanes] = (dvx[h, BEFORE:BEFORE + ROWS] + sums_in[1]).astype(BF16)
+
+    @pl.when(place < total - 1)
+    def _():
+        wait_bytes(kvx.at[:, :, :BEFORE], halo_send.at[0])
+        wait_bytes(from_after.at[:, 0], back_send.at[1])
+
+    @pl.when(place > 0)
+    def _():
+        wait_bytes(kvx.at[:, :, :PAIR], halo_send.at[1])
+        wait_bytes(from_after, back_send.at[0])
 
     @pl.when(tp == 1)
     def _():
@@ -390,6 +509,7 @@
     width = HEADS * HEAD_DIM
     hbm_spec = pl.BlockSpec(memory_space=pltpu.HBM)
     vmem_spec = pl.BlockSpec(memory_space=pltpu.VMEM)
+    first = (HEADS, SEG, HEAD_DIM)
     tile = (HEADS, ROWS, HEAD_DIM)
     wide = (HEADS, 2 * ROWS, HEAD_DIM)
     pairs = (HEADS, 2, 3 * PAIR, PAIR)
@@ -402,15 +522,16 @@
         in_specs=[hbm_spec] * 6,
         out_specs=(vmem_spec,) * 5,
         scratch_shapes=[
-            vmem((2, *tile), BF16), vmem((2, *wide), BF16),
+            vmem((2, *tile), BF16), vmem((2, *first), BF16), vmem((2, *wide), BF16),
             vmem((2, HEAD_DIM), F32), vmem((HEADS, ENTRIES), F32),
             vmem(tile, BF16), vmem(tile, F32), vmem(tile, F32),
             vmem(wide, BF16), vmem(wide, F32), vmem(tile, F32),
             vmem(pairs, F32), vmem(pairs, F32), vmem(pairs, F32),
-            vmem(wide, F32), vmem(wide, F32), vmem(tile, F32), vmem((HEADS, 3 * PAIR, PAIR), F32),
-            vmem((2, *tile), BF16), vmem((2, *tile), BF16),
+            vmem(wide, F32), vmem(wide, F32), vmem(tile, F32), vmem((HEADS, 3 * PAIR, PAIR), F32), vmem((2, HEAD_DIM), F32),
+            vmem((2, HEADS, BEFORE, HEAD_DIM), BF16), vmem((2, HEADS, BEFORE, HEAD_DIM), BF16),
+            vmem((2, *first), BF16), vmem((2, *first), BF16), vmem((SEG, width), BF16), vmem((SEG, width), BF16),
             vmem((2 * nx + ny, 8, HEAD_DIM), F32), vmem((2, 5, HEAD_DIM), F32), vmem((2 * nz, 5, HEAD_DIM), F32),
-            dma((2,)), dma, dma, dma, dma((4,)), dma, dma((HEADS,)),
+            dma((2,)), dma, dma, dma((2,)), dma((4,)), dma((HEADS,)), dma((2,)), dma((HEADS,)), dma,
             dma, dma, dma, dma, dma, regular, regular, regular, regular,
         ],
         compiler_params=pltpu.CompilerParams(

time: 39 us -> 40.2 us (1.031); the launches traced: 38.4 us -> 40 us
  Pallas kernels: 37.7 us -> 39.3 us
    pallas_call x1, Pallas kernels: 36.9 us -> 38.6 us  [local(): pl.pallas_call(functools.partial(kernel, sizes), out_shape=tuple((vmem(*o...]
where the time goes in v4:
time: 40.2 us; the launch traced here: 40 us
  Pallas kernels  39.3 us (98%)
  between operations  0.64 us (2%)
    pallas_call x1, Pallas kernels, local(): pl.pallas_call(functools.partial(kernel, sizes), out_shape=tuple((vmem(*o...  38.6 us

profile of v4, /device:TPU:1, one launch (start us, length us, event | category | flops | bytes accessed | tf_op | source)
XLA Modules:
  0.0 40.0 jit_solution(652522267195819055)
XLA Ops:
  0.6 38.6 %segment_attention_grad.1 = (bf16[256,256]{1,0:T(8,128)(2,1)S(1)}, bf16[256,256]{1,0:T(8,128)(2,1)S(1)}, bf16[256,256]{1,0:T(8,128)(2,1)S(1)}, f32[2,192]{1,0:T(2,128)S(1)}, f32[2,128]{1,0:T(2,128)S(1)}) custom-call(bf16[256,256]{1,0:T(8,128)(2,1)} %q_hbm.1, bf16[256,256]{1,0:T(8,128)(2,1)} %k_hbm.1, bf16[256,256]{1,0:T(8,128)(2,1)} %v_hbm.1, ...), custom_call_target="tpu_custom_call" | custom-call | tf_op jit(solution)/shard_map/segment_attention_grad/pallas_call | solution.py:519
  39.2 0.8 %write_out.1 = (bf16[256,256]{1,0:T(8,128)(2,1)}, bf16[256,256]{1,0:T(8,128)(2,1)}, bf16[256,256]{1,0:T(8,128)(2,1)}, f32[2,192]{1,0:T(2,128)}, f32[2,128]{1,0:T(2,128)}) custom-call(bf16[256,256]{1,0:T(8,128)(2,1)S(1)} %get-tuple-element.15.refs_0_, bf16[256,256]{1,0:T(8,128)(2,1)S(1)} %get-tuple-element.16.refs_1_, ...), custom_call_target="tpu_custom_call" | custom-call | tf_op jit(solution)/shard_map/write_out/pallas_call | solution.py:541

commit v5 on v4

--- a/solution.py
+++ b/solution.py
@@ -50,7 +50,7 @@
            dq_v, dk_v, dv_v, dtab_v, dgain_v,
            qdx, qd0, kvx, gains_v, table_v,
            qn, qu, qr, kn, ku, kr, bias_v, e_v, dp_v,
-           dkx, dvx, dqx, d_v, extra_gains,
+           dkx, dvx, dqx, d_v, prob_v, sum_v, gain_v, table_v2, extra_gains,
            to_before, from_after, to_after, from_before, dq_to_after, dq_from_before,
            lines, zout, zbuf,
            load_sem, gains_sem, table_sem, halo_send, left_recv, right_recv, back_send, after_recv, before_recv,
@@ -123,21 +123,19 @@
         pl.semaphore_wait(barrier, 1 + sides)
 
     wait_bytes(kvx.at[:, :, :ROWS + SEG], load_sem.at[0])
-    forth, back = {}, {}
+    forth = [remote(
+        kvx.at[:, :, ROWS + PAIR:ROWS + BEFORE], kvx.at[:, :, PAIR:BEFORE], halo_send.at[0], left_recv.at[HEADS], after)]
+    back = {}
     for h in range(HEADS):
-        forth[h, 1] = remote(
-            kvx.at[:, h, ROWS + PAIR:ROWS + BEFORE], kvx.at[:, h, PAIR:BEFORE],
-            halo_send.at[0], left_recv.at[2 * h + 1], after)
-        forth[h, 0] = remote(
-            kvx.at[:, h, ROWS:ROWS + PAIR], kvx.at[:, h, :PAIR],
-            halo_send.at[0], left_recv.at[2 * h], after)
+        forth.append(remote(
+            kvx.at[:, h, ROWS:ROWS + PAIR], kvx.at[:, h, :PAIR], halo_send.at[0], left_recv.at[h], after))
         back[h] = [
             remote(kvx.at[:, h, BEFORE:ROWS], kvx.at[:, h, BEFORE + ROWS:], halo_send.at[1], right_recv.at[h], before),
             remote(qd0.at[:, h], qdx.at[:, h, BEFORE:], halo_send.at[1], right_recv.at[h], before)]
 
     @pl.when(place < total - 1)
     def _():
-        for copy in forth.values():
+        for copy in forth:
             copy.start()
 
     @pl.when(place > 0)
@@ -220,8 +218,6 @@
             for b, tile in enumerate(tiles):
                 bias_v[h, p, b * PAIR:(b + 1) * PAIR] = (tile - top) * LOG2E
 
-    sums = {(h, p): (jnp.zeros((1, PAIR), F32), jnp.zeros((1, PAIR), F32)) for h in range(HEADS) for p in range(2)}
-
     def block(h, p, b):
         first = (p + b) * PAIR
         own = slice(p * PAIR, (p + 1) * PAIR)
@@ -230,37 +226,33 @@
         dp = dot(kvx[1, h, first:first + PAIR], qdx[1, h, own], 1, 1)
         e_v[h, p, b * PAIR:(b + 1) * PAIR] = e
         dp_v[h, p, b * PAIR:(b + 1) * PAIR] = dp
-        norm, weighted = sums[h, p]
-        sums[h, p] = (norm + jnp.sum(e, axis=0, keepdims=True), weighted + jnp.sum(e * dp, axis=0, keepdims=True))
-
-    gain_sums = [jnp.zeros((1, HEAD_DIM), F32), jnp.zeros((1, HEAD_DIM), F32)]
-
-    def finish(h, p):
-        norm, weighted = sums[h, p]
-        inv = 1.0 / norm
-        delta = weighted * inv
+        sum_v[h, p, b] = jnp.sum(e, axis=0, keepdims=True)
+        sum_v[h, p, 3 + b] = jnp.sum(e * dp, axis=0, keepdims=True)
+
+    def finish(h, p, again):
+        inv = 1.0 / (sum_v[h, p, 0] + sum_v[h, p, 1] + sum_v[h, p, 2])
+        delta = (sum_v[h, p, 3] + sum_v[h, p, 4] + sum_v[h, p, 5]) * inv
         own = slice(p * PAIR, (p + 1) * PAIR)
         keys = slice(p * PAIR, (p + 3) * PAIR)
         prob = e_v[h, p] * inv
         d_score = prob * (dp_v[h, p] - delta)
         prob_low = prob.astype(BF16)
         d_low = d_score.astype(BF16)
-        dv = dot(prob_low, qdx[1, h, own], 1, 0)
+        prob_v[h, p] = prob_low
         dk = dot(d_low, qn[h, own], 1, 0)
         dq = dot(d_low, kn[h, keys], 0, 0)
         dqx[h, own] = dq
-        gain_sums[0] = gain_sums[0] + jnp.sum(dq * qu[h, own], axis=0, keepdims=True)
-        gain_sums[1] = gain_sums[1] + jnp.sum(dk * ku[h, keys], axis=0, keepdims=True)
-        if p == 1:
-            dkx[h, keys] = dk
-            dvx[h, keys] = dv
-            d_v[h] = d_score
-        else:
-            dkx[h, 0:PAIR] = dk[:PAIR]
-            dvx[h, 0:PAIR] = dv[:PAIR]
-            dkx[h, PAIR:3 * PAIR] = dkx[h, PAIR:3 * PAIR] + dk[PAIR:]
-            dvx[h, PAIR:3 * PAIR] = dvx[h, PAIR:3 * PAIR] + dv[PAIR:]
-            d_v[h] = d_v[h] + d_score
+        gain_v[h, p, 0] = jnp.sum(dq * qu[h, own], axis=0, keepdims=True)
+        gain_v[h, p, 1] = jnp.sum(dk * ku[h, keys], axis=0, keepdims=True)
+        if again:
+            shared, alone = slice(PAIR, 3 * PAIR), slice(3 * p * PAIR, (3 * p + 1) * PAIR)
+            ours = slice((1 - p) * PAIR, (3 - p) * PAIR)
+            rest = slice(2 * p * PAIR, (2 * p + 1) * PAIR)
+            dkx[h, alone] = dk[rest]
+            dkx[h, shared] = dkx[h, shared] + dk[ours]
+            return d_v[h] + d_score
+        dkx[h, keys] = dk
+        d_v[h] = d_score
 
     def query_rows(g, u, r):
         g = g * FACTOR * gain_q
@@ -289,28 +281,27 @@
         extra_gains[0:1] = extra_gains[0:1] + jnp.sum(dq * u, axis=0, keepdims=True)
         extra_gains[1:2] = extra_gains[1:2] + jnp.sum(dk * ku[h, BEFORE:ROWS], axis=0, keepdims=True)
 
-    table_rows = []
     sublane = lax.broadcasted_iota(jnp.int32, (8, PAIR), 0)
 
-    def skewed_sum(tile):
-        total = pltpu.roll(tile[:8], SEG - 1, 1)
-        for first in range(8, PAIR, 8):
-            total = total + pltpu.roll(tile[first:first + 8], (SEG - 1 - first) % PAIR, 1)
-        for bit in (1, 2, 4):
-            total = jnp.where((sublane & bit) == 0, total, pltpu.roll(total, PAIR - bit, 1))
+    def skewed_sum(tile, right):
+        parts = [pltpu.roll(tile[first:first + 8], (right - first) % PAIR, 1) for first in range(0, PAIR, 8)]
+        while len(parts) > 1:
+            parts = [a + b for a, b in zip(parts[::2], parts[1::2])]
+        total = parts[0]
+        for bit in range(1, 8):
+            total = jnp.where(sublane == bit, pltpu.roll(parts[0], PAIR - bit, 1), total)
         return jnp.sum(total, axis=0, keepdims=True)
 
-    def fold_table(h):
-        d0, d1, d2 = (d_v[h, b * PAIR:(b + 1) * PAIR] for b in range(3))
+    def fold_table(h, d_score):
+        d0, d1, d2 = (d_score[b * PAIR:(b + 1) * PAIR] for b in range(3))
         mixed = jnp.where(past, d2, d1)
         ahead = jnp.where(past, 0.0, d2)
         rest = d0 + jnp.where(past, d1, 0.0)
-        behind_row, ahead_row = skewed_sum(mixed), skewed_sum(ahead)
+        behind_row, ahead_row = skewed_sum(mixed, SEG - 1), skewed_sum(ahead, SEG - 1)
+        high_row = skewed_sum(mixed, SEG - 1 + SEG) if h else behind_row
         rest_sum = jnp.sum(jnp.sum(rest, axis=0, keepdims=True), axis=1, keepdims=True)
-        table_rows.append((
-            jnp.where(lane < SEG - 1, ahead_row, behind_row),
-            jnp.where(lane == SEG - 1, rest_sum, behind_row),
-        ))
+        table_v2[h, 0] = jnp.where(lane < SEG - 1, ahead_row, behind_row)
+        table_v2[h, 1] = jnp.where(lane == SEG - 1 + h * SEG, rest_sum, high_row)
 
     for h in range(HEADS):
         block(h, 0, 2)
@@ -324,54 +315,108 @@
                 for o in near(n, 2):
                     signal(round2, along(a, o))
 
-    for h in range(HEADS):
+    def wait_left(piece):
+        @pl.when(place > 0)
+        def _():
+            forth[piece].wait_recv()
+
+    def wait_right(h):
         @pl.when(place < total - 1)
-        def _(h=h):
+        def _():
             wait_bytes(kvx.at[:, h, :PAIR], right_recv.at[h])
 
+    def greet_far():
+        @pl.when(tp == 1)
+        def _():
+            count = sum(len(near(n, 2)) for n in sizes[:2] if n > 5)
+            if count:
+                pl.semaphore_wait(round2, count)
+            if nz > 9:
+                for o in near(nz, 3):
+                    signal(round3, along(0, o))
+
+    def do_first(h):
+        @pl.when(is_first)
+        def _():
+            first_segment(h)
+
+    def from_left_near(h):
+        norm_keys(h, PAIR, SEG)
+        block(h, 0, 1)
+
+    def from_left_far(h):
+        norm_keys(h, 0, PAIR)
+        block(h, 0, 0)
+
+    def from_right(h):
         norm_keys(h, BEFORE + ROWS, SEG)
         norm_queries(h, BEFORE, SEG)
         block(h, 1, 1)
         block(h, 1, 2)
 
-        @pl.when(place > 0)
-        def _(h=h):
-            forth[h, 1].wait_recv()
-
-        norm_keys(h, PAIR, SEG)
-        block(h, 1, 0)
-        block(h, 0, 1)
-        finish(h, 1)
-
-        @pl.when(is_first)
-        def _(h=h):
-            first_segment(h)
-
-        @pl.when(place > 0)
-        def _(h=h):
-            forth[h, 0].wait_recv()
-
-        norm_keys(h, 0, PAIR)
-        block(h, 0, 0)
-        finish(h, 0)
-        fold_table(h)
-        if h == 0:
-            @pl.when(tp == 1)
-            def _():
-                count = sum(len(near(n, 2)) for n in sizes[:2] if n > 5)
-                if count:
-                    pl.semaphore_wait(round2, count)
-                if nz > 9:
-                    for o in near(nz, 3):
-                        signal(round3, along(0, o))
+    @pl.when(x == nx - 1)
+    def _():
+        wait_left(0)
+        for h in range(HEADS):
+            from_left_near(h)
+        for h in range(HEADS):
+            wait_left(1 + h)
+            from_left_far(h)
+            finish(h, 0, False)
+            if nx == 1:
+                do_first(h)
+        greet_far()
+        for h in range(HEADS):
+            wait_right(h)
+            from_right(h)
+            block(h, 1, 0)
+            fold_table(h, finish(h, 1, True))
+
+    if nx > 1:
+        @pl.when(x == 0)
+        def _():
+            for h in range(HEADS):
+                wait_right(h)
+            for h in range(HEADS):
+                from_right(h)
+            wait_left(0)
+            for h in range(HEADS):
+                from_left_near(h)
+                block(h, 1, 0)
+                finish(h, 1, False)
+            for h in range(HEADS):
+                do_first(h)
+            greet_far()
+            for h in range(HEADS):
+                wait_left(1 + h)
+                from_left_far(h)
+                fold_table(h, finish(h, 0, True))
+
+    if nx > 2:
+        @pl.when(jnp.logical_and(x > 0, x < nx - 1))
+        def _():
+            wait_left(0)
+            for h in range(HEADS):
+                from_left_near(h)
+            for h in range(HEADS):
+                wait_right(h)
+                from_right(h)
+                block(h, 1, 0)
+                finish(h, 1, False)
+                if h:
+                    greet_far()
+                wait_left(1 + h)
+                from_left_far(h)
+                fold_table(h, finish(h, 0, True))
 
     row = lax.broadcasted_iota(jnp.int32, (8, HEAD_DIM), 0)
     vec = jnp.zeros((8, HEAD_DIM), F32)
-    second = jnp.where(lane < SEG, table_rows[0][1], pltpu.roll(table_rows[1][1], SEG, 1))
-    for j, part in enumerate((table_rows[0][0], table_rows[1][0], second)):
+    second = jnp.where(lane < SEG, table_v2[0, 1], table_v2[1, 1])
+    for j, part in enumerate((table_v2[0, 0], table_v2[1, 0], second)):
         vec = jnp.where(row == 3 * tp + j, part, vec)
     for j in range(2):
-        part = gain_sums[j] + jnp.where(is_first, extra_gains[j:j + 1], 0.0)
+        part = gain_v[0, 0, j] + gain_v[0, 1, j] + gain_v[1, 0, j] + gain_v[1, 1, j]
+        part = part + jnp.where(is_first, extra_gains[j:j + 1], 0.0)
         vec = jnp.where(row == 6 + j, part * FACTOR, vec)
     mine = 2 * x + tp
     lines[mine] = vec
@@ -384,6 +429,10 @@
 
     def stage_results():
         for h in range(HEADS):
+            low, high_tile = (dot(prob_v[h, p], qdx[1, h, p * PAIR:(p + 1) * PAIR], 1, 0) for p in range(2))
+            dvx[h, :PAIR] = low[:PAIR]
+            dvx[h, PAIR:3 * PAIR] = low[PAIR:] + high_tile[:2 * PAIR]
+            dvx[h, 3 * PAIR:] = high_tile[2 * PAIR:]
             lanes = slice(h * HEAD_DIM, (h + 1) * HEAD_DIM)
             to_before[0, h] = (dkx[h, :BEFORE] * FACTOR).astype(BF16)
             to_before[1, h] = dvx[h, :BEFORE].astype(BF16)
@@ -415,8 +464,6 @@
 
     @pl.when(tp == 1)
     def _():
-        if nz > 9:
-            pl.semaphore_wait(round3, len(near(nz, 3)))
         for o in far_first(nx):
             remote(lines.at[mine], lines.at[mine], xy_send, x_recv, along(2, o)).start()
         stage_results()
@@ -433,6 +480,8 @@
             zout[core, :3] = part[3 * core:3 * core + 3]
             zout[core, 3:] = part[6:]
         zbuf[z] = zout[1]
+        if nz > 9:
+            pl.semaphore_wait(round3, len(near(nz, 3)))
         for o in [*far_first(nz), 0]:
             for core in range(2 if o else 1):
                 remote(zout.at[core], zbuf.at[z], z_send, z_recv, along(0, o, core)).start()
@@ -527,11 +576,12 @@
             vmem(tile, BF16), vmem(tile, F32), vmem(tile, F32),
             vmem(wide, BF16), vmem(wide, F32), vmem(tile, F32),
             vmem(pairs, F32), vmem(pairs, F32), vmem(pairs, F32),
-            vmem(wide, F32), vmem(wide, F32), vmem(tile, F32), vmem((HEADS, 3 * PAIR, PAIR), F32), vmem((2, HEAD_DIM), F32),
+            vmem(wide, F32), vmem(wide, F32), vmem(tile, F32), vmem((HEADS, 3 * PAIR, PAIR), F32),
+            vmem(pairs, BF16), vmem((HEADS, 2, 6, 1, PAIR), F32), vmem((HEADS, 2, 2, 1, PAIR), F32), vmem((HEADS, 2, 1, PAIR), F32), vmem((2, HEAD_DIM), F32),
             vmem((2, HEADS, BEFORE, HEAD_DIM), BF16), vmem((2, HEADS, BEFORE, HEAD_DIM), BF16),
             vmem((2, *first), BF16), vmem((2, *first), BF16), vmem((SEG, width), BF16), vmem((SEG, width), BF16),
             vmem((2 * nx + ny, 8, HEAD_DIM), F32), vmem((2, 5, HEAD_DIM), F32), vmem((2 * nz, 5, HEAD_DIM), F32),
-            dma((2,)), dma, dma, dma((2,)), dma((4,)), dma((HEADS,)), dma((2,)), dma((HEADS,)), dma,
+            dma((2,)), dma, dma, dma((2,)), dma((HEADS + 1,)), dma((HEADS,)), dma((2,)), dma((HEADS,)), dma,
             dma, dma, dma, dma, dma, regular, regular, regular, regular,
         ],
         compiler_params=pltpu.CompilerParams(

time: 40.2 us -> 38.6 us (0.960)
  Pallas kernels: 39.3 us -> 37.8 us
    pallas_call x1, Pallas kernels: 38.6 us -> 37 us  [local(): pl.pallas_call(functools.partial(kernel, sizes), out_shape=tuple((vmem(*o...]
where the time goes in v5:
time: 38.6 us; the launch traced here: 38.4 us
  Pallas kernels  37.8 us (98%)
  between operations  0.64 us (2%)
    pallas_call x1, Pallas kernels, local(): pl.pallas_call(functools.partial(kernel, sizes), out_shape=tuple((vmem(*o...  37 us
    pallas_call x1, Pallas kernels, local(): pl.pallas_call(write_out, out_shape=tuple((jax.ShapeDtypeStruct(*o) for o...  0.79 us

profile of v5, /device:TPU:1, one launch (start us, length us, event | category | flops | bytes accessed | tf_op | source)
XLA Modules:
  0.0 38.4 jit_solution(7940589451886563071)
XLA Ops:
  0.6 37.0 %segment_attention_grad.1 = (bf16[256,256]{1,0:T(8,128)(2,1)S(1)}, bf16[256,256]{1,0:T(8,128)(2,1)S(1)}, bf16[256,256]{1,0:T(8,128)(2,1)S(1)}, f32[2,192]{1,0:T(2,128)S(1)}, f32[2,128]{1,0:T(2,128)S(1)}) custom-call(bf16[256,256]{1,0:T(8,128)(2,1)} %q_hbm.1, bf16[256,256]{1,0:T(8,128)(2,1)} %k_hbm.1, bf16[256,256]{1,0:T(8,128)(2,1)} %v_hbm.1, ...), custom_call_target="tpu_custom_call" | custom-call | tf_op jit(solution)/shard_map/segment_attention_grad/pallas_call | solution.py:568
  37.6 0.8 %write_out.1 = (bf16[256,256]{1,0:T(8,128)(2,1)}, bf16[256,256]{1,0:T(8,128)(2,1)}, bf16[256,256]{1,0:T(8,128)(2,1)}, f32[2,192]{1,0:T(2,128)}, f32[2,128]{1,0:T(2,128)}) custom-call(bf16[256,256]{1,0:T(8,128)(2,1)S(1)} %get-tuple-element.15.refs_0_, bf16[256,256]{1,0:T(8,128)(2,1)S(1)} %get-tuple-element.16.refs_1_, ...), custom_call_target="tpu_custom_call" | custom-call | tf_op jit(solution)/shard_map/write_out/pallas_call | solution.py:591

commit v6 on v5

--- a/solution.py
+++ b/solution.py
@@ -48,18 +48,21 @@
 
 def kernel(sizes, q_hbm, k_hbm, v_hbm, do_hbm, gains_hbm, table_hbm,
            dq_v, dk_v, dv_v, dtab_v, dgain_v,
-           qdx, qd0, kvx, gains_v, table_v,
-           qn, qu, qr, kn, ku, kr, bias_v, e_v, dp_v,
-           dkx, dvx, dqx, d_v, prob_v, sum_v, gain_v, table_v2, extra_gains,
-           to_before, from_after, to_after, from_before, dq_to_after, dq_from_before,
+           q_raw, k_raw, qdx, qd0, kvx, first_kv, gains_v, table_v,
+           qu, qr, ku, kr, bias_v, e_v, dp_v,
+           dkx, dvx, dqx, d_v, prob_v, d_low_v, sum_v, gain_v, table_v2, extra_gain, extra_dv,
+           to_before, from_after, to_after, from_before, dq_from_before, to_before_first, from_after_first,
            lines, zout, zbuf,
-           load_sem, gains_sem, table_sem, halo_send, left_recv, right_recv, back_send, after_recv, before_recv,
+           load_sem, gains_sem, table_sem, halo_send, left_recv, right_recv, back_send, after_recv, before_recv, first_recv,
            xy_send, x_recv, y_recv, z_send, z_recv, round1, round2, round3, row_sem):
     nz, ny, nx = sizes
     z, y, x, tp = (lax.axis_index(a) for a in AXES)
     place = (z * ny + y) * nx + x
     total = nz * ny * nx
     is_first, is_last = place == 0, place == total - 1
+    opens, closes = jnp.logical_and(x == 0, y == 0), jnp.logical_and(x == nx - 1, y == ny - 1)
+    opens_later, closes_early = jnp.logical_and(opens, place > 0), jnp.logical_and(closes, place < total - 1)
+    takes_back, takes_next = jnp.logical_not(opens), jnp.logical_not(closes)
 
     def at(number, core):
         return (number // (ny * nx), (number // nx) % ny, number % nx, core)
@@ -96,17 +99,16 @@
         signal(barrier, after)
 
     sides = jnp.where(is_first, 0, 1) + jnp.where(is_last, 0, 1)
-    for n, (src, dst) in enumerate(((k_hbm, kvx.at[0]), (v_hbm, kvx.at[1]), (q_hbm, qdx.at[0]), (do_hbm, qdx.at[1]))):
-        for h in range(HEADS):
-            lanes = slice(h * HEAD_DIM, (h + 1) * HEAD_DIM)
-            if n < 2:
-                pltpu.make_async_copy(src.at[:, lanes], dst.at[h, BEFORE:BEFORE + ROWS], load_sem.at[0]).start()
-            else:
-                pltpu.make_async_copy(src.at[:SEG, lanes], qd0.at[n - 2, h], load_sem.at[0]).start()
-                pltpu.make_async_copy(src.at[SEG:, lanes], dst.at[h, :BEFORE], load_sem.at[1]).start()
     small_loads = [pltpu.make_async_copy(gains_hbm, gains_v, gains_sem), pltpu.make_async_copy(table_hbm, table_v, table_sem)]
     for load in small_loads:
         load.start()
+    for h in range(HEADS):
+        lanes = slice(h * HEAD_DIM, (h + 1) * HEAD_DIM)
+        pltpu.make_async_copy(k_hbm.at[:, lanes], k_raw.at[h], load_sem.at[0]).start()
+        pltpu.make_async_copy(q_hbm.at[:, lanes], q_raw.at[h], load_sem.at[0]).start()
+        pltpu.make_async_copy(v_hbm.at[:, lanes], kvx.at[1, h, BEFORE:BEFORE + ROWS], load_sem.at[0]).start()
+        pltpu.make_async_copy(do_hbm.at[:SEG, lanes], qd0.at[1, h], load_sem.at[0]).start()
+        pltpu.make_async_copy(do_hbm.at[SEG:, lanes], qdx.at[1, h, :BEFORE], load_sem.at[1]).start()
 
     close = [(a, o) for a, n in enumerate(sizes) for o in near(n)]
 
@@ -115,14 +117,30 @@
         for a, o in close:
             signal(barrier, along(a, o))
         signal(barrier, (z, y, x, 0))
-        pl.semaphore_wait(barrier, 1 + len(close) + sides)
 
     @pl.when(tp == 0)
     def _():
         signal(barrier, (z, y, x, 1))
-        pl.semaphore_wait(barrier, 1 + sides)
-
-    wait_bytes(kvx.at[:, :, :ROWS + SEG], load_sem.at[0])
+
+    for load in small_loads:
+        load.wait()
+    gains = gains_v[...]
+    gain_q, gain_k = gains[0:1, :], gains[1:2, :]
+    wait_bytes(kvx.at[:, :, :ROWS + PAIR + SEG // 2], load_sem.at[0])
+    def norm_keys(first, size):
+        for h in range(HEADS):
+            u, r = unit(k_raw[h, first:first + size])
+            ku[h, first:first + size] = u
+            kr[h, first:first + size] = jnp.broadcast_to(r, u.shape)
+            kvx[0, h, BEFORE + first:BEFORE + first + size] = (u * gain_k).astype(BF16)
+
+    def norm_queries(first, size, out):
+        for h in range(HEADS):
+            u, r = unit(q_raw[h, first:first + size])
+            qu[h, first:first + size] = u
+            qr[h, first:first + size] = jnp.broadcast_to(r, u.shape)
+            out[h] = (u * gain_q).astype(BF16)
+
     forth = [remote(
         kvx.at[:, :, ROWS + PAIR:ROWS + BEFORE], kvx.at[:, :, PAIR:BEFORE], halo_send.at[0], left_recv.at[HEADS], after)]
     back = {}
@@ -133,62 +151,57 @@
             remote(kvx.at[:, h, BEFORE:ROWS], kvx.at[:, h, BEFORE + ROWS:], halo_send.at[1], right_recv.at[h], before),
             remote(qd0.at[:, h], qdx.at[:, h, BEFORE:], halo_send.at[1], right_recv.at[h], before)]
 
-    @pl.when(place < total - 1)
-    def _():
-        for copy in forth:
-            copy.start()
-
-    @pl.when(place > 0)
-    def _():
-        for copies in back.values():
-            for copy in copies:
+    plane_piece = remote(kvx.at[:, :, BEFORE:ROWS], first_kv, halo_send.at[0], left_recv.at[HEADS + 1], after)
+
+    def go_on(pieces, when=place < total - 1):
+        @pl.when(when)
+        def _():
+            for copy in pieces:
                 copy.start()
+
+    norm_keys(BEFORE, SEG)
+    pl.semaphore_wait(barrier, sides + jnp.where(tp == 1, 1 + len(close), 1))
+    go_on(forth[:1])
+    norm_keys(0, SEG)
+    norm_queries(0, SEG, qd0.at[0])
+
+    go_on([copy for h in range(HEADS) for copy in back[h]], takes_back)
+    norm_keys(SEG, PAIR)
+    go_on(forth[1:])
+    go_on([plane_piece], closes_early)
+    norm_queries(SEG, BEFORE, qdx.at[0, :, :BEFORE])
 
     @pl.when(tp == 1)
     def _():
         for a, o in close:
             signal(round1, along(a, o))
 
-    wait_bytes(qdx.at[:, :, :BEFORE], load_sem.at[1])
-    for load in small_loads:
-        load.wait()
+    wait_bytes(qdx.at[1, :, :BEFORE], load_sem.at[1])
 
     @pl.when(is_first)
     def _():
         for h in range(HEADS):
             for n in range(2):
                 kvx[n, h, :BEFORE] = kvx[n, h, BEFORE:2 * BEFORE]
-                from_before[n, h] = jnp.zeros((SEG, HEAD_DIM), BF16)
-        extra_gains[...] = jnp.zeros((2, HEAD_DIM), F32)
-
-    @pl.when(is_last)
+                first_kv[n, h] = kvx[n, h, BEFORE:ROWS]
+
+    @pl.when(opens)
+    def _():
+        extra_gain[...] = jnp.zeros((1, HEAD_DIM), F32)
+
+    @pl.when(closes)
     def _():
         for h in range(HEADS):
             for n in range(2):
                 kvx[n, h, BEFORE + ROWS:] = kvx[n, h, BEFORE:ROWS]
-                from_after[n, h] = jnp.zeros((BEFORE, HEAD_DIM), BF16)
             qdx[0, h, BEFORE:] = qd0[0, h]
             qdx[1, h, BEFORE:] = jnp.zeros((SEG, HEAD_DIM), BF16)
 
-    gains = gains_v[...]
-    gain_q, gain_k = gains[0:1, :], gains[1:2, :]
-
-    def norm_keys(h, first, size):
-        u, r = unit(kvx[0, h, first:first + size])
-        ku[h, first:first + size] = u
-        kn[h, first:first + size] = (u * gain_k).astype(BF16)
-        if size == ROWS:
-            kr[h] = jnp.broadcast_to(r, u.shape)
-
-    def norm_queries(h, first, size):
-        u, r = unit(qdx[0, h, first:first + size])
-        qu[h, first:first + size] = u
-        qr[h, first:first + size] = jnp.broadcast_to(r, u.shape)
-        qn[h, first:first + size] = (u * gain_q).astype(BF16)
-
-    for h in range(HEADS):
-        norm_queries(h, 0, BEFORE)
-        norm_keys(h, BEFORE, ROWS)
+    @pl.when(is_last)
+    def _():
+        for h in range(HEADS):
+            for n in range(2):
+                from_after[n, h] = jnp.zeros((BEFORE, HEAD_DIM), BF16)
 
     key_at = lax.broadcasted_iota(jnp.int32, (PAIR, PAIR), 0)
     query_at = lax.broadcasted_iota(jnp.int32, (PAIR, PAIR), 1)
@@ -221,7 +234,7 @@
     def block(h, p, b):
         first = (p + b) * PAIR
         own = slice(p * PAIR, (p + 1) * PAIR)
-        s = dot(kn[h, first:first + PAIR], qn[h, own], 1, 1)
+        s = dot(kvx[0, h, first:first + PAIR], qdx[0, h, own], 1, 1)
         e = jnp.exp2(s * (FACTOR * LOG2E) + bias_v[h, p, b * PAIR:(b + 1) * PAIR])
         dp = dot(kvx[1, h, first:first + PAIR], qdx[1, h, own], 1, 1)
         e_v[h, p, b * PAIR:(b + 1) * PAIR] = e
@@ -239,11 +252,9 @@
         prob_low = prob.astype(BF16)
         d_low = d_score.astype(BF16)
         prob_v[h, p] = prob_low
-        dk = dot(d_low, qn[h, own], 1, 0)
-        dq = dot(d_low, kn[h, keys], 0, 0)
-        dqx[h, own] = dq
-        gain_v[h, p, 0] = jnp.sum(dq * qu[h, own], axis=0, keepdims=True)
-        gain_v[h, p, 1] = jnp.sum(dk * ku[h, keys], axis=0, keepdims=True)
+        d_low_v[h, p] = d_low
+        dk = dot(d_low, qdx[0, h, own], 1, 0)
+        gain_v[h, p] = jnp.sum(dk * kvx[0, h, keys].astype(F32), axis=0, keepdims=True)
         if again:
             shared, alone = slice(PAIR, 3 * PAIR), slice(3 * p * PAIR, (3 * p + 1) * PAIR)
             ours = slice((1 - p) * PAIR, (3 - p) * PAIR)
@@ -258,29 +269,6 @@
         g = g * FACTOR * gain_q
         return (r * (g - u * jnp.mean(g * u, axis=-1, keepdims=True))).astype(BF16)
 
-    def first_segment(h):
-        u, r = unit(qd0[0, h])
-        queries = (u * gain_q).astype(BF16)
-        keys = kn[h, BEFORE:ROWS]
-        bias = bias_v[h, 0, 2 * PAIR:2 * PAIR + SEG][:, :SEG]
-        bias = bias - jnp.max(bias, axis=0, keepdims=True)
-        e = jnp.exp2(dot(keys, queries, 1, 1) * (FACTOR * LOG2E) + bias)
-        dp = dot(kvx[1, h, BEFORE:ROWS], qd0[1, h], 1, 1)
-        inv = 1.0 / jnp.sum(e, axis=0, keepdims=True)
-        delta = jnp.sum(e * dp, axis=0, keepdims=True) * inv
-        prob = e * inv
-        d_score = prob * (dp - delta)
-        d_low = d_score.astype(BF16)
-        dk = dot(d_low, queries, 1, 0)
-        dq = dot(d_low, keys, 0, 0)
-        from_before[0, h] = (dk * FACTOR).astype(BF16)
-        from_before[1, h] = dot(prob.astype(BF16), qd0[1, h], 1, 0).astype(BF16)
-        dq_from_before[:, h * HEAD_DIM:(h + 1) * HEAD_DIM] = query_rows(dq, u, r)
-        at_tile = slice(2 * PAIR, 2 * PAIR + SEG)
-        d_v[h, at_tile] = d_v[h, at_tile] + jnp.concatenate([d_score, jnp.zeros((SEG, SEG), F32)], axis=1)
-        extra_gains[0:1] = extra_gains[0:1] + jnp.sum(dq * u, axis=0, keepdims=True)
-        extra_gains[1:2] = extra_gains[1:2] + jnp.sum(dk * ku[h, BEFORE:ROWS], axis=0, keepdims=True)
-
     sublane = lax.broadcasted_iota(jnp.int32, (8, PAIR), 0)
 
     def skewed_sum(tile, right):
@@ -292,7 +280,7 @@
             total = jnp.where(sublane == bit, pltpu.roll(parts[0], PAIR - bit, 1), total)
         return jnp.sum(total, axis=0, keepdims=True)
 
-    def fold_table(h, d_score):
+    def fold_rows(h, d_score):
         d0, d1, d2 = (d_score[b * PAIR:(b + 1) * PAIR] for b in range(3))
         mixed = jnp.where(past, d2, d1)
         ahead = jnp.where(past, 0.0, d2)
@@ -300,8 +288,43 @@
         behind_row, ahead_row = skewed_sum(mixed, SEG - 1), skewed_sum(ahead, SEG - 1)
         high_row = skewed_sum(mixed, SEG - 1 + SEG) if h else behind_row
         rest_sum = jnp.sum(jnp.sum(rest, axis=0, keepdims=True), axis=1, keepdims=True)
-        table_v2[h, 0] = jnp.where(lane < SEG - 1, ahead_row, behind_row)
-        table_v2[h, 1] = jnp.where(lane == SEG - 1 + h * SEG, rest_sum, high_row)
+        return (
+            jnp.where(lane < SEG - 1, ahead_row, behind_row),
+            jnp.where(lane == SEG - 1 + h * SEG, rest_sum, high_row))
+
+    def fold_table(h, d_score):
+        table_v2[h, 0], table_v2[h, 1] = fold_rows(h, d_score)
+
+    def first_segment(h):
+        queries, cotangents = qd0[0, h], qd0[1, h]
+        keys, rest = first_kv[0, h], kvx[0, h, :ROWS]
+        key_number = lax.broadcasted_iota(jnp.int32, (ROWS + SEG, SEG), 0)
+        bias = bias_v[h, 0, :ROWS + SEG][:, :SEG]
+        bias = jnp.where(jnp.logical_and(is_first, key_number < ROWS), MASKED, bias)
+        bias = bias - jnp.max(bias, axis=0, keepdims=True)
+        s = jnp.concatenate([dot(keys, queries, 1, 1), dot(rest, queries, 1, 1)], axis=0)
+        e = jnp.exp2(s * (FACTOR * LOG2E) + bias)
+        dp = jnp.concatenate([dot(first_kv[1, h], cotangents, 1, 1), dot(kvx[1, h, :ROWS], cotangents, 1, 1)], axis=0)
+        inv = 1.0 / jnp.sum(e, axis=0, keepdims=True)
+        delta = jnp.sum(e * dp, axis=0, keepdims=True) * inv
+        prob = e * inv
+        d_score = prob * (dp - delta)
+        d_low = d_score.astype(BF16)
+        dk = dot(d_low, queries, 1, 0)
+        dv = dot(prob.astype(BF16), cotangents, 1, 0)
+        dq_from_before[h] = dot(d_low[:SEG], keys, 0, 0) + dot(d_low[SEG:], rest, 0, 0)
+        for n, part in enumerate((dk * FACTOR, dv)):
+            to_before_first[n, h] = part[:SEG].astype(BF16)
+            from_before[n, h] = part[ROWS:].astype(BF16)
+        dkx[h, :BEFORE] = dkx[h, :BEFORE] + dk[SEG:ROWS]
+        extra_dv[h] = dv[SEG:ROWS]
+        extra_gain[...] = extra_gain[...] + (
+            jnp.sum(dk[:SEG] * keys.astype(F32), axis=0, keepdims=True)
+            + jnp.sum(dk[SEG:] * rest.astype(F32), axis=0, keepdims=True))
+        tile = jnp.concatenate([d_score, jnp.zeros((ROWS + SEG, SEG), F32)], axis=1)
+        rows = fold_rows(h, jnp.concatenate([tile, jnp.zeros((SEG, PAIR), F32)], axis=0))
+        for j in range(2):
+            table_v2[h, j] = table_v2[h, j] + rows[j]
 
     for h in range(HEADS):
         block(h, 0, 2)
@@ -321,7 +344,7 @@
             forth[piece].wait_recv()
 
     def wait_right(h):
-        @pl.when(place < total - 1)
+        @pl.when(takes_next)
         def _():
             wait_bytes(kvx.at[:, h, :PAIR], right_recv.at[h])
 
@@ -335,42 +358,34 @@
                 for o in near(nz, 3):
                     signal(round3, along(0, o))
 
-    def do_first(h):
-        @pl.when(is_first)
-        def _():
-            first_segment(h)
-
-    def from_left_near(h):
-        norm_keys(h, PAIR, SEG)
-        block(h, 0, 1)
-
-    def from_left_far(h):
-        norm_keys(h, 0, PAIR)
-        block(h, 0, 0)
-
-    def from_right(h):
-        norm_keys(h, BEFORE + ROWS, SEG)
-        norm_queries(h, BEFORE, SEG)
-        block(h, 1, 1)
-        block(h, 1, 2)
+    def do_first():
+        @pl.when(opens)
+        def _():
+            @pl.when(place > 0)
+            def _():
+                plane_piece.wait_recv()
+
+            for h in range(HEADS):
+                first_segment(h)
 
     @pl.when(x == nx - 1)
     def _():
         wait_left(0)
         for h in range(HEADS):
-            from_left_near(h)
+            block(h, 0, 1)
         for h in range(HEADS):
             wait_left(1 + h)
-            from_left_far(h)
+            block(h, 0, 0)
             finish(h, 0, False)
-            if nx == 1:
-                do_first(h)
         greet_far()
         for h in range(HEADS):
             wait_right(h)
-            from_right(h)
+            block(h, 1, 1)
+            block(h, 1, 2)
             block(h, 1, 0)
             fold_table(h, finish(h, 1, True))
+        if nx == 1:
+            do_first()
 
     if nx > 1:
         @pl.when(x == 0)
@@ -378,35 +393,36 @@
             for h in range(HEADS):
                 wait_right(h)
             for h in range(HEADS):
-                from_right(h)
+                block(h, 1, 1)
+                block(h, 1, 2)
             wait_left(0)
             for h in range(HEADS):
-                from_left_near(h)
+                block(h, 0, 1)
                 block(h, 1, 0)
                 finish(h, 1, False)
-            for h in range(HEADS):
-                do_first(h)
             greet_far()
             for h in range(HEADS):
                 wait_left(1 + h)
-                from_left_far(h)
+                block(h, 0, 0)
                 fold_table(h, finish(h, 0, True))
+            do_first()
 
     if nx > 2:
         @pl.when(jnp.logical_and(x > 0, x < nx - 1))
         def _():
             wait_left(0)
             for h in range(HEADS):
-                from_left_near(h)
+                block(h, 0, 1)
             for h in range(HEADS):
                 wait_right(h)
-                from_right(h)
+                block(h, 1, 1)
+                block(h, 1, 2)
                 block(h, 1, 0)
                 finish(h, 1, False)
                 if h:
                     greet_far()
                 wait_left(1 + h)
-                from_left_far(h)
+                block(h, 0, 0)
                 fold_table(h, finish(h, 0, True))
 
     row = lax.broadcasted_iota(jnp.int32, (8, HEAD_DIM), 0)
@@ -414,18 +430,17 @@
     second = jnp.where(lane < SEG, table_v2[0, 1], table_v2[1, 1])
     for j, part in enumerate((table_v2[0, 0], table_v2[1, 0], second)):
         vec = jnp.where(row == 3 * tp + j, part, vec)
-    for j in range(2):
-        part = gain_v[0, 0, j] + gain_v[0, 1, j] + gain_v[1, 0, j] + gain_v[1, 1, j]
-        part = part + jnp.where(is_first, extra_gains[j:j + 1], 0.0)
-        vec = jnp.where(row == 6 + j, part * FACTOR, vec)
+    part = gain_v[0, 0] + gain_v[0, 1] + gain_v[1, 0] + gain_v[1, 1] + jnp.where(opens, extra_gain[...], 0.0)
+    vec = jnp.where(row == 6, part * FACTOR, vec)
     mine = 2 * x + tp
-    lines[mine] = vec
+    lines[mine] = vec[:7]
 
     to_neighbours = [
         remote(to_before.at[:, h], from_after.at[:, h], back_send.at[0], after_recv.at[h], before) for h in range(HEADS)]
     to_next = [
         remote(to_after, from_before, back_send.at[1], before_recv, after),
-        remote(dq_to_after, dq_from_before, back_send.at[1], before_recv, after)]
+        remote(dqx.at[:, BEFORE:], dq_from_before, back_send.at[1], before_recv, after)]
+    to_plane_before = remote(to_before_first, from_after_first, back_send.at[0], first_recv, before)
 
     def stage_results():
         for h in range(HEADS):
@@ -433,14 +448,19 @@
             dvx[h, :PAIR] = low[:PAIR]
             dvx[h, PAIR:3 * PAIR] = low[PAIR:] + high_tile[:2 * PAIR]
             dvx[h, 3 * PAIR:] = high_tile[2 * PAIR:]
+
+            @pl.when(opens)
+            def _(h=h):
+                dvx[h, :BEFORE] = dvx[h, :BEFORE] + extra_dv[h]
+
             lanes = slice(h * HEAD_DIM, (h + 1) * HEAD_DIM)
             to_before[0, h] = (dkx[h, :BEFORE] * FACTOR).astype(BF16)
             to_before[1, h] = dvx[h, :BEFORE].astype(BF16)
             to_after[0, h] = (dkx[h, BEFORE + ROWS:] * FACTOR).astype(BF16)
             to_after[1, h] = dvx[h, BEFORE + ROWS:].astype(BF16)
-            rows = query_rows(dqx[h], qu[h], qr[h])
-            dq_v[SEG:, lanes] = rows[:BEFORE]
-            dq_to_after[:, lanes] = rows[BEFORE:]
+            for p in range(2):
+                dqx[h, p * PAIR:(p + 1) * PAIR] = dot(d_low_v[h, p], kvx[0, h, p * PAIR:(p + 3) * PAIR], 0, 0)
+            dq_v[SEG:, lanes] = query_rows(dqx[h, :BEFORE], qu[h, SEG:], qr[h, SEG:])
 
     def send_results(when):
         @pl.when(jnp.logical_and(when, place > 0))
@@ -448,7 +468,11 @@
             for copy in to_neighbours:
                 copy.start()
 
-        @pl.when(jnp.logical_and(when, place < total - 1))
+        @pl.when(jnp.logical_and(when, opens_later))
+        def _():
+            to_plane_before.start()
+
+        @pl.when(jnp.logical_and(when, takes_next))
         def _():
             for copy in to_next:
                 copy.start()
@@ -494,11 +518,17 @@
         stage_results()
         send_results(place >= 0)
 
-    @pl.when(place > 0)
-    def _():
-        wait_bytes(from_after.at[:, 0], before_recv)
-
-    dq_v[:SEG] = dq_from_before[...]
+    @pl.when(takes_back)
+    def _():
+        wait_bytes(kvx.at[:, :, :PAIR], before_recv)
+
+    @pl.when(closes_early)
+    def _():
+        to_plane_before.wait_recv()
+
+    for h in range(HEADS):
+        dq_v[:SEG, h * HEAD_DIM:(h + 1) * HEAD_DIM] = query_rows(dq_from_before[h], qu[h, :SEG], qr[h, :SEG])
+
     for h in range(HEADS):
         @pl.when(place < total - 1)
         def _(h=h):
@@ -506,21 +536,31 @@
 
         lanes = slice(h * HEAD_DIM, (h + 1) * HEAD_DIM)
         sums_in = [
-            jnp.concatenate([from_before[n, h].astype(F32), from_after[n, h].astype(F32)], axis=0) for n in range(2)]
+            jnp.concatenate([
+                jnp.where(takes_next, 0.0, jnp.where(is_last, 0.0, from_after_first[n, h].astype(F32)))
+                + from_before[n, h].astype(F32), from_after[n, h].astype(F32)], axis=0) for n in range(2)]
         g = (dkx[h, BEFORE:BEFORE + ROWS] * FACTOR + sums_in[0]) * gain_k
-        u = ku[h, BEFORE:BEFORE + ROWS]
+        u = ku[h]
         dk_v[:, lanes] = (kr[h] * (g - u * jnp.mean(g * u, axis=-1, keepdims=True))).astype(BF16)
         dv_v[:, lanes] = (dvx[h, BEFORE:BEFORE + ROWS] + sums_in[1]).astype(BF16)
 
-    @pl.when(place < total - 1)
+    @pl.when(takes_next)
     def _():
         wait_bytes(kvx.at[:, :, :BEFORE], halo_send.at[0])
-        wait_bytes(from_after.at[:, 0], back_send.at[1])
-
-    @pl.when(place > 0)
+        wait_bytes(kvx.at[:, :, :PAIR], back_send.at[1])
+
+    @pl.when(closes_early)
+    def _():
+        wait_bytes(kvx.at[:, :, :ROWS], halo_send.at[0])
+
+    @pl.when(takes_back)
     def _():
         wait_bytes(kvx.at[:, :, :PAIR], halo_send.at[1])
         wait_bytes(from_after, back_send.at[0])
+
+    @pl.when(opens_later)
+    def _():
+        wait_bytes(kvx.at[:, :, :ROWS], back_send.at[0])
 
     @pl.when(tp == 1)
     def _():
@@ -541,7 +581,8 @@
     for j in range(HEADS):
         dtab_v[j:j + 1, :PAIR] = result[j:j + 1]
         dtab_v[j:j + 1, PAIR:] = result[2:3, j * SEG:(j + 1) * SEG]
-    dgain_v[...] = result[3:]
+    dgain_v[0:1] = result[3:] / gain_q
+    dgain_v[1:2] = result[3:] / gain_k
 
 
 def write_out(*refs):
@@ -571,17 +612,17 @@
         in_specs=[hbm_spec] * 6,
         out_specs=(vmem_spec,) * 5,
         scratch_shapes=[
-            vmem((2, *tile), BF16), vmem((2, *first), BF16), vmem((2, *wide), BF16),
+            vmem(tile, BF16), vmem(tile, BF16), vmem((2, *tile), BF16), vmem((2, *first), BF16), vmem((2, *wide), BF16), vmem((2, *first), BF16),
             vmem((2, HEAD_DIM), F32), vmem((HEADS, ENTRIES), F32),
-            vmem(tile, BF16), vmem(tile, F32), vmem(tile, F32),
-            vmem(wide, BF16), vmem(wide, F32), vmem(tile, F32),
+            vmem(tile, F32), vmem(tile, F32), vmem(tile, F32), vmem(tile, F32),
             vmem(pairs, F32), vmem(pairs, F32), vmem(pairs, F32),
             vmem(wide, F32), vmem(wide, F32), vmem(tile, F32), vmem((HEADS, 3 * PAIR, PAIR), F32),
-            vmem(pairs, BF16), vmem((HEADS, 2, 6, 1, PAIR), F32), vmem((HEADS, 2, 2, 1, PAIR), F32), vmem((HEADS, 2, 1, PAIR), F32), vmem((2, HEAD_DIM), F32),
+            vmem(pairs, BF16), vmem(pairs, BF16), vmem((HEADS, 2, 6, 1, PAIR), F32), vmem((HEADS, 2, 1, PAIR), F32),
+            vmem((HEADS, 2, 1, PAIR), F32), vmem((1, HEAD_DIM), F32), vmem((HEADS, BEFORE, HEAD_DIM), F32),
             vmem((2, HEADS, BEFORE, HEAD_DIM), BF16), vmem((2, HEADS, BEFORE, HEAD_DIM), BF16),
-            vmem((2, *first), BF16), vmem((2, *first), BF16), vmem((SEG, width), BF16), vmem((SEG, width), BF16),
-            vmem((2 * nx + ny, 8, HEAD_DIM), F32), vmem((2, 5, HEAD_DIM), F32), vmem((2 * nz, 5, HEAD_DIM), F32),
-            dma((2,)), dma, dma, dma((2,)), dma((HEADS + 1,)), dma((HEADS,)), dma((2,)), dma((HEADS,)), dma,
+            vmem((2, *first), BF16), vmem((2, *first), BF16), vmem(first, F32), vmem((2, *first), BF16), vmem((2, *first), BF16),
+            vmem((2 * nx + ny, 7, HEAD_DIM), F32), vmem((2, 4, HEAD_DIM), F32), vmem((2 * nz, 4, HEAD_DIM), F32),
+            dma((2,)), dma, dma, dma((2,)), dma((HEADS + 2,)), dma((HEADS,)), dma((2,)), dma((HEADS,)), dma, dma,
             dma, dma, dma, dma, dma, regular, regular, regular, regular,
         ],
         compiler_params=pltpu.CompilerParams(

time: 38.6 us -> 37.8 us (0.979)
  Pallas kernels: 37.8 us -> 37 us
    pallas_call x1, Pallas kernels: 37 us -> 36.2 us  [local(): pl.pallas_call(functools.partial(kernel, sizes), out_shape=tuple((vmem(*o...]
where the time goes in v6:
time: 37.8 us; the launch traced here: 37.6 us
  Pallas kernels  37 us (98%)
  between operations  0.64 us (2%)
    pallas_call x1, Pallas kernels, local(): pl.pallas_call(functools.partial(kernel, sizes), out_shape=tuple((vmem(*o...  36.2 us
    pallas_call x1, Pallas kernels, local(): pl.pallas_call(write_out, out_shape=tuple((jax.ShapeDtypeStruct(*o) for o...  0.79 us

profile of v6, /device:TPU:1, one launch (start us, length us, event | category | flops | bytes accessed | tf_op | source)
XLA Modules:
  0.0 37.6 jit_solution(6475981245897170708)
XLA Ops:
  0.6 36.2 %segment_attention_grad.1 = (bf16[256,256]{1,0:T(8,128)(2,1)S(1)}, bf16[256,256]{1,0:T(8,128)(2,1)S(1)}, bf16[256,256]{1,0:T(8,128)(2,1)S(1)}, f32[2,192]{1,0:T(2,128)S(1)}, f32[2,128]{1,0:T(2,128)S(1)}) custom-call(bf16[256,256]{1,0:T(8,128)(2,1)} %q_hbm.1, bf16[256,256]{1,0:T(8,128)(2,1)} %k_hbm.1, bf16[256,256]{1,0:T(8,128)(2,1)} %v_hbm.1, ...), custom_call_target="tpu_custom_call" | custom-call | tf_op jit(solution)/shard_map/segment_attention_grad/pallas_call | solution.py:609
  36.8 0.8 %write_out.1 = (bf16[256,256]{1,0:T(8,128)(2,1)}, bf16[256,256]{1,0:T(8,128)(2,1)}, bf16[256,256]{1,0:T(8,128)(2,1)}, f32[2,192]{1,0:T(2,128)}, f32[2,128]{1,0:T(2,128)}) custom-call(bf16[256,256]{1,0:T(8,128)(2,1)S(1)} %get-tuple-element.15.refs_0_, bf16[256,256]{1,0:T(8,128)(2,1)S(1)} %get-tuple-element.16.refs_1_, ...), custom_call_target="tpu_custom_call" | custom-call | tf_op jit(solution)/shard_map/write_out/pallas_call | solution.py:632

commit v7 on v6

--- a/solution.py
+++ b/solution.py
@@ -167,7 +167,8 @@
 
     go_on([copy for h in range(HEADS) for copy in back[h]], takes_back)
     norm_keys(SEG, PAIR)
-    go_on(forth[1:])
+    go_on(forth[1:], jnp.logical_and(tp == 0, place < total - 1))
+    go_on(forth[1:2], jnp.logical_and(tp == 1, place < total - 1))
     go_on([plane_piece], closes_early)
     norm_queries(SEG, BEFORE, qdx.at[0, :, :BEFORE])
 
@@ -231,39 +232,43 @@
             for b, tile in enumerate(tiles):
                 bias_v[h, p, b * PAIR:(b + 1) * PAIR] = (tile - top) * LOG2E
 
-    def block(h, p, b):
-        first = (p + b) * PAIR
-        own = slice(p * PAIR, (p + 1) * PAIR)
-        s = dot(kvx[0, h, first:first + PAIR], qdx[0, h, own], 1, 1)
-        e = jnp.exp2(s * (FACTOR * LOG2E) + bias_v[h, p, b * PAIR:(b + 1) * PAIR])
-        dp = dot(kvx[1, h, first:first + PAIR], qdx[1, h, own], 1, 1)
-        e_v[h, p, b * PAIR:(b + 1) * PAIR] = e
-        dp_v[h, p, b * PAIR:(b + 1) * PAIR] = dp
-        sum_v[h, p, b] = jnp.sum(e, axis=0, keepdims=True)
-        sum_v[h, p, 3 + b] = jnp.sum(e * dp, axis=0, keepdims=True)
-
-    def finish(h, p, again):
-        inv = 1.0 / (sum_v[h, p, 0] + sum_v[h, p, 1] + sum_v[h, p, 2])
-        delta = (sum_v[h, p, 3] + sum_v[h, p, 4] + sum_v[h, p, 5]) * inv
-        own = slice(p * PAIR, (p + 1) * PAIR)
-        keys = slice(p * PAIR, (p + 3) * PAIR)
-        prob = e_v[h, p] * inv
-        d_score = prob * (dp_v[h, p] - delta)
-        prob_low = prob.astype(BF16)
-        d_low = d_score.astype(BF16)
-        prob_v[h, p] = prob_low
-        d_low_v[h, p] = d_low
-        dk = dot(d_low, qdx[0, h, own], 1, 0)
-        gain_v[h, p] = jnp.sum(dk * kvx[0, h, keys].astype(F32), axis=0, keepdims=True)
-        if again:
-            shared, alone = slice(PAIR, 3 * PAIR), slice(3 * p * PAIR, (3 * p + 1) * PAIR)
-            ours = slice((1 - p) * PAIR, (3 - p) * PAIR)
-            rest = slice(2 * p * PAIR, (2 * p + 1) * PAIR)
-            dkx[h, alone] = dk[rest]
-            dkx[h, shared] = dkx[h, shared] + dk[ours]
-            return d_v[h] + d_score
-        dkx[h, keys] = dk
-        d_v[h] = d_score
+    def work(blocks, tiles=()):
+        at_keys = {(p, b): slice((p + b) * PAIR, (p + b + 1) * PAIR) for h, p, b in blocks}
+        at_queries = [slice(p * PAIR, (p + 1) * PAIR) for p in range(2)]
+        at_rows = [slice(b * PAIR, (b + 1) * PAIR) for b in range(3)]
+        scores = [dot(kvx[0, h, at_keys[p, b]], qdx[0, h, at_queries[p]], 1, 1) for h, p, b in blocks]
+        d_probs = [dot(kvx[1, h, at_keys[p, b]], qdx[1, h, at_queries[p]], 1, 1) for h, p, b in blocks]
+        for (h, p, b), s, dp in zip(blocks, scores, d_probs):
+            e = jnp.exp2(s * (FACTOR * LOG2E) + bias_v[h, p, at_rows[b]])
+            e_v[h, p, at_rows[b]] = e
+            dp_v[h, p, at_rows[b]] = dp
+            sum_v[h, p, b] = jnp.sum(e, axis=0, keepdims=True)
+            sum_v[h, p, 3 + b] = jnp.sum(e * dp, axis=0, keepdims=True)
+        d_scores, products = [], []
+        for h, p, _ in tiles:
+            inv = 1.0 / (sum_v[h, p, 0] + sum_v[h, p, 1] + sum_v[h, p, 2])
+            delta = (sum_v[h, p, 3] + sum_v[h, p, 4] + sum_v[h, p, 5]) * inv
+            prob = e_v[h, p] * inv
+            d_score = prob * (dp_v[h, p] - delta)
+            d_low = d_score.astype(BF16)
+            prob_v[h, p] = prob.astype(BF16)
+            d_low_v[h, p] = d_low
+            d_scores.append(d_score)
+            products.append(dot(d_low, qdx[0, h, at_queries[p]], 1, 0))
+        for (h, p, again), d_score in zip(tiles, d_scores):
+            if again:
+                fold_table(h, d_v[h] + d_score)
+            else:
+                d_v[h] = d_score
+        for (h, p, again), dk in zip(tiles, products):
+            keys = slice(p * PAIR, (p + 3) * PAIR)
+            gain_v[h, p] = jnp.sum(dk * kvx[0, h, keys].astype(F32), axis=0, keepdims=True)
+            if again:
+                shared, alone = slice(PAIR, 3 * PAIR), slice(3 * p * PAIR, (3 * p + 1) * PAIR)
+                dkx[h, alone] = dk[2 * p * PAIR:(2 * p + 1) * PAIR]
+                dkx[h, shared] = dkx[h, shared] + dk[(1 - p) * PAIR:(3 - p) * PAIR]
+            else:
+                dkx[h, keys] = dk
 
     def query_rows(g, u, r):
         g = g * FACTOR * gain_q
@@ -326,9 +331,10 @@
         for j in range(2):
             table_v2[h, j] = table_v2[h, j] + rows[j]
 
-    for h in range(HEADS):
-        block(h, 0, 2)
-
+    heads = range(HEADS)
+    work([(h, 0, 2) for h in heads])
+
+    go_on(forth[2:], jnp.logical_and(tp == 1, place < total - 1))
     @pl.when(tp == 1)
     def _():
         pl.semaphore_wait(round1, len(close))
@@ -371,59 +377,43 @@
     @pl.when(x == nx - 1)
     def _():
         wait_left(0)
-        for h in range(HEADS):
-            block(h, 0, 1)
-        for h in range(HEADS):
+        work([(h, 0, 1) for h in heads])
+        for h in heads:
             wait_left(1 + h)
-            block(h, 0, 0)
-            finish(h, 0, False)
+            work([(h, 0, 0)], [(h, 0, False)])
         greet_far()
-        for h in range(HEADS):
+        for h in heads:
             wait_right(h)
-            block(h, 1, 1)
-            block(h, 1, 2)
-            block(h, 1, 0)
-            fold_table(h, finish(h, 1, True))
+        work([(h, 1, b) for b in range(3) for h in heads], [(h, 1, True) for h in heads])
         if nx == 1:
             do_first()
 
     if nx > 1:
         @pl.when(x == 0)
         def _():
-            for h in range(HEADS):
+            for h in heads:
                 wait_right(h)
-            for h in range(HEADS):
-                block(h, 1, 1)
-                block(h, 1, 2)
+            work([(h, 1, b) for b in (1, 2) for h in heads])
             wait_left(0)
-            for h in range(HEADS):
-                block(h, 0, 1)
-                block(h, 1, 0)
-                finish(h, 1, False)
+            work([(h, p, 1 - p) for p in (1, 0) for h in heads], [(h, 1, False) for h in heads])
             greet_far()
-            for h in range(HEADS):
+            for h in heads:
                 wait_left(1 + h)
-                block(h, 0, 0)
-                fold_table(h, finish(h, 0, True))
+                work([(h, 0, 0)], [(h, 0, True)])
             do_first()
 
     if nx > 2:
         @pl.when(jnp.logical_and(x > 0, x < nx - 1))
         def _():
             wait_left(0)
-            for h in range(HEADS):
-                block(h, 0, 1)
-            for h in range(HEADS):
+            work([(h, 0, 1) for h in heads])
+            for h in heads:
                 wait_right(h)
-                block(h, 1, 1)
-                block(h, 1, 2)
-                block(h, 1, 0)
-                finish(h, 1, False)
-                if h:
-                    greet_far()
+            work([(h, 1, b) for b in range(3) for h in heads], [(h, 1, False) for h in heads])
+            greet_far()
+            for h in heads:
                 wait_left(1 + h)
-                block(h, 0, 0)
-                fold_table(h, finish(h, 0, True))
+                work([(h, 0, 0)], [(h, 0, True)])
 
     row = lax.broadcasted_iota(jnp.int32, (8, HEAD_DIM), 0)
     vec = jnp.zeros((8, HEAD_DIM), F32)
@@ -491,12 +481,10 @@
         for o in far_first(nx):
             remote(lines.at[mine], lines.at[mine], xy_send, x_recv, along(2, o)).start()
         stage_results()
-        send_results(jnp.logical_not(at_end))
         wait_bytes(lines.at[:2 * nx - 1], x_recv)
         lines[ys + y] = line_sum(0, 2 * nx)
         for o in far_first(ny):
             remote(lines.at[ys + y], lines.at[ys + y], xy_send, y_recv, along(1, o)).start()
-        send_results(at_end)
         if ny > 1:
             wait_bytes(lines.at[:ny - 1], y_recv)
         part = line_sum(ys, ny)
@@ -509,6 +497,8 @@
         for o in [*far_first(nz), 0]:
             for core in range(2 if o else 1):
                 remote(zout.at[core], zbuf.at[z], z_send, z_recv, along(0, o, core)).start()
+        send_results(place >= 0)
+        signal(row_sem, (z, y, x, 0))
 
     @pl.when(tp == 0)
     def _():
@@ -516,6 +506,7 @@
         for o in [*far_first(nx), 0]:
             remote(lines.at[mine], lines.at[mine], xy_send, x_recv, along(2, o)).start()
         stage_results()
+        pl.semaphore_wait(row_sem, 1)
         send_results(place >= 0)
 
     @pl.when(takes_back)

time: 37.8 us -> 37.5 us (level)
  no operation moved by 1% of the time
where the time goes in v7:
time: 37.5 us; the launch traced here: 37.4 us
  Pallas kernels  36.7 us (98%)
  between operations  0.64 us (2%)
    pallas_call x1, Pallas kernels, local(): pl.pallas_call(functools.partial(kernel, sizes), out_shape=tuple((vmem(*o...  35.9 us
    pallas_call x1, Pallas kernels, local(): pl.pallas_call(write_out, out_shape=tuple((jax.ShapeDtypeStruct(*o) for o...  0.79 us

profile of v7, /device:TPU:1, one launch (start us, length us, event | category | flops | bytes accessed | tf_op | source)
XLA Modules:
  0.0 37.4 jit_solution(9785955141376069863)
XLA Ops:
  0.6 35.9 %segment_attention_grad.1 = (bf16[256,256]{1,0:T(8,128)(2,1)S(1)}, bf16[256,256]{1,0:T(8,128)(2,1)S(1)}, bf16[256,256]{1,0:T(8,128)(2,1)S(1)}, f32[2,192]{1,0:T(2,128)S(1)}, f32[2,128]{1,0:T(2,128)S(1)}) custom-call(bf16[256,256]{1,0:T(8,128)(2,1)} %q_hbm.1, bf16[256,256]{1,0:T(8,128)(2,1)} %k_hbm.1, bf16[256,256]{1,0:T(8,128)(2,1)} %v_hbm.1, ...), custom_call_target="tpu_custom_call" | custom-call | tf_op jit(solution)/shard_map/segment_attention_grad/pallas_call | solution.py:600
  36.6 0.8 %write_out.1 = (bf16[256,256]{1,0:T(8,128)(2,1)}, bf16[256,256]{1,0:T(8,128)(2,1)}, bf16[256,256]{1,0:T(8,128)(2,1)}, f32[2,192]{1,0:T(2,128)}, f32[2,128]{1,0:T(2,128)}) custom-call(bf16[256,256]{1,0:T(8,128)(2,1)S(1)} %get-tuple-element.15.refs_0_, bf16[256,256]{1,0:T(8,128)(2,1)S(1)} %get-tuple-element.16.refs_1_, ...), custom_call_target="tpu_custom_call" | custom-call | tf_op jit(solution)/shard_map/write_out/pallas_call | solution.py:623

commit v8 on v7

--- a/solution.py
+++ b/solution.py
@@ -52,9 +52,9 @@
            qu, qr, ku, kr, bias_v, e_v, dp_v,
            dkx, dvx, dqx, d_v, prob_v, d_low_v, sum_v, gain_v, table_v2, extra_gain, extra_dv,
            to_before, from_after, to_after, from_before, dq_from_before, to_before_first, from_after_first,
-           lines, zout, zbuf,
+           lines, plane, zout, zbuf,
            load_sem, gains_sem, table_sem, halo_send, left_recv, right_recv, back_send, after_recv, before_recv, first_recv,
-           xy_send, x_recv, y_recv, z_send, z_recv, round1, round2, round3, row_sem):
+           xy_send, x_recv, y_recv, plane_recv, z_send, z_recv, round1, round2, round3, plane_round):
     nz, ny, nx = sizes
     z, y, x, tp = (lax.axis_index(a) for a in AXES)
     place = (z * ny + y) * nx + x
@@ -338,7 +338,6 @@
     @pl.when(tp == 1)
     def _():
         pl.semaphore_wait(round1, len(close))
-        signal(row_sem, (z, y, x, 0))
         for a, n in enumerate(sizes[:2]):
             if n > 5:
                 for o in near(n, 2):
@@ -354,12 +353,16 @@
         def _():
             wait_bytes(kvx.at[:, h, :PAIR], right_recv.at[h])
 
+    beside = sorted({*near(ny), *near(ny, 2)})
+
     def greet_far():
         @pl.when(tp == 1)
         def _():
             count = sum(len(near(n, 2)) for n in sizes[:2] if n > 5)
             if count:
                 pl.semaphore_wait(round2, count)
+            for o in beside:
+                signal(plane_round, along(1, o))
             if nz > 9:
                 for o in near(nz, 3):
                     signal(round3, along(0, o))
@@ -381,7 +384,8 @@
         for h in heads:
             wait_left(1 + h)
             work([(h, 0, 0)], [(h, 0, False)])
-        greet_far()
+            if not h:
+                greet_far()
         for h in heads:
             wait_right(h)
         work([(h, 1, b) for b in range(3) for h in heads], [(h, 1, True) for h in heads])
@@ -394,9 +398,9 @@
             for h in heads:
                 wait_right(h)
             work([(h, 1, b) for b in (1, 2) for h in heads])
+            greet_far()
             wait_left(0)
             work([(h, p, 1 - p) for p in (1, 0) for h in heads], [(h, 1, False) for h in heads])
-            greet_far()
             for h in heads:
                 wait_left(1 + h)
                 work([(h, 0, 0)], [(h, 0, True)])
@@ -415,15 +419,10 @@
                 wait_left(1 + h)
                 work([(h, 0, 0)], [(h, 0, True)])
 
-    row = lax.broadcasted_iota(jnp.int32, (8, HEAD_DIM), 0)
-    vec = jnp.zeros((8, HEAD_DIM), F32)
+    gain = gain_v[0, 0] + gain_v[0, 1] + gain_v[1, 0] + gain_v[1, 1] + jnp.where(opens, extra_gain[...], 0.0)
     second = jnp.where(lane < SEG, table_v2[0, 1], table_v2[1, 1])
-    for j, part in enumerate((table_v2[0, 0], table_v2[1, 0], second)):
-        vec = jnp.where(row == 3 * tp + j, part, vec)
-    part = gain_v[0, 0] + gain_v[0, 1] + gain_v[1, 0] + gain_v[1, 1] + jnp.where(opens, extra_gain[...], 0.0)
-    vec = jnp.where(row == 6, part * FACTOR, vec)
-    mine = 2 * x + tp
-    lines[mine] = vec[:7]
+    vec = jnp.concatenate([table_v2[0, 0], table_v2[1, 0], second, gain * FACTOR], axis=0)
+    chip = y * nx + x
 
     to_neighbours = [
         remote(to_before.at[:, h], from_after.at[:, h], back_send.at[0], after_recv.at[h], before) for h in range(HEADS)]
@@ -467,30 +466,35 @@
             for copy in to_next:
                 copy.start()
 
-    def line_sum(first, count):
-        part = lines[first]
-        for n in range(first + 1, first + count):
-            part = part + lines[n]
-        return part
-
-    ys, zs = 2 * nx, 2 * nx + ny
-    at_end = jnp.logical_or(x == 0, x == nx - 1)
+    def sum_of(ref, first, count):
+        parts = [ref[n] for n in range(first, first + count)]
+        while len(parts) > 1:
+            parts = [sum(parts[n:n + 2]) for n in range(0, len(parts), 2)]
+        return parts[0]
 
     @pl.when(tp == 1)
     def _():
+        lines[x] = vec
         for o in far_first(nx):
-            remote(lines.at[mine], lines.at[mine], xy_send, x_recv, along(2, o)).start()
+            remote(lines.at[x], lines.at[x], xy_send, x_recv, along(2, o)).start()
+        if beside:
+            pl.semaphore_wait(plane_round, len(beside))
+        signal(round1, (z, y, x, 0))
         stage_results()
-        wait_bytes(lines.at[:2 * nx - 1], x_recv)
-        lines[ys + y] = line_sum(0, 2 * nx)
+        if nx > 1:
+            wait_bytes(lines.at[:nx - 1], x_recv)
+        lines[nx + y] = sum_of(lines, 0, nx)
         for o in far_first(ny):
-            remote(lines.at[ys + y], lines.at[ys + y], xy_send, y_recv, along(1, o)).start()
+            remote(lines.at[nx + y], lines.at[nx + y], xy_send, y_recv, along(1, o)).start()
+        wait_bytes(plane, plane_recv)
+        others = sum_of(plane, 0, nx * ny)
         if ny > 1:
             wait_bytes(lines.at[:ny - 1], y_recv)
-        part = line_sum(ys, ny)
-        for core in range(2):
-            zout[core, :3] = part[3 * core:3 * core + 3]
-            zout[core, 3:] = part[6:]
+        part = sum_of(lines, nx, ny)
+        gain = part[3:] + others[3:]
+        for core, rows in enumerate((others, part)):
+            zout[core, :3] = rows[:3]
+            zout[core, 3:] = gain
         zbuf[z] = zout[1]
         if nz > 9:
             pl.semaphore_wait(round3, len(near(nz, 3)))
@@ -498,15 +502,20 @@
             for core in range(2 if o else 1):
                 remote(zout.at[core], zbuf.at[z], z_send, z_recv, along(0, o, core)).start()
         send_results(place >= 0)
-        signal(row_sem, (z, y, x, 0))
+        signal(round2, (z, y, x, 0))
 
     @pl.when(tp == 0)
     def _():
-        pl.semaphore_wait(row_sem, 1)
-        for o in [*far_first(nx), 0]:
-            remote(lines.at[mine], lines.at[mine], xy_send, x_recv, along(2, o)).start()
+        plane[chip] = vec
+        pl.semaphore_wait(round1, 1)
+        for oy, ox in sorted(
+                ((oy, ox) for oy in range(ny) for ox in range(nx)),
+                key=lambda o: -min(o[0], ny - o[0]) - min(o[1], nx - o[1])):
+            remote(
+                plane.at[chip], plane.at[chip], xy_send, plane_recv,
+                (z, lax.rem(y + oy, ny), lax.rem(x + ox, nx), 1)).start()
         stage_results()
-        pl.semaphore_wait(row_sem, 1)
+        pl.semaphore_wait(round2, 1)
         send_results(place >= 0)
 
     @pl.when(takes_back)
@@ -563,7 +572,7 @@
 
     @pl.when(tp == 0)
     def _():
-        wait_bytes(lines.at[:nx], xy_send)
+        wait_bytes(plane, xy_send)
         wait_bytes(zbuf.at[:nz], z_recv)
 
     result = zbuf[0]
@@ -612,9 +621,9 @@
             vmem((HEADS, 2, 1, PAIR), F32), vmem((1, HEAD_DIM), F32), vmem((HEADS, BEFORE, HEAD_DIM), F32),
             vmem((2, HEADS, BEFORE, HEAD_DIM), BF16), vmem((2, HEADS, BEFORE, HEAD_DIM), BF16),
             vmem((2, *first), BF16), vmem((2, *first), BF16), vmem(first, F32), vmem((2, *first), BF16), vmem((2, *first), BF16),
-            vmem((2 * nx + ny, 7, HEAD_DIM), F32), vmem((2, 4, HEAD_DIM), F32), vmem((2 * nz, 4, HEAD_DIM), F32),
+            vmem((nx + ny, 4, HEAD_DIM), F32), vmem((nx * ny, 4, HEAD_DIM), F32), vmem((2, 4, HEAD_DIM), F32), vmem((2 * nz, 4, HEAD_DIM), F32),
             dma((2,)), dma, dma, dma((2,)), dma((HEADS + 2,)), dma((HEADS,)), dma((2,)), dma((HEADS,)), dma, dma,
-            dma, dma, dma, dma, dma, regular, regular, regular, regular,
+            dma, dma, dma, dma, dma, dma, regular, regular, regular, regular,
         ],
         compiler_params=pltpu.CompilerParams(
             collective_id=0, has_side_effects=True, vmem_limit_bytes=32 * 1024 * 1024),

time: 37.5 us -> 37.2 us (level)
  the two profiles are of different devices: /device:TPU:1 before, /device:TPU:62 now
where the time goes in v8:
time: 37.2 us; the launch traced here: 37 us
  Pallas kernels  36.4 us (98%)
  between operations  0.64 us (2%)
    pallas_call x1, Pallas kernels, local(): pl.pallas_call(functools.partial(kernel, sizes), out_shape=tuple((vmem(*o...  35.6 us
    pallas_call x1, Pallas kernels, local(): pl.pallas_call(write_out, out_shape=tuple((jax.ShapeDtypeStruct(*o) for o...  0.79 us

profile of v8, /device:TPU:62, one launch (start us, length us, event | category | flops | bytes accessed | tf_op | source)
XLA Modules:
  0.0 37.0 jit_solution(15403081767345664659)
XLA Ops:
  0.6 35.6 %segment_attention_grad.1 = (bf16[256,256]{1,0:T(8,128)(2,1)S(1)}, bf16[256,256]{1,0:T(8,128)(2,1)S(1)}, bf16[256,256]{1,0:T(8,128)(2,1)S(1)}, f32[2,192]{1,0:T(2,128)S(1)}, f32[2,128]{1,0:T(2,128)S(1)}) custom-call(bf16[256,256]{1,0:T(8,128)(2,1)} %q_hbm.1, bf16[256,256]{1,0:T(8,128)(2,1)} %k_hbm.1, bf16[256,256]{1,0:T(8,128)(2,1)} %v_hbm.1, ...), custom_call_target="tpu_custom_call" | custom-call | tf_op jit(solution)/shard_map/segment_attention_grad/pallas_call | solution.py:609
  36.2 0.8 %write_out.1 = (bf16[256,256]{1,0:T(8,128)(2,1)}, bf16[256,256]{1,0:T(8,128)(2,1)}, bf16[256,256]{1,0:T(8,128)(2,1)}, f32[2,192]{1,0:T(2,128)}, f32[2,128]{1,0:T(2,128)}) custom-call(bf16[256,256]{1,0:T(8,128)(2,1)S(1)} %get-tuple-element.15.refs_0_, bf16[256,256]{1,0:T(8,128)(2,1)S(1)} %get-tuple-element.16.refs_1_, ...), custom_call_target="tpu_custom_call" | custom-call | tf_op jit(solution)/shard_map/write_out/pallas_call | solution.py:632

commit v9 on v8

--- a/solution.py
+++ b/solution.py
@@ -481,6 +481,7 @@
             pl.semaphore_wait(plane_round, len(beside))
         signal(round1, (z, y, x, 0))
         stage_results()
+        send_results(jnp.logical_and(x > 0, x < nx - 1))
         if nx > 1:
             wait_bytes(lines.at[:nx - 1], x_recv)
         lines[nx + y] = sum_of(lines, 0, nx)
@@ -501,7 +502,7 @@
         for o in [*far_first(nz), 0]:
             for core in range(2 if o else 1):
                 remote(zout.at[core], zbuf.at[z], z_send, z_recv, along(0, o, core)).start()
-        send_results(place >= 0)
+        send_results(jnp.logical_or(x == 0, x == nx - 1))
         signal(round2, (z, y, x, 0))
 
     @pl.when(tp == 0)
@@ -515,8 +516,9 @@
                 plane.at[chip], plane.at[chip], xy_send, plane_recv,
                 (z, lax.rem(y + oy, ny), lax.rem(x + ox, nx), 1)).start()
         stage_results()
+        send_results(jnp.logical_or(opens, jnp.logical_and(x > 0, x < nx - 1)))
         pl.semaphore_wait(round2, 1)
-        send_results(place >= 0)
+        send_results(jnp.logical_and(jnp.logical_not(opens), jnp.logical_or(x == 0, x == nx - 1)))
 
     @pl.when(takes_back)
     def _():

time: 37.2 us -> 36.5 us (0.981)
  the two profiles are of different devices: /device:TPU:62 before, /device:TPU:1 now
where the time goes in v9:
time: 36.5 us; the launch traced here: 36.3 us
  Pallas kernels  35.7 us (98%)
  between operations  0.64 us (2%)
    pallas_call x1, Pallas kernels, local(): pl.pallas_call(functools.partial(kernel, sizes), out_shape=tuple((vmem(*o...  34.9 us
    pallas_call x1, Pallas kernels, local(): pl.pallas_call(write_out, out_shape=tuple((jax.ShapeDtypeStruct(*o) for o...  0.79 us

profile of v9, /device:TPU:1, one launch (start us, length us, event | category | flops | bytes accessed | tf_op | source)
XLA Modules:
  0.0 36.3 jit_solution(17298626421535738027)
XLA Ops:
  0.6 34.9 %segment_attention_grad.1 = (bf16[256,256]{1,0:T(8,128)(2,1)S(1)}, bf16[256,256]{1,0:T(8,128)(2,1)S(1)}, bf16[256,256]{1,0:T(8,128)(2,1)S(1)}, f32[2,192]{1,0:T(2,128)S(1)}, f32[2,128]{1,0:T(2,128)S(1)}) custom-call(bf16[256,256]{1,0:T(8,128)(2,1)} %q_hbm.1, bf16[256,256]{1,0:T(8,128)(2,1)} %k_hbm.1, bf16[256,256]{1,0:T(8,128)(2,1)} %v_hbm.1, ...), custom_call_target="tpu_custom_call" | custom-call | tf_op jit(solution)/shard_map/segment_attention_grad/pallas_call | solution.py:611
  35.5 0.8 %write_out.1 = (bf16[256,256]{1,0:T(8,128)(2,1)}, bf16[256,256]{1,0:T(8,128)(2,1)}, bf16[256,256]{1,0:T(8,128)(2,1)}, f32[2,192]{1,0:T(2,128)}, f32[2,128]{1,0:T(2,128)}) custom-call(bf16[256,256]{1,0:T(8,128)(2,1)S(1)} %get-tuple-element.15.refs_0_, bf16[256,256]{1,0:T(8,128)(2,1)S(1)} %get-tuple-element.16.refs_1_, ...), custom_call_target="tpu_custom_call" | custom-call | tf_op jit(solution)/shard_map/write_out/pallas_call | solution.py:634

commit v10 on v9

--- a/solution.py
+++ b/solution.py
@@ -50,11 +50,11 @@
            dq_v, dk_v, dv_v, dtab_v, dgain_v,
            q_raw, k_raw, qdx, qd0, kvx, first_kv, gains_v, table_v,
            qu, qr, ku, kr, bias_v, e_v, dp_v,
-           dkx, dvx, dqx, d_v, prob_v, d_low_v, sum_v, gain_v, table_v2, extra_gain, extra_dv,
+           dkx, dvx, dqx, d_v, prob_v, d_low_v, sum_v, gain_v, table_v2, extra_gain, first_prob, first_d_low, first_dk,
            to_before, from_after, to_after, from_before, dq_from_before, to_before_first, from_after_first,
-           lines, plane, zout, zbuf,
-           load_sem, gains_sem, table_sem, halo_send, left_recv, right_recv, back_send, after_recv, before_recv, first_recv,
-           xy_send, x_recv, y_recv, plane_recv, z_send, z_recv, round1, round2, round3, plane_round):
+           rows_x, plane, zout, zbuf,
+           load_sem, more_sem, gains_sem, table_sem, left_recv, right_recv, after_recv, before_recv,
+           sum_send, x_recv, plane_recv, z_recv, round1, round2, round3, plane_round):
     nz, ny, nx = sizes
     z, y, x, tp = (lax.axis_index(a) for a in AXES)
     place = (z * ny + y) * nx + x
@@ -104,11 +104,11 @@
         load.start()
     for h in range(HEADS):
         lanes = slice(h * HEAD_DIM, (h + 1) * HEAD_DIM)
-        pltpu.make_async_copy(k_hbm.at[:, lanes], k_raw.at[h], load_sem.at[0]).start()
-        pltpu.make_async_copy(q_hbm.at[:, lanes], q_raw.at[h], load_sem.at[0]).start()
-        pltpu.make_async_copy(v_hbm.at[:, lanes], kvx.at[1, h, BEFORE:BEFORE + ROWS], load_sem.at[0]).start()
-        pltpu.make_async_copy(do_hbm.at[:SEG, lanes], qd0.at[1, h], load_sem.at[0]).start()
-        pltpu.make_async_copy(do_hbm.at[SEG:, lanes], qdx.at[1, h, :BEFORE], load_sem.at[1]).start()
+        pltpu.make_async_copy(k_hbm.at[:, lanes], k_raw.at[h], load_sem).start()
+        pltpu.make_async_copy(q_hbm.at[:, lanes], q_raw.at[h], load_sem).start()
+        pltpu.make_async_copy(v_hbm.at[:, lanes], kvx.at[1, h, BEFORE:BEFORE + ROWS], load_sem).start()
+        pltpu.make_async_copy(do_hbm.at[:SEG, lanes], qd0.at[1, h], load_sem).start()
+        pltpu.make_async_copy(do_hbm.at[SEG:, lanes], qdx.at[1, h, :BEFORE], more_sem).start()
 
     close = [(a, o) for a, n in enumerate(sizes) for o in near(n)]
 
@@ -126,7 +126,7 @@
         load.wait()
     gains = gains_v[...]
     gain_q, gain_k = gains[0:1, :], gains[1:2, :]
-    wait_bytes(kvx.at[:, :, :ROWS + PAIR + SEG // 2], load_sem.at[0])
+    wait_bytes(kvx.at[:, :, :ROWS + PAIR + SEG // 2], load_sem)
     def norm_keys(first, size):
         for h in range(HEADS):
             u, r = unit(k_raw[h, first:first + size])
@@ -142,16 +142,16 @@
             out[h] = (u * gain_q).astype(BF16)
 
     forth = [remote(
-        kvx.at[:, :, ROWS + PAIR:ROWS + BEFORE], kvx.at[:, :, PAIR:BEFORE], halo_send.at[0], left_recv.at[HEADS], after)]
+        kvx.at[:, :, ROWS + PAIR:ROWS + BEFORE], kvx.at[:, :, PAIR:BEFORE], load_sem, left_recv.at[HEADS], after)]
     back = {}
     for h in range(HEADS):
         forth.append(remote(
-            kvx.at[:, h, ROWS:ROWS + PAIR], kvx.at[:, h, :PAIR], halo_send.at[0], left_recv.at[h], after))
+            kvx.at[:, h, ROWS:ROWS + PAIR], kvx.at[:, h, :PAIR], load_sem, left_recv.at[h], after))
         back[h] = [
-            remote(kvx.at[:, h, BEFORE:ROWS], kvx.at[:, h, BEFORE + ROWS:], halo_send.at[1], right_recv.at[h], before),
-            remote(qd0.at[:, h], qdx.at[:, h, BEFORE:], halo_send.at[1], right_recv.at[h], before)]
-
-    plane_piece = remote(kvx.at[:, :, BEFORE:ROWS], first_kv, halo_send.at[0], left_recv.at[HEADS + 1], after)
+            remote(kvx.at[:, h, BEFORE:ROWS], kvx.at[:, h, BEFORE + ROWS:], gains_sem, right_recv, before),
+            remote(qd0.at[:, h], qdx.at[:, h, BEFORE:], gains_sem, right_recv, before)]
+
+    plane_piece = remote(kvx.at[:, :, BEFORE:ROWS], first_kv, load_sem, left_recv.at[HEADS - 1], after)
 
     def go_on(pieces, when=place < total - 1):
         @pl.when(when)
@@ -177,7 +177,7 @@
         for a, o in close:
             signal(round1, along(a, o))
 
-    wait_bytes(qdx.at[1, :, :BEFORE], load_sem.at[1])
+    wait_bytes(qdx.at[1, :, :BEFORE], more_sem)
 
     @pl.when(is_first)
     def _():
@@ -185,10 +185,6 @@
             for n in range(2):
                 kvx[n, h, :BEFORE] = kvx[n, h, BEFORE:2 * BEFORE]
                 first_kv[n, h] = kvx[n, h, BEFORE:ROWS]
-
-    @pl.when(opens)
-    def _():
-        extra_gain[...] = jnp.zeros((1, HEAD_DIM), F32)
 
     @pl.when(closes)
     def _():
@@ -300,36 +296,49 @@
     def fold_table(h, d_score):
         table_v2[h, 0], table_v2[h, 1] = fold_rows(h, d_score)
 
-    def first_segment(h):
-        queries, cotangents = qd0[0, h], qd0[1, h]
-        keys, rest = first_kv[0, h], kvx[0, h, :ROWS]
+    def first_segment():
         key_number = lax.broadcasted_iota(jnp.int32, (ROWS + SEG, SEG), 0)
-        bias = bias_v[h, 0, :ROWS + SEG][:, :SEG]
-        bias = jnp.where(jnp.logical_and(is_first, key_number < ROWS), MASKED, bias)
-        bias = bias - jnp.max(bias, axis=0, keepdims=True)
-        s = jnp.concatenate([dot(keys, queries, 1, 1), dot(rest, queries, 1, 1)], axis=0)
-        e = jnp.exp2(s * (FACTOR * LOG2E) + bias)
-        dp = jnp.concatenate([dot(first_kv[1, h], cotangents, 1, 1), dot(kvx[1, h, :ROWS], cotangents, 1, 1)], axis=0)
-        inv = 1.0 / jnp.sum(e, axis=0, keepdims=True)
-        delta = jnp.sum(e * dp, axis=0, keepdims=True) * inv
-        prob = e * inv
-        d_score = prob * (dp - delta)
-        d_low = d_score.astype(BF16)
-        dk = dot(d_low, queries, 1, 0)
-        dv = dot(prob.astype(BF16), cotangents, 1, 0)
-        dq_from_before[h] = dot(d_low[:SEG], keys, 0, 0) + dot(d_low[SEG:], rest, 0, 0)
-        for n, part in enumerate((dk * FACTOR, dv)):
+        hidden = jnp.logical_and(is_first, key_number < ROWS)
+
+        def against(n, h, side):
+            return jnp.concatenate([dot(first_kv[n, h], side, 1, 1), dot(kvx[n, h, :ROWS], side, 1, 1)], axis=0)
+
+        scores = [against(0, h, qd0[0, h]) for h in heads]
+        d_probs = [against(1, h, qd0[1, h]) for h in heads]
+        d_scores = []
+        for h in heads:
+            bias = jnp.where(hidden, MASKED, bias_v[h, 0, :ROWS + SEG][:, :SEG])
+            bias = bias - jnp.max(bias, axis=0, keepdims=True)
+            e = jnp.exp2(scores[h] * (FACTOR * LOG2E) + bias)
+            inv = 1.0 / jnp.sum(e, axis=0, keepdims=True)
+            delta = jnp.sum(e * d_probs[h], axis=0, keepdims=True) * inv
+            prob = e * inv
+            d_scores.append(prob * (d_probs[h] - delta))
+            first_prob[h] = prob.astype(BF16)
+            first_d_low[h] = d_scores[h].astype(BF16)
+        products = [dot(d_scores[h].astype(BF16), qd0[0, h], 1, 0) for h in heads]
+        for h in heads:
+            tile = jnp.concatenate([d_scores[h], jnp.zeros((ROWS + SEG, SEG), F32)], axis=1)
+            rows = fold_rows(h, jnp.concatenate([tile, jnp.zeros((SEG, PAIR), F32)], axis=0))
+            for j in range(2):
+                table_v2[h, j] = table_v2[h, j] + rows[j]
+        gain = jnp.zeros((1, HEAD_DIM), F32)
+        for h in heads:
+            dk = products[h]
+            first_dk[h] = dk
+            gain = gain + jnp.sum(dk[:SEG] * first_kv[0, h].astype(F32), axis=0, keepdims=True)
+            gain = gain + jnp.sum(dk[SEG:] * kvx[0, h, :ROWS].astype(F32), axis=0, keepdims=True)
+        extra_gain[...] = gain
+
+    def first_results(h):
+        d_low = first_d_low[h]
+        dv = dot(first_prob[h], qd0[1, h], 1, 0)
+        dq_from_before[h] = dot(d_low[:SEG], first_kv[0, h], 0, 0) + dot(d_low[SEG:], kvx[0, h, :ROWS], 0, 0)
+        for n, part in enumerate((first_dk[h] * FACTOR, dv)):
             to_before_first[n, h] = part[:SEG].astype(BF16)
             from_before[n, h] = part[ROWS:].astype(BF16)
-        dkx[h, :BEFORE] = dkx[h, :BEFORE] + dk[SEG:ROWS]
-        extra_dv[h] = dv[SEG:ROWS]
-        extra_gain[...] = extra_gain[...] + (
-            jnp.sum(dk[:SEG] * keys.astype(F32), axis=0, keepdims=True)
-            + jnp.sum(dk[SEG:] * rest.astype(F32), axis=0, keepdims=True))
-        tile = jnp.concatenate([d_score, jnp.zeros((ROWS + SEG, SEG), F32)], axis=1)
-        rows = fold_rows(h, jnp.concatenate([tile, jnp.zeros((SEG, PAIR), F32)], axis=0))
-        for j in range(2):
-            table_v2[h, j] = table_v2[h, j] + rows[j]
+        dkx[h, :BEFORE] = dkx[h, :BEFORE] + first_dk[h, SEG:ROWS]
+        dvx[h, :BEFORE] = dvx[h, :BEFORE] + dv[SEG:ROWS]
 
     heads = range(HEADS)
     work([(h, 0, 2) for h in heads])
@@ -346,12 +355,21 @@
     def wait_left(piece):
         @pl.when(place > 0)
         def _():
-            forth[piece].wait_recv()
-
-    def wait_right(h):
+            if piece < HEADS:
+                forth[piece].wait_recv()
+            else:
+                @pl.when(opens)
+                def _():
+                    wait_bytes(kvx.at[:, :, :PAIR], left_recv.at[piece - 1])
+
+                @pl.when(takes_back)
+                def _():
+                    forth[piece].wait_recv()
+
+    def wait_right():
         @pl.when(takes_next)
         def _():
-            wait_bytes(kvx.at[:, h, :PAIR], right_recv.at[h])
+            wait_bytes(kvx.at[:, :, :PAIR], right_recv)
 
     beside = sorted({*near(ny), *near(ny, 2)})
 
@@ -370,12 +388,7 @@
     def do_first():
         @pl.when(opens)
         def _():
-            @pl.when(place > 0)
-            def _():
-                plane_piece.wait_recv()
-
-            for h in range(HEADS):
-                first_segment(h)
+            first_segment()
 
     @pl.when(x == nx - 1)
     def _():
@@ -386,8 +399,7 @@
             work([(h, 0, 0)], [(h, 0, False)])
             if not h:
                 greet_far()
-        for h in heads:
-            wait_right(h)
+        wait_right()
         work([(h, 1, b) for b in range(3) for h in heads], [(h, 1, True) for h in heads])
         if nx == 1:
             do_first()
@@ -395,8 +407,7 @@
     if nx > 1:
         @pl.when(x == 0)
         def _():
-            for h in heads:
-                wait_right(h)
+            wait_right()
             work([(h, 1, b) for b in (1, 2) for h in heads])
             greet_far()
             wait_left(0)
@@ -411,8 +422,7 @@
         def _():
             wait_left(0)
             work([(h, 0, 1) for h in heads])
-            for h in heads:
-                wait_right(h)
+            wait_right()
             work([(h, 1, b) for b in range(3) for h in heads], [(h, 1, False) for h in heads])
             greet_far()
             for h in heads:
@@ -425,13 +435,25 @@
     chip = y * nx + x
 
     to_neighbours = [
-        remote(to_before.at[:, h], from_after.at[:, h], back_send.at[0], after_recv.at[h], before) for h in range(HEADS)]
+        remote(to_before.at[:, h], from_after.at[:, h], more_sem, after_recv, before) for h in range(HEADS)]
     to_next = [
-        remote(to_after, from_before, back_send.at[1], before_recv, after),
-        remote(dqx.at[:, BEFORE:], dq_from_before, back_send.at[1], before_recv, after)]
-    to_plane_before = remote(to_before_first, from_after_first, back_send.at[0], first_recv, before)
+        remote(to_after, from_before, table_sem, before_recv, after),
+        remote(dqx.at[:, BEFORE:], dq_from_before, table_sem, before_recv, after)]
+    to_plane_before = remote(to_before_first, from_after_first, more_sem, after_recv, before)
 
     def stage_results():
+        @pl.when(takes_next)
+        def _():
+            wait_bytes(kvx.at[:, :, :BEFORE], load_sem)
+
+        @pl.when(closes_early)
+        def _():
+            wait_bytes(kvx.at[:, :, :ROWS], load_sem)
+
+        @pl.when(takes_back)
+        def _():
+            wait_bytes(kvx.at[:, :, :PAIR], gains_sem)
+
         for h in range(HEADS):
             low, high_tile = (dot(prob_v[h, p], qdx[1, h, p * PAIR:(p + 1) * PAIR], 1, 0) for p in range(2))
             dvx[h, :PAIR] = low[:PAIR]
@@ -440,7 +462,7 @@
 
             @pl.when(opens)
             def _(h=h):
-                dvx[h, :BEFORE] = dvx[h, :BEFORE] + extra_dv[h]
+                first_results(h)
 
             lanes = slice(h * HEAD_DIM, (h + 1) * HEAD_DIM)
             to_before[0, h] = (dkx[h, :BEFORE] * FACTOR).astype(BF16)
@@ -472,26 +494,35 @@
             parts = [sum(parts[n:n + 2]) for n in range(0, len(parts), 2)]
         return parts[0]
 
+    has_across = ny > 3 and ny % 2 == 0
+    across, column = nx * ny, nx * ny + nx
+
     @pl.when(tp == 1)
     def _():
-        lines[x] = vec
+        rows_x[x] = vec
         for o in far_first(nx):
-            remote(lines.at[x], lines.at[x], xy_send, x_recv, along(2, o)).start()
+            remote(rows_x.at[x], rows_x.at[x], sum_send, x_recv, along(2, o)).start()
         if beside:
             pl.semaphore_wait(plane_round, len(beside))
         signal(round1, (z, y, x, 0))
+        if has_across:
+            for o in far_first(nx) + [0]:
+                remote(
+                    rows_x.at[x], plane.at[across + x], sum_send, plane_recv,
+                    (z, lax.rem(y + ny // 2, ny), lax.rem(x + o, nx), 1)).start()
         stage_results()
         send_results(jnp.logical_and(x > 0, x < nx - 1))
         if nx > 1:
-            wait_bytes(lines.at[:nx - 1], x_recv)
-        lines[nx + y] = sum_of(lines, 0, nx)
-        for o in far_first(ny):
-            remote(lines.at[nx + y], lines.at[nx + y], xy_send, y_recv, along(1, o)).start()
-        wait_bytes(plane, plane_recv)
-        others = sum_of(plane, 0, nx * ny)
-        if ny > 1:
-            wait_bytes(lines.at[:ny - 1], y_recv)
-        part = sum_of(lines, nx, ny)
+            wait_bytes(rows_x.at[:nx - 1], x_recv)
+        plane[column + y] = sum_of(rows_x, 0, nx)
+        y_ways = [o for o in far_first(ny) if not has_across or o != ny // 2]
+        for o in y_ways:
+            remote(plane.at[column + y], plane.at[column + y], sum_send, plane_recv, along(1, o)).start()
+        came = nx * ny + len(y_ways) + (nx if has_across else 0)
+        wait_bytes(plane.at[:came], plane_recv)
+        if has_across:
+            plane[column + lax.rem(y + ny // 2, ny)] = sum_of(plane, across, nx)
+        others, part = sum_of(plane, 0, nx * ny), sum_of(plane, column, ny)
         gain = part[3:] + others[3:]
         for core, rows in enumerate((others, part)):
             zout[core, :3] = rows[:3]
@@ -501,7 +532,7 @@
             pl.semaphore_wait(round3, len(near(nz, 3)))
         for o in [*far_first(nz), 0]:
             for core in range(2 if o else 1):
-                remote(zout.at[core], zbuf.at[z], z_send, z_recv, along(0, o, core)).start()
+                remote(zout.at[core], zbuf.at[z], sum_send, z_recv, along(0, o, core)).start()
         send_results(jnp.logical_or(x == 0, x == nx - 1))
         signal(round2, (z, y, x, 0))
 
@@ -513,7 +544,7 @@
                 ((oy, ox) for oy in range(ny) for ox in range(nx)),
                 key=lambda o: -min(o[0], ny - o[0]) - min(o[1], nx - o[1])):
             remote(
-                plane.at[chip], plane.at[chip], xy_send, plane_recv,
+                plane.at[chip], plane.at[chip], sum_send, plane_recv,
                 (z, lax.rem(y + oy, ny), lax.rem(x + ox, nx), 1)).start()
         stage_results()
         send_results(jnp.logical_or(opens, jnp.logical_and(x > 0, x < nx - 1)))
@@ -524,18 +555,18 @@
     def _():
         wait_bytes(kvx.at[:, :, :PAIR], before_recv)
 
+    @pl.when(takes_next)
+    def _():
+        wait_bytes(from_after, after_recv)
+
     @pl.when(closes_early)
     def _():
-        to_plane_before.wait_recv()
+        wait_bytes(kvx.at[:, :, :ROWS], after_recv)
 
     for h in range(HEADS):
         dq_v[:SEG, h * HEAD_DIM:(h + 1) * HEAD_DIM] = query_rows(dq_from_before[h], qu[h, :SEG], qr[h, :SEG])
 
     for h in range(HEADS):
-        @pl.when(place < total - 1)
-        def _(h=h):
-            to_neighbours[h].wait_recv()
-
         lanes = slice(h * HEAD_DIM, (h + 1) * HEAD_DIM)
         sums_in = [
             jnp.concatenate([
@@ -548,33 +579,25 @@
 
     @pl.when(takes_next)
     def _():
-        wait_bytes(kvx.at[:, :, :BEFORE], halo_send.at[0])
-        wait_bytes(kvx.at[:, :, :PAIR], back_send.at[1])
-
-    @pl.when(closes_early)
-    def _():
-        wait_bytes(kvx.at[:, :, :ROWS], halo_send.at[0])
+        wait_bytes(kvx.at[:, :, :PAIR], table_sem)
 
     @pl.when(takes_back)
     def _():
-        wait_bytes(kvx.at[:, :, :PAIR], halo_send.at[1])
-        wait_bytes(from_after, back_send.at[0])
+        wait_bytes(from_after, more_sem)
 
     @pl.when(opens_later)
     def _():
-        wait_bytes(kvx.at[:, :, :ROWS], back_send.at[0])
+        wait_bytes(kvx.at[:, :, :ROWS], more_sem)
 
     @pl.when(tp == 1)
     def _():
-        if nx + ny > 2:
-            wait_bytes(lines.at[:nx + ny - 2], xy_send)
-        wait_bytes(zbuf.at[:2 * nz - 1], z_send)
+        wait_bytes(plane.at[:nx - 1 + 2 * nz - 1 + ny - 1 + (nx - 1 if has_across else 0)], sum_send)
         if nz > 1:
             wait_bytes(zbuf.at[:nz - 1], z_recv)
 
     @pl.when(tp == 0)
     def _():
-        wait_bytes(plane, xy_send)
+        wait_bytes(plane.at[:nx * ny], sum_send)
         wait_bytes(zbuf.at[:nz], z_recv)
 
     result = zbuf[0]
@@ -620,12 +643,13 @@
             vmem(pairs, F32), vmem(pairs, F32), vmem(pairs, F32),
             vmem(wide, F32), vmem(wide, F32), vmem(tile, F32), vmem((HEADS, 3 * PAIR, PAIR), F32),
             vmem(pairs, BF16), vmem(pairs, BF16), vmem((HEADS, 2, 6, 1, PAIR), F32), vmem((HEADS, 2, 1, PAIR), F32),
-            vmem((HEADS, 2, 1, PAIR), F32), vmem((1, HEAD_DIM), F32), vmem((HEADS, BEFORE, HEAD_DIM), F32),
+            vmem((HEADS, 2, 1, PAIR), F32), vmem((1, HEAD_DIM), F32),
+            vmem((HEADS, ROWS + SEG, SEG), BF16), vmem((HEADS, ROWS + SEG, SEG), BF16), vmem((HEADS, ROWS + SEG, HEAD_DIM), F32),
             vmem((2, HEADS, BEFORE, HEAD_DIM), BF16), vmem((2, HEADS, BEFORE, HEAD_DIM), BF16),
             vmem((2, *first), BF16), vmem((2, *first), BF16), vmem(first, F32), vmem((2, *first), BF16), vmem((2, *first), BF16),
-            vmem((nx + ny, 4, HEAD_DIM), F32), vmem((nx * ny, 4, HEAD_DIM), F32), vmem((2, 4, HEAD_DIM), F32), vmem((2 * nz, 4, HEAD_DIM), F32),
-            dma((2,)), dma, dma, dma((2,)), dma((HEADS + 2,)), dma((HEADS,)), dma((2,)), dma((HEADS,)), dma, dma,
-            dma, dma, dma, dma, dma, dma, regular, regular, regular, regular,
+            vmem((nx, 4, HEAD_DIM), F32), vmem((nx * ny + nx + ny + 2 * nz, 4, HEAD_DIM), F32), vmem((2, 4, HEAD_DIM), F32), vmem((2 * nz, 4, HEAD_DIM), F32),
+            dma, dma, dma, dma, dma((HEADS + 1,)), dma, dma, dma,
+            dma, dma, dma, dma, regular, regular, regular, regular,
         ],
         compiler_params=pltpu.CompilerParams(
             collective_id=0, has_side_effects=True, vmem_limit_bytes=32 * 1024 * 1024),

time: 36.5 us -> 36.4 us (level)
  no operation moved by 1% of the time
where the time goes in v10:
time: 36.4 us; the launch traced here: 36.2 us
  Pallas kernels  35.6 us (98%)
  between operations  0.64 us (2%)
    pallas_call x1, Pallas kernels, local(): pl.pallas_call(functools.partial(kernel, sizes), out_shape=tuple((vmem(*o...  34.8 us
    pallas_call x1, Pallas kernels, local(): pl.pallas_call(write_out, out_shape=tuple((jax.ShapeDtypeStruct(*o) for o...  0.79 us

profile of v10, /device:TPU:1, one launch (start us, length us, event | category | flops | bytes accessed | tf_op | source)
XLA Modules:
  0.0 36.2 jit_solution(12131278167766092456)
XLA Ops:
  0.6 34.8 %segment_attention_grad.1 = (bf16[256,256]{1,0:T(8,128)(2,1)S(1)}, bf16[256,256]{1,0:T(8,128)(2,1)S(1)}, bf16[256,256]{1,0:T(8,128)(2,1)S(1)}, f32[2,192]{1,0:T(2,128)S(1)}, f32[2,128]{1,0:T(2,128)S(1)}) custom-call(bf16[256,256]{1,0:T(8,128)(2,1)} %q_hbm.1, bf16[256,256]{1,0:T(8,128)(2,1)} %k_hbm.1, bf16[256,256]{1,0:T(8,128)(2,1)} %v_hbm.1, ...), custom_call_target="tpu_custom_call" | custom-call | tf_op jit(solution)/shard_map/segment_attention_grad/pallas_call | solution.py:634
  35.4 0.8 %write_out.1 = (bf16[256,256]{1,0:T(8,128)(2,1)}, bf16[256,256]{1,0:T(8,128)(2,1)}, bf16[256,256]{1,0:T(8,128)(2,1)}, f32[2,192]{1,0:T(2,128)}, f32[2,128]{1,0:T(2,128)}) custom-call(bf16[256,256]{1,0:T(8,128)(2,1)S(1)} %get-tuple-element.15.refs_0_, bf16[256,256]{1,0:T(8,128)(2,1)S(1)} %get-tuple-element.16.refs_1_, ...), custom_call_target="tpu_custom_call" | custom-call | tf_op jit(solution)/shard_map/write_out/pallas_call | solution.py:658

commit v11 on v10

--- a/solution.py
+++ b/solution.py
@@ -531,7 +531,7 @@
         if nz > 9:
             pl.semaphore_wait(round3, len(near(nz, 3)))
         for o in [*far_first(nz), 0]:
-            for core in range(2 if o else 1):
+            for core in ((1, 0) if o else (0,)):
                 remote(zout.at[core], zbuf.at[z], sum_send, z_recv, along(0, o, core)).start()
         send_results(jnp.logical_or(x == 0, x == nx - 1))
         signal(round2, (z, y, x, 0))

time: 36.4 us -> 36.1 us (level)
  no operation moved by 1% of the time
where the time goes in v11:
time: 36.1 us; the launch traced here: 35.9 us
  Pallas kernels  35.3 us (98%)
  between operations  0.64 us (2%)
    pallas_call x1, Pallas kernels, local(): pl.pallas_call(functools.partial(kernel, sizes), out_shape=tuple((vmem(*o...  34.5 us
    pallas_call x1, Pallas kernels, local(): pl.pallas_call(write_out, out_shape=tuple((jax.ShapeDtypeStruct(*o) for o...  0.79 us

profile of v11, /device:TPU:1, one launch (start us, length us, event | category | flops | bytes accessed | tf_op | source)
XLA Modules:
  0.0 35.9 jit_solution(13054811333897977165)
XLA Ops:
  0.6 34.5 %segment_attention_grad.1 = (bf16[256,256]{1,0:T(8,128)(2,1)S(1)}, bf16[256,256]{1,0:T(8,128)(2,1)S(1)}, bf16[256,256]{1,0:T(8,128)(2,1)S(1)}, f32[2,192]{1,0:T(2,128)S(1)}, f32[2,128]{1,0:T(2,128)S(1)}) custom-call(bf16[256,256]{1,0:T(8,128)(2,1)} %q_hbm.1, bf16[256,256]{1,0:T(8,128)(2,1)} %k_hbm.1, bf16[256,256]{1,0:T(8,128)(2,1)} %v_hbm.1, ...), custom_call_target="tpu_custom_call" | custom-call | tf_op jit(solution)/shard_map/segment_attention_grad/pallas_call | solution.py:634
  35.1 0.8 %write_out.1 = (bf16[256,256]{1,0:T(8,128)(2,1)}, bf16[256,256]{1,0:T(8,128)(2,1)}, bf16[256,256]{1,0:T(8,128)(2,1)}, f32[2,192]{1,0:T(2,128)}, f32[2,128]{1,0:T(2,128)}) custom-call(bf16[256,256]{1,0:T(8,128)(2,1)S(1)} %get-tuple-element.15.refs_0_, bf16[256,256]{1,0:T(8,128)(2,1)S(1)} %get-tuple-element.16.refs_1_, ...), custom_call_target="tpu_custom_call" | custom-call | tf_op jit(solution)/shard_map/write_out/pallas_call | solution.py:658

commit v12 on v11

--- a/solution.py
+++ b/solution.py
@@ -48,8 +48,8 @@
 
 def kernel(sizes, q_hbm, k_hbm, v_hbm, do_hbm, gains_hbm, table_hbm,
            dq_v, dk_v, dv_v, dtab_v, dgain_v,
-           q_raw, k_raw, qdx, qd0, kvx, first_kv, gains_v, table_v,
-           qu, qr, ku, kr, bias_v, e_v, dp_v,
+           qdx, qd0, kvx, first_kv, gains_v, table_v,
+           qn, qn0, qu, qr, kn, ku, kr, first_kn, first_ku, bias_v, e_v, dp_v,
            dkx, dvx, dqx, d_v, prob_v, d_low_v, sum_v, gain_v, table_v2, extra_gain, first_prob, first_d_low, first_dk,
            to_before, from_after, to_after, from_before, dq_from_before, to_before_first, from_after_first,
            rows_x, plane, zout, zbuf,
@@ -104,11 +104,10 @@
         load.start()
     for h in range(HEADS):
         lanes = slice(h * HEAD_DIM, (h + 1) * HEAD_DIM)
-        pltpu.make_async_copy(k_hbm.at[:, lanes], k_raw.at[h], load_sem).start()
-        pltpu.make_async_copy(q_hbm.at[:, lanes], q_raw.at[h], load_sem).start()
-        pltpu.make_async_copy(v_hbm.at[:, lanes], kvx.at[1, h, BEFORE:BEFORE + ROWS], load_sem).start()
-        pltpu.make_async_copy(do_hbm.at[:SEG, lanes], qd0.at[1, h], load_sem).start()
-        pltpu.make_async_copy(do_hbm.at[SEG:, lanes], qdx.at[1, h, :BEFORE], more_sem).start()
+        for n, (keys_or_values, queries_or_cotangents) in enumerate(((k_hbm, q_hbm), (v_hbm, do_hbm))):
+            pltpu.make_async_copy(keys_or_values.at[:, lanes], kvx.at[n, h, BEFORE:BEFORE + ROWS], load_sem).start()
+            pltpu.make_async_copy(queries_or_cotangents.at[:SEG, lanes], qd0.at[n, h], load_sem).start()
+            pltpu.make_async_copy(queries_or_cotangents.at[SEG:, lanes], qdx.at[n, h, :BEFORE], more_sem).start()
 
     close = [(a, o) for a, n in enumerate(sizes) for o in near(n)]
 
@@ -121,25 +120,6 @@
     @pl.when(tp == 0)
     def _():
         signal(barrier, (z, y, x, 1))
-
-    for load in small_loads:
-        load.wait()
-    gains = gains_v[...]
-    gain_q, gain_k = gains[0:1, :], gains[1:2, :]
-    wait_bytes(kvx.at[:, :, :ROWS + PAIR + SEG // 2], load_sem)
-    def norm_keys(first, size):
-        for h in range(HEADS):
-            u, r = unit(k_raw[h, first:first + size])
-            ku[h, first:first + size] = u
-            kr[h, first:first + size] = jnp.broadcast_to(r, u.shape)
-            kvx[0, h, BEFORE + first:BEFORE + first + size] = (u * gain_k).astype(BF16)
-
-    def norm_queries(first, size, out):
-        for h in range(HEADS):
-            u, r = unit(q_raw[h, first:first + size])
-            qu[h, first:first + size] = u
-            qr[h, first:first + size] = jnp.broadcast_to(r, u.shape)
-            out[h] = (u * gain_q).astype(BF16)
 
     forth = [remote(
         kvx.at[:, :, ROWS + PAIR:ROWS + BEFORE], kvx.at[:, :, PAIR:BEFORE], load_sem, left_recv.at[HEADS], after)]
@@ -159,25 +139,43 @@
             for copy in pieces:
                 copy.start()
 
-    norm_keys(BEFORE, SEG)
+    wait_bytes(kvx.at[:, :, :ROWS + SEG], load_sem)
+    small_loads[0].wait()
     pl.semaphore_wait(barrier, sides + jnp.where(tp == 1, 1 + len(close), 1))
     go_on(forth[:1])
-    norm_keys(0, SEG)
-    norm_queries(0, SEG, qd0.at[0])
-
     go_on([copy for h in range(HEADS) for copy in back[h]], takes_back)
-    norm_keys(SEG, PAIR)
     go_on(forth[1:], jnp.logical_and(tp == 0, place < total - 1))
     go_on(forth[1:2], jnp.logical_and(tp == 1, place < total - 1))
     go_on([plane_piece], closes_early)
-    norm_queries(SEG, BEFORE, qdx.at[0, :, :BEFORE])
 
     @pl.when(tp == 1)
     def _():
         for a, o in close:
             signal(round1, along(a, o))
 
-    wait_bytes(qdx.at[1, :, :BEFORE], more_sem)
+    wait_bytes(qdx.at[:, :, :BEFORE], more_sem)
+    small_loads[1].wait()
+    gains = gains_v[...]
+    gain_q, gain_k = gains[0:1, :], gains[1:2, :]
+
+    def take_keys(h, first, size):
+        u, r = unit(kvx[0, h, first:first + size])
+        ku[h, first:first + size] = u
+        kn[h, first:first + size] = (u * gain_k).astype(BF16)
+        return r
+
+    def take_queries(h):
+        qn[h, BEFORE:] = (unit(qdx[0, h, BEFORE:])[0] * gain_q).astype(BF16)
+
+    for h in range(HEADS):
+        kr[h] = jnp.broadcast_to(take_keys(h, BEFORE, ROWS), (ROWS, HEAD_DIM))
+        for raw, normed, rows in (
+                (qd0[0, h], qn0.at[h], slice(0, SEG)),
+                (qdx[0, h, :BEFORE], qn.at[h, :BEFORE], slice(SEG, ROWS))):
+            u, r = unit(raw)
+            qu[h, rows] = u
+            qr[h, rows] = jnp.broadcast_to(r, u.shape)
+            normed[...] = (u * gain_q).astype(BF16)
 
     @pl.when(is_first)
     def _():
@@ -232,7 +230,7 @@
         at_keys = {(p, b): slice((p + b) * PAIR, (p + b + 1) * PAIR) for h, p, b in blocks}
         at_queries = [slice(p * PAIR, (p + 1) * PAIR) for p in range(2)]
         at_rows = [slice(b * PAIR, (b + 1) * PAIR) for b in range(3)]
-        scores = [dot(kvx[0, h, at_keys[p, b]], qdx[0, h, at_queries[p]], 1, 1) for h, p, b in blocks]
+        scores = [dot(kn[h, at_keys[p, b]], qn[h, at_queries[p]], 1, 1) for h, p, b in blocks]
         d_probs = [dot(kvx[1, h, at_keys[p, b]], qdx[1, h, at_queries[p]], 1, 1) for h, p, b in blocks]
         for (h, p, b), s, dp in zip(blocks, scores, d_probs):
             e = jnp.exp2(s * (FACTOR * LOG2E) + bias_v[h, p, at_rows[b]])
@@ -250,7 +248,7 @@
             prob_v[h, p] = prob.astype(BF16)
             d_low_v[h, p] = d_low
             d_scores.append(d_score)
-            products.append(dot(d_low, qdx[0, h, at_queries[p]], 1, 0))
+            products.append(dot(d_low, qn[h, at_queries[p]], 1, 0))
         for (h, p, again), d_score in zip(tiles, d_scores):
             if again:
                 fold_table(h, d_v[h] + d_score)
@@ -258,7 +256,8 @@
                 d_v[h] = d_score
         for (h, p, again), dk in zip(tiles, products):
             keys = slice(p * PAIR, (p + 3) * PAIR)
-            gain_v[h, p] = jnp.sum(dk * kvx[0, h, keys].astype(F32), axis=0, keepdims=True)
+            gain_v[h, p, 0] = jnp.sum(dk * kn[h, keys].astype(F32), axis=0, keepdims=True)
+            gain_v[h, p, 1] = jnp.sum(dk * ku[h, keys], axis=0, keepdims=True)
             if again:
                 shared, alone = slice(PAIR, 3 * PAIR), slice(3 * p * PAIR, (3 * p + 1) * PAIR)
                 dkx[h, alone] = dk[2 * p * PAIR:(2 * p + 1) * PAIR]
@@ -300,11 +299,16 @@
         key_number = lax.broadcasted_iota(jnp.int32, (ROWS + SEG, SEG), 0)
         hidden = jnp.logical_and(is_first, key_number < ROWS)
 
-        def against(n, h, side):
-            return jnp.concatenate([dot(first_kv[n, h], side, 1, 1), dot(kvx[n, h, :ROWS], side, 1, 1)], axis=0)
-
-        scores = [against(0, h, qd0[0, h]) for h in heads]
-        d_probs = [against(1, h, qd0[1, h]) for h in heads]
+        for h in heads:
+            u, _ = unit(first_kv[0, h])
+            first_ku[h] = u
+            first_kn[h] = (u * gain_k).astype(BF16)
+
+        def against(first, rest, side):
+            return jnp.concatenate([dot(first, side, 1, 1), dot(rest, side, 1, 1)], axis=0)
+
+        scores = [against(first_kn[h], kn[h, :ROWS], qn0[h]) for h in heads]
+        d_probs = [against(first_kv[1, h], kvx[1, h, :ROWS], qd0[1, h]) for h in heads]
         d_scores = []
         for h in heads:
             bias = jnp.where(hidden, MASKED, bias_v[h, 0, :ROWS + SEG][:, :SEG])
@@ -316,24 +320,25 @@
             d_scores.append(prob * (d_probs[h] - delta))
             first_prob[h] = prob.astype(BF16)
             first_d_low[h] = d_scores[h].astype(BF16)
-        products = [dot(d_scores[h].astype(BF16), qd0[0, h], 1, 0) for h in heads]
+        products = [dot(d_scores[h].astype(BF16), qn0[h], 1, 0) for h in heads]
         for h in heads:
             tile = jnp.concatenate([d_scores[h], jnp.zeros((ROWS + SEG, SEG), F32)], axis=1)
             rows = fold_rows(h, jnp.concatenate([tile, jnp.zeros((SEG, PAIR), F32)], axis=0))
             for j in range(2):
                 table_v2[h, j] = table_v2[h, j] + rows[j]
-        gain = jnp.zeros((1, HEAD_DIM), F32)
         for h in heads:
-            dk = products[h]
-            first_dk[h] = dk
-            gain = gain + jnp.sum(dk[:SEG] * first_kv[0, h].astype(F32), axis=0, keepdims=True)
-            gain = gain + jnp.sum(dk[SEG:] * kvx[0, h, :ROWS].astype(F32), axis=0, keepdims=True)
-        extra_gain[...] = gain
+            first_dk[h] = products[h]
+        for n, (first, rest) in enumerate(((first_kn, kn), (first_ku, ku))):
+            gain = jnp.zeros((1, HEAD_DIM), F32)
+            for h in heads:
+                gain = gain + jnp.sum(products[h][:SEG] * first[h].astype(F32), axis=0, keepdims=True)
+                gain = gain + jnp.sum(products[h][SEG:] * rest[h, :ROWS].astype(F32), axis=0, keepdims=True)
+            extra_gain[n:n + 1] = gain
 
     def first_results(h):
         d_low = first_d_low[h]
         dv = dot(first_prob[h], qd0[1, h], 1, 0)
-        dq_from_before[h] = dot(d_low[:SEG], first_kv[0, h], 0, 0) + dot(d_low[SEG:], kvx[0, h, :ROWS], 0, 0)
+        dq_from_before[h] = dot(d_low[:SEG], first_kn[h], 0, 0) + dot(d_low[SEG:], kn[h, :ROWS], 0, 0)
         for n, part in enumerate((first_dk[h] * FACTOR, dv)):
             to_before_first[n, h] = part[:SEG].astype(BF16)
             from_before[n, h] = part[ROWS:].astype(BF16)
@@ -390,16 +395,28 @@
         def _():
             first_segment()
 
+    def near_keys():
+        for h in heads:
+            take_keys(h, PAIR, SEG)
+
+    def next_rows():
+        for h in heads:
+            take_keys(h, BEFORE + ROWS, SEG)
+            take_queries(h)
+
     @pl.when(x == nx - 1)
     def _():
         wait_left(0)
+        near_keys()
         work([(h, 0, 1) for h in heads])
         for h in heads:
             wait_left(1 + h)
+            take_keys(h, 0, PAIR)
             work([(h, 0, 0)], [(h, 0, False)])
             if not h:
                 greet_far()
         wait_right()
+        next_rows()
         work([(h, 1, b) for b in range(3) for h in heads], [(h, 1, True) for h in heads])
         if nx == 1:
             do_first()
@@ -408,12 +425,15 @@
         @pl.when(x == 0)
         def _():
             wait_right()
+            next_rows()
             work([(h, 1, b) for b in (1, 2) for h in heads])
             greet_far()
             wait_left(0)
+            near_keys()
             work([(h, p, 1 - p) for p in (1, 0) for h in heads], [(h, 1, False) for h in heads])
             for h in heads:
                 wait_left(1 + h)
+                take_keys(h, 0, PAIR)
                 work([(h, 0, 0)], [(h, 0, True)])
             do_first()
 
@@ -421,17 +441,22 @@
         @pl.when(jnp.logical_and(x > 0, x < nx - 1))
         def _():
             wait_left(0)
+            near_keys()
             work([(h, 0, 1) for h in heads])
             wait_right()
+            next_rows()
             work([(h, 1, b) for b in range(3) for h in heads], [(h, 1, False) for h in heads])
             greet_far()
             for h in heads:
                 wait_left(1 + h)
+                take_keys(h, 0, PAIR)
                 work([(h, 0, 0)], [(h, 0, True)])
 
-    gain = gain_v[0, 0] + gain_v[0, 1] + gain_v[1, 0] + gain_v[1, 1] + jnp.where(opens, extra_gain[...], 0.0)
     second = jnp.where(lane < SEG, table_v2[0, 1], table_v2[1, 1])
-    vec = jnp.concatenate([table_v2[0, 0], table_v2[1, 0], second, gain * FACTOR], axis=0)
+    gain_rows = [
+        (gain_v[0, 0, j] + gain_v[0, 1, j] + gain_v[1, 0, j] + gain_v[1, 1, j]
+         + jnp.where(opens, extra_gain[j:j + 1], 0.0)) * FACTOR for j in range(2)]
+    vec = jnp.concatenate([table_v2[0, 0], table_v2[1, 0], second, *gain_rows], axis=0)
     chip = y * nx + x
 
     to_neighbours = [
@@ -470,7 +495,7 @@
             to_after[0, h] = (dkx[h, BEFORE + ROWS:] * FACTOR).astype(BF16)
             to_after[1, h] = dvx[h, BEFORE + ROWS:].astype(BF16)
             for p in range(2):
-                dqx[h, p * PAIR:(p + 1) * PAIR] = dot(d_low_v[h, p], kvx[0, h, p * PAIR:(p + 3) * PAIR], 0, 0)
+                dqx[h, p * PAIR:(p + 1) * PAIR] = dot(d_low_v[h, p], kn[h, p * PAIR:(p + 3) * PAIR], 0, 0)
             dq_v[SEG:, lanes] = query_rows(dqx[h, :BEFORE], qu[h, SEG:], qr[h, SEG:])
 
     def send_results(when):
@@ -573,7 +598,7 @@
                 jnp.where(takes_next, 0.0, jnp.where(is_last, 0.0, from_after_first[n, h].astype(F32)))
                 + from_before[n, h].astype(F32), from_after[n, h].astype(F32)], axis=0) for n in range(2)]
         g = (dkx[h, BEFORE:BEFORE + ROWS] * FACTOR + sums_in[0]) * gain_k
-        u = ku[h]
+        u = ku[h, BEFORE:BEFORE + ROWS]
         dk_v[:, lanes] = (kr[h] * (g - u * jnp.mean(g * u, axis=-1, keepdims=True))).astype(BF16)
         dv_v[:, lanes] = (dvx[h, BEFORE:BEFORE + ROWS] + sums_in[1]).astype(BF16)
 
@@ -606,8 +631,8 @@
     for j in range(HEADS):
         dtab_v[j:j + 1, :PAIR] = result[j:j + 1]
         dtab_v[j:j + 1, PAIR:] = result[2:3, j * SEG:(j + 1) * SEG]
-    dgain_v[0:1] = result[3:] / gain_q
-    dgain_v[1:2] = result[3:] / gain_k
+    dgain_v[0:1] = result[3:4] / gain_q
+    dgain_v[1:2] = result[4:5]
 
 
 def write_out(*refs):
@@ -637,17 +662,19 @@
         in_specs=[hbm_spec] * 6,
         out_specs=(vmem_spec,) * 5,
         scratch_shapes=[
-            vmem(tile, BF16), vmem(tile, BF16), vmem((2, *tile), BF16), vmem((2, *first), BF16), vmem((2, *wide), BF16), vmem((2, *first), BF16),
+            vmem((2, *tile), BF16), vmem((2, *first), BF16), vmem((2, *wide), BF16), vmem((2, *first), BF16),
             vmem((2, HEAD_DIM), F32), vmem((HEADS, ENTRIES), F32),
-            vmem(tile, F32), vmem(tile, F32), vmem(tile, F32), vmem(tile, F32),
+            vmem(tile, BF16), vmem(first, BF16), vmem(tile, F32), vmem(tile, F32),
+            vmem(wide, BF16), vmem(wide, F32), vmem(tile, F32),
+            vmem(first, BF16), vmem(first, F32),
             vmem(pairs, F32), vmem(pairs, F32), vmem(pairs, F32),
             vmem(wide, F32), vmem(wide, F32), vmem(tile, F32), vmem((HEADS, 3 * PAIR, PAIR), F32),
-            vmem(pairs, BF16), vmem(pairs, BF16), vmem((HEADS, 2, 6, 1, PAIR), F32), vmem((HEADS, 2, 1, PAIR), F32),
-            vmem((HEADS, 2, 1, PAIR), F32), vmem((1, HEAD_DIM), F32),
+            vmem(pairs, BF16), vmem(pairs, BF16), vmem((HEADS, 2, 6, 1, PAIR), F32), vmem((HEADS, 2, 2, 1, PAIR), F32),
+            vmem((HEADS, 2, 1, PAIR), F32), vmem((2, HEAD_DIM), F32),
             vmem((HEADS, ROWS + SEG, SEG), BF16), vmem((HEADS, ROWS + SEG, SEG), BF16), vmem((HEADS, ROWS + SEG, HEAD_DIM), F32),
             vmem((2, HEADS, BEFORE, HEAD_DIM), BF16), vmem((2, HEADS, BEFORE, HEAD_DIM), BF16),
             vmem((2, *first), BF16), vmem((2, *first), BF16), vmem(first, F32), vmem((2, *first), BF16), vmem((2, *first), BF16),
-            vmem((nx, 4, HEAD_DIM), F32), vmem((nx * ny + nx + ny + 2 * nz, 4, HEAD_DIM), F32), vmem((2, 4, HEAD_DIM), F32), vmem((2 * nz, 4, HEAD_DIM), F32),
+            vmem((nx, 5, HEAD_DIM), F32), vmem((nx * ny + nx + ny + 2 * nz, 5, HEAD_DIM), F32), vmem((2, 5, HEAD_DIM), F32), vmem((2 * nz, 5, HEAD_DIM), F32),
             dma, dma, dma, dma, dma((HEADS + 1,)), dma, dma, dma,
             dma, dma, dma, dma, regular, regular, regular, regular,
         ],

time: 36.1 us -> 36.3 us (level)
  no operation moved by 1% of the time
where the time goes in v12:
time: 36.3 us; the launch traced here: 36.1 us
  Pallas kernels  35.4 us (98%)
  between operations  0.64 us (2%)
    pallas_call x1, Pallas kernels, local(): pl.pallas_call(functools.partial(kernel, sizes), out_shape=tuple((vmem(*o...  34.6 us
    pallas_call x1, Pallas kernels, local(): pl.pallas_call(write_out, out_shape=tuple((jax.ShapeDtypeStruct(*o) for o...  0.79 us

profile of v12, /device:TPU:1, one launch (start us, length us, event | category | flops | bytes accessed | tf_op | source)
XLA Modules:
  0.0 36.1 jit_solution(5496955693148292432)
XLA Ops:
  0.6 34.6 %segment_attention_grad.1 = (bf16[256,256]{1,0:T(8,128)(2,1)S(1)}, bf16[256,256]{1,0:T(8,128)(2,1)S(1)}, bf16[256,256]{1,0:T(8,128)(2,1)S(1)}, f32[2,192]{1,0:T(2,128)S(1)}, f32[2,128]{1,0:T(2,128)S(1)}) custom-call(bf16[256,256]{1,0:T(8,128)(2,1)} %q_hbm.1, bf16[256,256]{1,0:T(8,128)(2,1)} %k_hbm.1, bf16[256,256]{1,0:T(8,128)(2,1)} %v_hbm.1, ...), custom_call_target="tpu_custom_call" | custom-call | tf_op jit(solution)/shard_map/segment_attention_grad/pallas_call | solution.py:659
  35.3 0.8 %write_out.1 = (bf16[256,256]{1,0:T(8,128)(2,1)}, bf16[256,256]{1,0:T(8,128)(2,1)}, bf16[256,256]{1,0:T(8,128)(2,1)}, f32[2,192]{1,0:T(2,128)}, f32[2,128]{1,0:T(2,128)}) custom-call(bf16[256,256]{1,0:T(8,128)(2,1)S(1)} %get-tuple-element.15.refs_0_, bf16[256,256]{1,0:T(8,128)(2,1)S(1)} %get-tuple-element.16.refs_1_, ...), custom_call_target="tpu_custom_call" | custom-call | tf_op jit(solution)/shard_map/write_out/pallas_call | solution.py:685

commit v13 on v12

--- a/solution.py
+++ b/solution.py
@@ -141,6 +141,20 @@
 
     wait_bytes(kvx.at[:, :, :ROWS + SEG], load_sem)
     small_loads[0].wait()
+    gains = gains_v[...]
+    gain_q, gain_k = gains[0:1, :], gains[1:2, :]
+
+    def take_keys(h, first, size):
+        u, r = unit(kvx[0, h, first:first + size])
+        ku[h, first:first + size] = u
+        kn[h, first:first + size] = (u * gain_k).astype(BF16)
+        return r
+
+    def take_queries(h):
+        qn[h, BEFORE:] = (unit(qdx[0, h, BEFORE:])[0] * gain_q).astype(BF16)
+
+    for h in range(HEADS):
+        kr[h] = jnp.broadcast_to(take_keys(h, BEFORE, ROWS), (ROWS, HEAD_DIM))
     pl.semaphore_wait(barrier, sides + jnp.where(tp == 1, 1 + len(close), 1))
     go_on(forth[:1])
     go_on([copy for h in range(HEADS) for copy in back[h]], takes_back)
@@ -155,20 +169,7 @@
 
     wait_bytes(qdx.at[:, :, :BEFORE], more_sem)
     small_loads[1].wait()
-    gains = gains_v[...]
-    gain_q, gain_k = gains[0:1, :], gains[1:2, :]
-
-    def take_keys(h, first, size):
-        u, r = unit(kvx[0, h, first:first + size])
-        ku[h, first:first + size] = u
-        kn[h, first:first + size] = (u * gain_k).astype(BF16)
-        return r
-
-    def take_queries(h):
-        qn[h, BEFORE:] = (unit(qdx[0, h, BEFORE:])[0] * gain_q).astype(BF16)
-
     for h in range(HEADS):
-        kr[h] = jnp.broadcast_to(take_keys(h, BEFORE, ROWS), (ROWS, HEAD_DIM))
         for raw, normed, rows in (
                 (qd0[0, h], qn0.at[h], slice(0, SEG)),
                 (qdx[0, h, :BEFORE], qn.at[h, :BEFORE], slice(SEG, ROWS))):

time: 36.3 us -> 36.3 us (level)
  no operation moved by 1% of the time
where the time goes in v13:
time: 36.3 us; the launch traced here: 36.1 us
  Pallas kernels  35.4 us (98%)
  between operations  0.64 us (2%)
    pallas_call x1, Pallas kernels, local(): pl.pallas_call(functools.partial(kernel, sizes), out_shape=tuple((vmem(*o...  34.6 us
    pallas_call x1, Pallas kernels, local(): pl.pallas_call(write_out, out_shape=tuple((jax.ShapeDtypeStruct(*o) for o...  0.79 us

profile of v13, /device:TPU:1, one launch (start us, length us, event | category | flops | bytes accessed | tf_op | source)
XLA Modules:
  0.0 36.1 jit_solution(3550402956265698863)
XLA Ops:
  0.6 34.6 %segment_attention_grad.1 = (bf16[256,256]{1,0:T(8,128)(2,1)S(1)}, bf16[256,256]{1,0:T(8,128)(2,1)S(1)}, bf16[256,256]{1,0:T(8,128)(2,1)S(1)}, f32[2,192]{1,0:T(2,128)S(1)}, f32[2,128]{1,0:T(2,128)S(1)}) custom-call(bf16[256,256]{1,0:T(8,128)(2,1)} %q_hbm.1, bf16[256,256]{1,0:T(8,128)(2,1)} %k_hbm.1, bf16[256,256]{1,0:T(8,128)(2,1)} %v_hbm.1, ...), custom_call_target="tpu_custom_call" | custom-call | tf_op jit(solution)/shard_map/segment_attention_grad/pallas_call | solution.py:660
  35.3 0.8 %write_out.1 = (bf16[256,256]{1,0:T(8,128)(2,1)}, bf16[256,256]{1,0:T(8,128)(2,1)}, bf16[256,256]{1,0:T(8,128)(2,1)}, f32[2,192]{1,0:T(2,128)}, f32[2,128]{1,0:T(2,128)}) custom-call(bf16[256,256]{1,0:T(8,128)(2,1)S(1)} %get-tuple-element.15.refs_0_, bf16[256,256]{1,0:T(8,128)(2,1)S(1)} %get-tuple-element.16.refs_1_, ...), custom_call_target="tpu_custom_call" | custom-call | tf_op jit(solution)/shard_map/write_out/pallas_call | solution.py:686

commit v14 on v13

--- a/solution.py
+++ b/solution.py
@@ -145,16 +145,15 @@
     gain_q, gain_k = gains[0:1, :], gains[1:2, :]
 
     def take_keys(h, first, size):
-        u, r = unit(kvx[0, h, first:first + size])
+        u, _ = unit(kvx[0, h, first:first + size])
         ku[h, first:first + size] = u
         kn[h, first:first + size] = (u * gain_k).astype(BF16)
-        return r
 
     def take_queries(h):
         qn[h, BEFORE:] = (unit(qdx[0, h, BEFORE:])[0] * gain_q).astype(BF16)
 
     for h in range(HEADS):
-        kr[h] = jnp.broadcast_to(take_keys(h, BEFORE, ROWS), (ROWS, HEAD_DIM))
+        take_keys(h, BEFORE, ROWS)
     pl.semaphore_wait(barrier, sides + jnp.where(tp == 1, 1 + len(close), 1))
     go_on(forth[:1])
     go_on([copy for h in range(HEADS) for copy in back[h]], takes_back)
@@ -170,13 +169,8 @@
     wait_bytes(qdx.at[:, :, :BEFORE], more_sem)
     small_loads[1].wait()
     for h in range(HEADS):
-        for raw, normed, rows in (
-                (qd0[0, h], qn0.at[h], slice(0, SEG)),
-                (qdx[0, h, :BEFORE], qn.at[h, :BEFORE], slice(SEG, ROWS))):
-            u, r = unit(raw)
-            qu[h, rows] = u
-            qr[h, rows] = jnp.broadcast_to(r, u.shape)
-            normed[...] = (u * gain_q).astype(BF16)
+        for raw, normed in ((qd0[0, h], qn0.at[h]), (qdx[0, h, :BEFORE], qn.at[h, :BEFORE])):
+            normed[...] = (unit(raw)[0] * gain_q).astype(BF16)
 
     @pl.when(is_first)
     def _():
@@ -497,7 +491,10 @@
             to_after[1, h] = dvx[h, BEFORE + ROWS:].astype(BF16)
             for p in range(2):
                 dqx[h, p * PAIR:(p + 1) * PAIR] = dot(d_low_v[h, p], kn[h, p * PAIR:(p + 3) * PAIR], 0, 0)
-            dq_v[SEG:, lanes] = query_rows(dqx[h, :BEFORE], qu[h, SEG:], qr[h, SEG:])
+            qu[h], r = unit(qd0[0, h])
+            qr[h] = jnp.broadcast_to(r, (SEG, HEAD_DIM))
+            kr[h] = jnp.broadcast_to(unit(kvx[0, h, BEFORE:BEFORE + ROWS])[1], (ROWS, HEAD_DIM))
+            dq_v[SEG:, lanes] = query_rows(dqx[h, :BEFORE], *unit(qdx[0, h, :BEFORE]))
 
     def send_results(when):
         @pl.when(jnp.logical_and(when, place > 0))
@@ -590,7 +587,7 @@
         wait_bytes(kvx.at[:, :, :ROWS], after_recv)
 
     for h in range(HEADS):
-        dq_v[:SEG, h * HEAD_DIM:(h + 1) * HEAD_DIM] = query_rows(dq_from_before[h], qu[h, :SEG], qr[h, :SEG])
+        dq_v[:SEG, h * HEAD_DIM:(h + 1) * HEAD_DIM] = query_rows(dq_from_before[h], qu[h], qr[h])
 
     for h in range(HEADS):
         lanes = slice(h * HEAD_DIM, (h + 1) * HEAD_DIM)
@@ -665,7 +662,7 @@
         scratch_shapes=[
             vmem((2, *tile), BF16), vmem((2, *first), BF16), vmem((2, *wide), BF16), vmem((2, *first), BF16),
             vmem((2, HEAD_DIM), F32), vmem((HEADS, ENTRIES), F32),
-            vmem(tile, BF16), vmem(first, BF16), vmem(tile, F32), vmem(tile, F32),
+            vmem(tile, BF16), vmem(first, BF16), vmem(first, F32), vmem(first, F32),
             vmem(wide, BF16), vmem(wide, F32), vmem(tile, F32),
             vmem(first, BF16), vmem(first, F32),
             vmem(pairs, F32), vmem(pairs, F32), vmem(pairs, F32),

time: 36.3 us -> 36.3 us (level)
  no operation moved by 1% of the time
where the time goes in v14:
time: 36.3 us; the launch traced here: 36.1 us
  Pallas kernels  35.4 us (98%)
  between operations  0.64 us (2%)
    pallas_call x1, Pallas kernels, local(): pl.pallas_call(functools.partial(kernel, sizes), out_shape=tuple((vmem(*o...  34.6 us
    pallas_call x1, Pallas kernels, local(): pl.pallas_call(write_out, out_shape=tuple((jax.ShapeDtypeStruct(*o) for o...  0.79 us

profile of v14, /device:TPU:1, one launch (start us, length us, event | category | flops | bytes accessed | tf_op | source)
XLA Modules:
  0.0 36.1 jit_solution(3022508917575415098)
XLA Ops:
  0.6 34.6 %segment_attention_grad.1 = (bf16[256,256]{1,0:T(8,128)(2,1)S(1)}, bf16[256,256]{1,0:T(8,128)(2,1)S(1)}, bf16[256,256]{1,0:T(8,128)(2,1)S(1)}, f32[2,192]{1,0:T(2,128)S(1)}, f32[2,128]{1,0:T(2,128)S(1)}) custom-call(bf16[256,256]{1,0:T(8,128)(2,1)} %q_hbm.1, bf16[256,256]{1,0:T(8,128)(2,1)} %k_hbm.1, bf16[256,256]{1,0:T(8,128)(2,1)} %v_hbm.1, ...), custom_call_target="tpu_custom_call" | custom-call | tf_op jit(solution)/shard_map/segment_attention_grad/pallas_call | solution.py:657
  35.3 0.8 %write_out.1 = (bf16[256,256]{1,0:T(8,128)(2,1)}, bf16[256,256]{1,0:T(8,128)(2,1)}, bf16[256,256]{1,0:T(8,128)(2,1)}, f32[2,192]{1,0:T(2,128)}, f32[2,128]{1,0:T(2,128)}) custom-call(bf16[256,256]{1,0:T(8,128)(2,1)S(1)} %get-tuple-element.15.refs_0_, bf16[256,256]{1,0:T(8,128)(2,1)S(1)} %get-tuple-element.16.refs_1_, ...), custom_call_target="tpu_custom_call" | custom-call | tf_op jit(solution)/shard_map/write_out/pallas_call | solution.py:683

commit v15 on v13

--- a/solution.py
+++ b/solution.py
@@ -156,11 +156,11 @@
     for h in range(HEADS):
         kr[h] = jnp.broadcast_to(take_keys(h, BEFORE, ROWS), (ROWS, HEAD_DIM))
     pl.semaphore_wait(barrier, sides + jnp.where(tp == 1, 1 + len(close), 1))
+    go_on([plane_piece], closes_early)
     go_on(forth[:1])
     go_on([copy for h in range(HEADS) for copy in back[h]], takes_back)
     go_on(forth[1:], jnp.logical_and(tp == 0, place < total - 1))
     go_on(forth[1:2], jnp.logical_and(tp == 1, place < total - 1))
-    go_on([plane_piece], closes_early)
 
     @pl.when(tp == 1)
     def _():

time: 36.3 us -> 36.3 us (level)
  no operation moved by 1% of the time
where the time goes in v15:
time: 36.3 us; the launch traced here: 36.1 us
  Pallas kernels  35.4 us (98%)
  between operations  0.64 us (2%)
    pallas_call x1, Pallas kernels, local(): pl.pallas_call(functools.partial(kernel, sizes), out_shape=tuple((vmem(*o...  34.6 us
    pallas_call x1, Pallas kernels, local(): pl.pallas_call(write_out, out_shape=tuple((jax.ShapeDtypeStruct(*o) for o...  0.79 us

profile of v15, /device:TPU:1, one launch (start us, length us, event | category | flops | bytes accessed | tf_op | source)
XLA Modules:
  0.0 36.1 jit_solution(2888976646599866820)
XLA Ops:
  0.6 34.6 %segment_attention_grad.1 = (bf16[256,256]{1,0:T(8,128)(2,1)S(1)}, bf16[256,256]{1,0:T(8,128)(2,1)S(1)}, bf16[256,256]{1,0:T(8,128)(2,1)S(1)}, f32[2,192]{1,0:T(2,128)S(1)}, f32[2,128]{1,0:T(2,128)S(1)}) custom-call(bf16[256,256]{1,0:T(8,128)(2,1)} %q_hbm.1, bf16[256,256]{1,0:T(8,128)(2,1)} %k_hbm.1, bf16[256,256]{1,0:T(8,128)(2,1)} %v_hbm.1, ...), custom_call_target="tpu_custom_call" | custom-call | tf_op jit(solution)/shard_map/segment_attention_grad/pallas_call | solution.py:660
  35.3 0.8 %write_out.1 = (bf16[256,256]{1,0:T(8,128)(2,1)}, bf16[256,256]{1,0:T(8,128)(2,1)}, bf16[256,256]{1,0:T(8,128)(2,1)}, f32[2,192]{1,0:T(2,128)}, f32[2,128]{1,0:T(2,128)}) custom-call(bf16[256,256]{1,0:T(8,128)(2,1)S(1)} %get-tuple-element.15.refs_0_, bf16[256,256]{1,0:T(8,128)(2,1)S(1)} %get-tuple-element.16.refs_1_, ...), custom_call_target="tpu_custom_call" | custom-call | tf_op jit(solution)/shard_map/write_out/pallas_call | solution.py:686
